TPU v7x, 256 devices: a whole 4x4x8 slice. The times are simulated.
256 devices in a mesh: ep: 128 (over z, y, x), tp: 2 (over core).
Axes of the slice: x: 4, y: 4, z: 8, core: 2. Of those that a mesh axis runs over, the one named last changes fastest.
Arguments:
- tokens: bfloat16 [2048, 2048], P('ep', 'tp'), may hold values from -6 to 6
- state: float32 [2048, 4, 128, 128], P('ep', 'tp'), may hold values from -4 to 4
- norm_mix: float32 [2048], replicated, may hold values from 0.1 to 1.9
- w_query: bfloat16 [2048, 512], P(None, 'tp'), may hold values from -0.125 to 0.125
- w_key: bfloat16 [2048, 512], P(None, 'tp'), may hold values from -0.125 to 0.125
- w_value: bfloat16 [2048, 512], P(None, 'tp'), may hold values from -0.125 to 0.125
- w_out: bfloat16 [512, 2048], P('tp'), may hold values from -0.25 to 0.25
- norm_ffn: float32 [2048], P('tp'), may hold values from 0.1 to 1.9
- gate_vector: bfloat16 [2048], P('tp'), may hold values from -0.125 to 0.125
- dense_gate: bfloat16 [2048, 2816], P('tp', 'ep'), may hold values from -0.125 to 0.125
- dense_up: bfloat16 [2048, 2816], P('tp', 'ep'), may hold values from -0.125 to 0.125
- dense_down: bfloat16 [2816, 2048], P('ep', 'tp'), may hold values from -0.109375 to 0.109375
- exp_gate: bfloat16 [128, 2048, 176], P('ep', None, 'tp'), may hold values from -0.125 to 0.125
- exp_up: bfloat16 [128, 2048, 176], P('ep', None, 'tp'), may hold values from -0.125 to 0.125
- exp_down: bfloat16 [128, 176, 2048], P('ep', 'tp'), may hold values from -0.109375 to 0.109375
- routes: int32 [2048, 2], P('ep'), may hold values from 0 to 7, all different within a row; in each aligned block of 16 rows (0 to 15, 16 to 31, ...) at most 5 rows name the same one
- route_w: bfloat16 [2048, 2], P('ep'), may hold values from 0.099609375 to 1
Outputs:
- mixed: bfloat16 [2048, 2048], P('ep', 'tp')
- new_state: float32 [2048, 4, 128, 128], P('ep', 'tp')
Inputs may be any that keep to these rules, and one draw needn't show every extreme that they name: `routes`: each row names 2 different experts. Within the rows of one device (aligned blocks of 16 rows) no expert is named by more than 5 rows, a bound that some blocks reach.
All inputs are finite; a program needn't handle non-finite values.
Results may differ from a plain program's by a relative error of at most 0.014.
Values may be sent and summed in bfloat16 or wider, within the bound.
No kernel may reach another device: no remote copies, remote signals or barrier semaphores. Data moves between devices by JAX's collectives and lax.ppermute only.
A program may use at most 128 MiB of HBM per device.

v0:
```python
import jax
import jax.numpy as jnp
from jax import lax
from jax.experimental import pallas as pl
from jax.experimental.pallas import tpu as pltpu
from jax.sharding import Mesh
from jax.sharding import PartitionSpec as P


EXPERTS = 8
SLOTS = 3
EP = ("ep_0", "ep_1", "ep_2")
PLANE = ("ep_1", "ep_2")
PAD = 24
CHUNK = 80

epsilon = 1e-06
F32 = jnp.float32
BF16 = jnp.bfloat16


def swap(value):
    return lax.ppermute(value, "tp", [(0, 1), (1, 0)])


def along_z(value, shift):
    size = lax.axis_size("ep_0")
    return lax.ppermute(value, "ep_0", [(i, (i + shift) % size) for i in range(size)])


def to_all(value, axis):
    size = lax.axis_size(axis)
    copies = jnp.broadcast_to(value[None], (size, *value.shape))
    return lax.all_to_all(copies, axis, split_axis=0, concat_axis=0, tiled=True)


def dot(a, b):
    return jnp.dot(a, b, preferred_element_type=F32)


def dot_t(a, b):
    return lax.dot_general(a, b, (((1,), (1,)), ((), ())), preferred_element_type=F32)


def silu(v):
    return v / (1.0 + jnp.exp(-v))


def branch_kernel(
    hidden, core_ref, x_ref, g1, u1, d1, g2, u2, d2, own_ref, other_ref, out_ref, acc_ref
):
    half = own_ref.shape[1]
    width = 2 * half
    core = core_ref[0]
    here = pl.multiple_of(core * half, half)
    there = pl.multiple_of((1 - core) * half, half)
    total = x_ref.shape[0]
    step = total // 3
    for start in range(0, total, step):
        band = pl.ds(start, step)
        x = x_ref[band, :width]
        w = x_ref[band, width : width + 1].astype(F32)
        h1 = (w * silu(dot_t(x, g1[...])) * dot_t(x, u1[...])).astype(BF16)
        h2 = (w * silu(dot_t(x, g2[...])) * dot_t(x, u2[...])).astype(BF16)
        acc_ref[...] = dot(h1, d1[...]) + dot(h2, d2[...])
        pre = dot_t(x_ref[band, pl.ds(here, half)], own_ref[...])
        pre = pre + dot_t(x_ref[band, pl.ds(there, half)], other_ref[...])
        logit = pre[:, hidden : hidden + 1]
        gate = pltpu.roll(pre, 2 * PAD, 1)
        up = pltpu.roll(pre, PAD, 1)
        unit = lax.broadcasted_iota(jnp.int32, pre.shape, 1) % CHUNK
        live = (unit >= 2 * PAD) & (unit < 2 * PAD + hidden)
        scale = 0.5 / (1.0 + jnp.exp(-logit))
        hd = jnp.where(live, scale * silu(gate) * up, 0.0).astype(BF16)
        acc_ref[:, pl.ds(here, half)] += dot(hd, own_ref[...])
        acc_ref[:, pl.ds(there, half)] += dot(hd, other_ref[...])
        out_ref[band, :] = acc_ref[...].astype(BF16)


def experts_and_dense(core, x, own, other, dense_own, dense_other, hidden):
    rows, width = x.shape[0], 2 * dense_own.shape[1]
    vmem = pl.BlockSpec(memory_space=pltpu.VMEM)
    return pl.pallas_call(
        lambda *refs: branch_kernel(hidden, *refs),
        name="branch",
        out_shape=jax.ShapeDtypeStruct((rows, width), BF16),
        in_specs=[pl.BlockSpec(memory_space=pltpu.SMEM)] + [vmem] * 9,
        out_specs=vmem,
        scratch_shapes=[pltpu.VMEM((rows // 3, width), F32)],
    )(core.reshape(1), x, *own, *other, dense_own, dense_other)


def mixer_kernel(
    core_ref, x_ref, y_ref, gain_ref, wq, wk, wv, wo, state_ref, mix_ref, new_hbm,
    new_ref, turn_ref, read_ref, sem,
):
    rows, half = x_ref.shape
    heads, head = state_ref.shape[1], state_ref.shape[2]
    core = core_ref[0]
    here = pl.multiple_of(core * half, half)
    there = pl.multiple_of((1 - core) * half, half)
    x = x_ref[...].astype(F32)
    y = y_ref[...].astype(F32)
    total = jnp.sum(x * x, axis=1, keepdims=True) + jnp.sum(y * y, axis=1, keepdims=True)
    scale = lax.rsqrt(total / (2 * half) + epsilon)
    x = (x * scale * gain_ref[:, pl.ds(here, half)]).astype(BF16)
    y = (y * scale * gain_ref[:, pl.ds(there, half)]).astype(BF16)

    def project(ref):
        both = dot(x, ref[pl.ds(here, half), :]) + dot(y, ref[pl.ds(there, half), :])
        return both.astype(BF16).astype(F32)

    query = project(wq)
    key = project(wk) * head ** (-0.5)
    value = project(wv)
    turn_ref[0] = query.T
    turn_ref[1] = key.T
    decays = [
        jnp.where(core == 0, 1.0 - 2.0 ** (-3 - 2 * h), 1.0 - 2.0 ** (-3 - 2 * (h + heads)))
        for h in range(heads)
    ]
    group = 4
    copies = []
    for s in range(rows):
        for h in range(heads):
            part = slice(h * head, (h + 1) * head)
            q = turn_ref[0, part, s : s + 1]
            k = turn_ref[1, part, s : s + 1]
            new = decays[h] * state_ref[s, h] + k * value[s : s + 1, part]
            new_ref[s, h] = new
            read_ref[s : s + 1, part] = jnp.sum(q * new, axis=0, keepdims=True)
        if s % group == group - 1:
            band = pl.ds(s + 1 - group, group)
            copy = pltpu.make_async_copy(new_ref.at[band], new_hbm.at[band], sem.at[s // group])
            copy.start()
            copies.append(copy)
    outs = []
    for h in range(heads):
        read = read_ref[:, h * head : (h + 1) * head]
        centre = jnp.mean(read, axis=1, keepdims=True)
        spread = jnp.mean(jnp.square(read - centre), axis=1, keepdims=True)
        outs.append(((read - centre) * lax.rsqrt(spread + epsilon)).astype(BF16))
    mix = jnp.zeros(mix_ref.shape, F32)
    for h in range(heads):
        mix = mix + dot(outs[h], wo[h * head : (h + 1) * head, :])
    mix_ref[...] = mix.astype(BF16)
    for copy in copies:
        copy.wait()


def mixer(core, own, other, gain, wq, wk, wv, wo, state):
    rows, half = own.shape
    heads, head = state.shape[1], state.shape[2]
    vmem = pl.BlockSpec(memory_space=pltpu.VMEM)
    return pl.pallas_call(
        mixer_kernel,
        name="mixer",
        out_shape=(
            jax.ShapeDtypeStruct((rows, 2 * half), BF16),
            jax.ShapeDtypeStruct(state.shape, F32),
        ),
        in_specs=[pl.BlockSpec(memory_space=pltpu.SMEM)] + [vmem] * 8,
        out_specs=(vmem, pl.BlockSpec(memory_space=pl.ANY)),
        scratch_shapes=[
            pltpu.VMEM(state.shape, F32),
            pltpu.VMEM((2, heads * head, rows), F32),
            pltpu.VMEM((rows, heads * head), F32),
            pltpu.SemaphoreType.DMA((rows // 4,)),
        ],
    )(core.reshape(1), own, other, gain.reshape(1, 2 * half), wq, wk, wv, wo, state)


def third(index):
    return (index * 11) >> 5


def slots_kernel(
    core_ref, x_ref, y_ref, mix_ref, mix2_ref, gain_ref, gain2_ref, routes_ref, weights_ref,
    slot_ref, after_ref,
):
    rows, half = x_ref.shape
    core = core_ref[0]
    here = pl.multiple_of(core * half, half)
    there = pl.multiple_of((1 - core) * half, half)

    def add(ref, at):
        total = mix_ref[:, pl.ds(at, half)].astype(F32) + mix2_ref[:, pl.ds(at, half)].astype(F32)
        return (ref[...].astype(F32) + total).astype(BF16)

    after = add(x_ref, here)
    after_ref[...] = after
    x = after.astype(F32)
    y = add(y_ref, there).astype(F32)
    total = jnp.sum(x * x, axis=1, keepdims=True) + jnp.sum(y * y, axis=1, keepdims=True)
    scale = lax.rsqrt(total / (2 * half) + epsilon)
    x = (x * scale * gain_ref[...]).astype(BF16)
    y = (y * scale * gain2_ref[...]).astype(BF16)

    shape = (EXPERTS * SLOTS, rows)
    slot = lax.broadcasted_iota(jnp.int32, shape, 0)
    expert = third(slot)
    slot = slot - SLOTS * expert + SLOTS * core
    first = (routes_ref[0:1, :] == expert).astype(F32)
    second = (routes_ref[1:2, :] == expert).astype(F32)
    member = first + second
    earlier = lax.broadcasted_iota(jnp.int32, (rows, rows), 0) < lax.broadcasted_iota(
        jnp.int32, (rows, rows), 1
    )
    place = dot(member.astype(BF16), earlier.astype(F32).astype(BF16))
    select = jnp.where(place == slot.astype(F32), member, 0.0)
    weight = first * weights_ref[0:1, :].astype(F32) + second * weights_ref[1:2, :].astype(F32)
    weight = jnp.sum(select * weight, axis=1, keepdims=True)
    select = select.astype(BF16)
    slot_ref[:, pl.ds(here, half)] = dot(select, x).astype(BF16)
    slot_ref[:, pl.ds(there, half)] = dot(select, y).astype(BF16)
    slot_ref[:, 2 * half :] = jnp.broadcast_to(weight, (EXPERTS * SLOTS, 128)).astype(BF16)


def to_slots(core, own, other, mix, mix2, gain, gain2, routes, route_w):
    rows, half = own.shape
    vmem = pl.BlockSpec(memory_space=pltpu.VMEM)
    return pl.pallas_call(
        slots_kernel,
        name="slots",
        out_shape=(
            jax.ShapeDtypeStruct((EXPERTS * SLOTS, 2 * half + 128), BF16),
            jax.ShapeDtypeStruct((rows, half), BF16),
        ),
        in_specs=[pl.BlockSpec(memory_space=pltpu.SMEM)] + [vmem] * 8,
        out_specs=(vmem, vmem),
    )(
        core.reshape(1), own, other, mix, mix2, gain.reshape(1, half), gain2.reshape(1, half),
        routes.T, route_w.astype(F32).T,
    )


def home_kernel(home_ref, after_ref, routes_ref, out_ref):
    rows = after_ref.shape[0]
    shape = (rows, home_ref.shape[0])
    slot = lax.broadcasted_iota(jnp.int32, shape, 1)
    expert = third(slot >> 1)
    slot = slot - 2 * SLOTS * expert
    member = (routes_ref[:, 0:1] == expert).astype(F32) + (routes_ref[:, 1:2] == expert).astype(F32)
    earlier = lax.broadcasted_iota(jnp.int32, (rows, rows), 1) < lax.broadcasted_iota(
        jnp.int32, (rows, rows), 0
    )
    place = dot(earlier.astype(F32).astype(BF16), member.astype(BF16))
    select = jnp.where(place == slot.astype(F32), member, 0.0).astype(BF16)
    total = after_ref[...].astype(F32) + dot(select, home_ref[...])
    out_ref[...] = total.astype(BF16)


def at_home(home, after, routes):
    vmem = pl.BlockSpec(memory_space=pltpu.VMEM)
    return pl.pallas_call(
        home_kernel,
        name="home",
        out_shape=jax.ShapeDtypeStruct(after.shape, BF16),
        in_specs=[vmem] * 3,
        out_specs=vmem,
    )(home, after, routes)


def layer(
    tokens, state, norm_mix, w_query, w_key, w_value, w_out, norm_ffn, gate_vector,
    dense_gate, dense_up, dense_down, exp_gate, exp_up, exp_down, routes, route_w,
):
    core = lax.axis_index("tp")
    half = tokens.shape[1]
    width = 2 * half
    hidden = dense_gate.shape[1]

    def fill(size):
        return jnp.zeros((size, half), BF16)

    other_x = swap(tokens)
    other_gain = swap(norm_ffn)
    packed = jnp.concatenate(
        [
            dense_gate.T,
            gate_vector[None],
            fill(PAD - hidden - 1),
            dense_up.T,
            fill(PAD - hidden),
            dense_down,
            fill(CHUNK - 2 * PAD - hidden),
        ],
        axis=0,
    )
    mine = (exp_gate[0].T, exp_up[0].T, exp_down[0])
    theirs = tuple(swap(weights) for weights in mine)

    mix, new_state = mixer(core, tokens, other_x, norm_mix, w_query, w_key, w_value, w_out, state)
    mix2 = swap(mix)
    slot_rows, after = to_slots(
        core, tokens, other_x, mix, mix2, norm_ffn, other_gain, routes, route_w
    )
    at_plane = lax.all_to_all(
        slot_rows.reshape(EXPERTS, SLOTS, width + 128), "ep_0", 0, 0, tiled=True
    ).reshape(EXPERTS * SLOTS, width + 128)
    pieces = [packed] + [along_z(packed, k) for k in range(1, EXPERTS)]
    dense_own = jnp.concatenate(pieces, axis=0)
    dense_other = swap(dense_own)
    gathered = to_all(at_plane, PLANE)
    chips = gathered.shape[0]
    partial = experts_and_dense(
        core,
        gathered.reshape(-1, width + 128),
        mine,
        theirs,
        dense_own,
        dense_other,
        hidden,
    )
    back = lax.all_to_all(partial.reshape(chips, EXPERTS * SLOTS, width), PLANE, 0, 0, tiled=True)
    summed = jnp.sum(back.astype(F32), axis=0).astype(BF16)
    send = summed.reshape(EXPERTS, SLOTS, 2, half).transpose(0, 2, 1, 3)
    home = lax.all_to_all(
        send.reshape(2 * EXPERTS, SLOTS, half), ("ep_0", "tp"), 0, 0, tiled=True
    ).reshape(2 * EXPERTS * SLOTS, half)
    return (at_home(home, after, routes), new_state)


def solution(mesh):
    finer = Mesh(mesh.devices.reshape(8, 4, 4, mesh.shape["tp"]), ("ep_0", "ep_1", "ep_2", "tp"))
    in_specs = (
        P(EP, "tp"),
        P(EP, "tp", None, None),
        P(),
        P(None, "tp"),
        P(None, "tp"),
        P(None, "tp"),
        P("tp", None),
        P("tp"),
        P("tp"),
        P("tp", EP),
        P("tp", EP),
        P(EP, "tp"),
        P(EP, None, "tp"),
        P(EP, None, "tp"),
        P(EP, "tp", None),
        P(EP, None),
        P(EP, None),
    )
    out_specs = (P(EP, "tp"), P(EP, "tp", None, None))
    return jax.shard_map(layer, mesh=finer, in_specs=in_specs, out_specs=out_specs, check_vma=False)
```

profile of v0, /device:TPU:1, one launch (start us, length us, event | category | flops | bytes accessed | tf_op | source)
XLA Modules:
  0.0 146.6 jit_solution(15771493454581698674)
XLA Ops:
  0.6 3.3 %collective-permute-start = (bf16[16,1024]{1,0:T(8,128)(2,1)}, bf16[16,1024]{1,0:T(8,128)(2,1)S(1)}, u32[]{:S(2)}, u32[]{:S(2)}) collective-permute-start(bf16[16,1024]{1,0:T(8,128)(2,1)} %x_ref.3), channel_id=1, source_target_pairs={{0,1},{1,0},{2,3},{3,2},{4,5},{5,4},{6,7},{7,6},{8,9},{9,8},{10,11... | collective-permute-start | bytes 98312 | tf_op jit(solution)/shard_map/ppermute | solution.py:23
  3.9 0.1 collective-permute-start.2
  4.0 1.0 collective-permute-done.y_ref
  5.0 0.6 copy-done.15
  5.6 6.6 %mixer.1 = (bf16[16,2048]{1,0:T(8,128)(2,1)}, f32[16,2,128,128]{3,2,1,0:T(8,128)}) custom-call(s32[1]{0:T(128)} %bitcast.core_ref.refs_0_, bf16[16,1024]{1,0:T(8,128)(2,1)} %x_ref.3, bf16[16,1024]{1,0:T(8,128)(2,1)} %copy-done.15, f32[1,2048]{1,0:T(1,128)} %bitcast.33, bf16[2048,256]{1,0:T(8,128)(2,1)} %wq.1, bf16[2048,256]{1,0:T(8,128)(2,1)} %wk.1, ...), custom_call_target="tpu_custom_call" | custom-call | tf_op jit(solution)/shard_map/mixer/pallas_call | solution.py:155
  12.2 0.4 collective-permute-start.1
  12.6 0.6 convert_bitcast_fusion.weights_ref
  13.2 0.5 collective-permute-done.1.mix2_ref
  13.7 0.1 copy-done.18
  13.8 0.6 copy-done.16
  14.4 1.9 %slots.1 = (bf16[24,2176]{1,0:T(8,128)(2,1)}, bf16[16,1024]{1,0:T(8,128)(2,1)}) custom-call(s32[1]{0:T(128)} %bitcast.core_ref.refs_0_, bf16[16,1024]{1,0:T(8,128)(2,1)} %x_ref.3, bf16[16,1024]{1,0:T(8,128)(2,1)} %copy-done.15, bf16[16,2048]{1,0:T(8,128)(2,1)} %get-tuple-element.6.mix_ref, bf16[16,2048]{1,0:T(8,128)(2,1)} %copy-done.16, f32[1,1024]{1,0:T(1,128)} %bitcast.35, ...), custom_call_target="tpu_custom_call" | custom-call | tf_op jit(solution)/shard_map/slots/pallas_call | solution.py:222
  16.2 1.6 %reshape.41 = bf16[8,3,2176]{2,1,0:T(4,128)(2,1)} reshape(bf16[24,2176]{1,0:T(8,128)(2,1)} %get-tuple-element.7) | data formatting | bytes 208896 | tf_op jit(solution)/shard_map/reshape | solution.py:299
  17.8 6.5 %all-to-all-start = ((bf16[8,3,2176]{2,1,0:T(4,128)(2,1)}), bf16[8,3,2176]{2,1,0:T(4,128)(2,1)S(1)}, u32[]{:S(2)}, u32[]{:S(2)}) async-start(bf16[8,3,2176]{2,1,0:T(4,128)(2,1)} %reshape.41), calls=%async_computation | async-start | bytes 278528 | tf_op jit(solution)/shard_map/all_to_all | solution.py:298
  24.4 0.2 concatenate.7
  24.6 4.5 %collective-permute-start.10 = (bf16[80,1024]{1,0:T(8,128)(2,1)S(1)}, bf16[80,1024]{1,0:T(8,128)(2,1)S(1)}, u32[]{:S(2)}, u32[]{:S(2)}) collective-permute-start(bf16[80,1024]{1,0:T(8,128)(2,1)S(1)} %concatenate.7), channel_id=1, source_target_pairs={{0,160},{32,192},{64,224},{96,0},{128,32},{160,64},{192,96},{224,1... | collective-permute-start | bytes 491528 | tf_op jit(solution)/shard_map/ppermute | solution.py:28
  29.2 1.2 collective-permute-start.11
  30.3 2.1 %all-to-all-done = bf16[8,3,2176]{2,1,0:T(4,128)(2,1)S(1)} async-done(((bf16[8,3,2176]{2,1,0:T(4,128)(2,1)}), bf16[8,3,2176]{2,1,0:T(4,128)(2,1)S(1)}, u32[]{:S(2)}, u32[]{:S(2)}) %all-to-all-start) | async-done | bytes 104480 | tf_op jit(solution)/shard_map/all_to_all | solution.py:298
  32.4 0.1 broadcast_in_dim.19
  32.5 1.3 broadcast_in_dim.20
  33.9 6.8 %all-to-all-start.1 = ((bf16[16,24,2176]{2,1,0:T(8,128)(2,1)}), bf16[16,24,2176]{2,1,0:T(8,128)(2,1)S(1)}, u32[]{:S(2)}, u32[]{:S(2)}) async-start(bf16[16,24,2176]{2,1,0:T(8,128)(2,1)} %broadcast_in_dim.20), calls=%async_computation.1 | async-start | bytes 3342336 | tf_op jit(solution)/shard_map/all_to_all | solution.py:34
  40.6 0.0 copy-start.2
  40.6 0.1 collective-permute-start.12
  40.7 1.5 collective-permute-start.6
  42.2 2.1 %collective-permute-start.8 = (bf16[80,1024]{1,0:T(8,128)(2,1)S(1)}, bf16[80,1024]{1,0:T(8,128)(2,1)S(1)}, u32[]{:S(2)}, u32[]{:S(2)}) collective-permute-start(bf16[80,1024]{1,0:T(8,128)(2,1)S(1)} %concatenate.7), channel_id=1, source_target_pairs={{0,96},{32,128},{64,160},{96,192},{128,224},{160,0},{192,32},{224,... | collective-permute-start | bytes 491528 | tf_op jit(solution)/shard_map/ppermute | solution.py:28
  44.3 4.5 %collective-permute-done.11 = bf16[80,1024]{1,0:T(8,128)(2,1)S(1)} collective-permute-done((bf16[80,1024]{1,0:T(8,128)(2,1)S(1)}, bf16[80,1024]{1,0:T(8,128)(2,1)S(1)}, u32[]{:S(2)}, u32[]{:S(2)}) %collective-permute-start.11) | collective-permute-done | bytes 163872 | tf_op jit(solution)/shard_map/ppermute | solution.py:28
  48.8 2.9 %collective-permute-start.9 = (bf16[80,1024]{1,0:T(8,128)(2,1)S(1)}, bf16[80,1024]{1,0:T(8,128)(2,1)}, u32[]{:S(2)}, u32[]{:S(2)}) collective-permute-start(bf16[80,1024]{1,0:T(8,128)(2,1)S(1)} %concatenate.7), channel_id=1, source_target_pairs={{0,128},{32,160},{64,192},{96,224},{128,0},{160,32},{192,64},{224,... | collective-permute-start | bytes 491528 | tf_op jit(solution)/shard_map/ppermute | solution.py:28
  51.7 15.4 %collective-permute-done.8 = bf16[80,1024]{1,0:T(8,128)(2,1)S(1)} collective-permute-done((bf16[80,1024]{1,0:T(8,128)(2,1)S(1)}, bf16[80,1024]{1,0:T(8,128)(2,1)S(1)}, u32[]{:S(2)}, u32[]{:S(2)}) %collective-permute-start.8) | collective-permute-done | bytes 163872 | tf_op jit(solution)/shard_map/ppermute | solution.py:28
  67.2 0.7 copy-done.14
  67.8 6.7 %concatenate.8.refs_8_ = bf16[640,1024]{1,0:T(8,128)(2,1)S(1)} concatenate(bf16[22,1024]{1,0:T(8,128)(2,1)S(1)} %bitcast.30, bf16[1,1024]{1,0:T(2,128)(2,1)S(1)} %broadcast_in_dim.21, bf16[1,1024]{1,0:T(2,128)(2,1)S(1)} %broadcast_in_dim.22, bf16[22,1024]{1,0:T(8,128)(2,1)S(1)} %bitcast.32, bf16[2,1024]{1,0:T(2,128)(2,1)S(1)} %broadcast_in_dim.23, ...), dimensions={0} | concatenate | bytes 2621440 | tf_op jit(solution)/shard_map/concatenate | solution.py:302
  74.6 4.7 %collective-permute-start.13 = (bf16[640,1024]{1,0:T(8,128)(2,1)S(1)}, bf16[640,1024]{1,0:T(8,128)(2,1)}, u32[]{:S(2)}, u32[]{:S(2)}) collective-permute-start(bf16[640,1024]{1,0:T(8,128)(2,1)S(1)} %concatenate.8.refs_8_), channel_id=1, source_target_pairs={{0,1},{1,0},{2,3},{3,2},{4,5},{5,4},{6,7},{7,6},{8,9},{9,8},{10,11... | collective-permute-start | bytes 3932168 | tf_op jit(solution)/shard_map/ppermute | solution.py:23
  79.3 0.1 collective-permute-start.3
  79.4 0.4 collective-permute-start.4
  79.8 0.1 collective-permute-start.5
  79.9 2.6 %collective-permute-done.3.refs_5_ = bf16[88,2048]{1,0:T(8,128)(2,1)S(1)} collective-permute-done((bf16[88,2048]{1,0:T(8,128)(2,1)S(1)}, bf16[88,2048]{1,0:T(8,128)(2,1)S(1)}, u32[]{:S(2)}, u32[]{:S(2)}) %collective-permute-start.3) | collective-permute-done | bytes 360480 | tf_op jit(solution)/shard_map/ppermute | solution.py:23
  82.5 0.5 collective-permute-done.4.refs_6_
  83.0 0.5 collective-permute-done.5.refs_7_
  83.5 0.2 copy-done.4
  83.7 0.7 copy-done.5
  84.5 1.2 copy-done
  85.7 12.0 %branch.1 = bf16[384,2048]{1,0:T(8,128)(2,1)} custom-call(s32[1]{0:T(128)} %bitcast.core_ref.refs_0_, bf16[384,2176]{1,0:T(8,128)(2,1)} %bitcast.20, bf16[88,2048]{1,0:T(8,128)(2,1)} %bitcast.23, bf16[88,2048]{1,0:T(8,128)(2,1)} %bitcast.26, bf16[88,2048]{1,0:T(8,128)(2,1)} %bitcast.28, bf16[88,2048]{1,0:T(8,128)(2,1)} %copy-done.3, ...), custom_call_target="tpu_custom_call" | custom-call | tf_op jit(solution)/shard_map/branch/pallas_call | solution.py:83
  97.7 28.9 %all_to_all.20 = bf16[16,24,2048]{2,1,0:T(8,128)(2,1)S(1)} all-to-all(bf16[16,24,2048]{2,1,0:T(8,128)(2,1)} %bitcast.21), channel_id=1, replica_groups=mesh['ep_0'=8,'ep_1'=4,'ep_2'=4,'tp'=2] {'ep_1','ep_2'}, dimensions={0} | all-to-all | bytes 3145728 | tf_op jit(solution)/shard_map/all_to_all | solution.py:315
  126.6 0.3 reduce_sum.12
  126.9 0.7 copy.27
  127.7 7.5 %all-to-all-start.3 = ((bf16[16,3,1024]{2,1,0:T(4,128)(2,1)}), bf16[16,3,1024]{2,1,0:T(4,128)(2,1)S(1)}, u32[]{:S(2)}, u32[]{:S(2)}) async-start(bf16[16,3,1024]{2,1,0:T(4,128)(2,1)} %bitcast.18), calls=%async_computation.3 | async-start | bytes 262144 | tf_op jit(solution)/shard_map/all_to_all | solution.py:318
  135.2 0.7 copy.26.routes_ref
  135.8 8.2 %all-to-all-done.3 = bf16[16,3,1024]{2,1,0:T(4,128)(2,1)S(1)} async-done(((bf16[16,3,1024]{2,1,0:T(4,128)(2,1)}), bf16[16,3,1024]{2,1,0:T(4,128)(2,1)S(1)}, u32[]{:S(2)}, u32[]{:S(2)}) %all-to-all-start.3) | async-done | bytes 98336 | tf_op jit(solution)/shard_map/all_to_all | solution.py:318
  144.0 0.7 reshape.46.home_ref
  144.8 1.8 %home.1 = bf16[16,1024]{1,0:T(8,128)(2,1)} custom-call(bf16[48,1024]{1,0:T(8,128)(2,1)} %reshape.46.home_ref, bf16[16,1024]{1,0:T(8,128)(2,1)} %get-tuple-element.8.after_ref, s32[16,2]{1,0:T(8,128)} %copy.26.routes_ref), custom_call_target="tpu_custom_call" | custom-call | tf_op jit(solution)/shard_map/home/pallas_call | solution.py:255
  (48 shorter events, 0.2 us)
Async XLA Ops:
  0.6 4.4 %collective-permute-start = (bf16[16,1024]{1,0:T(8,128)(2,1)}, bf16[16,1024]{1,0:T(8,128)(2,1)S(1)}, u32[]{:S(2)}, u32[]{:S(2)}) collective-permute-start(bf16[16,1024]{1,0:T(8,128)(2,1)} %x_ref.3), channel_id=1, source_target_pairs={{0,1},{1,0},{2,3},{3,2},{4,5},{5,4},{6,7},{7,6},{8,9},{9,8},{10,11... | collective-permute-start | bytes 98312 | tf_op jit(solution)/shard_map/ppermute | solution.py:23
  3.9 9.3 %collective-permute-start.2 = (f32[1024]{0:T(1024)}, f32[1024]{0:T(1024)S(1)}, u32[]{:S(2)}, u32[]{:S(2)}) collective-permute-start(f32[1024]{0:T(1024)} %param.24), channel_id=1, source_target_pairs={{0,1},{1,0},{2,3},{3,2},{4,5},{5,4},{6,7},{7,6},{8,9},{9,8},{10,11... | collective-permute-start | bytes 12296 | tf_op jit(solution)/shard_map/ppermute | solution.py:23
  5.0 0.6 copy-start.15
  5.6 7.0 %copy-start.20 = (bf16[16,2]{0,1:T(2,128)(2,1)S(1)}, bf16[16,2]{0,1:T(2,128)(2,1)}, u32[]{:S(2)}) copy-start(bf16[16,2]{0,1:T(2,128)(2,1)} %param.33) | copy-start | bytes 196
  5.6 18.7 %copy-start.19 = (bf16[1024]{0:T(1024)(128)(2,1)S(1)}, bf16[1024]{0:T(1024)(128)(2,1)}, u32[]{:S(2)}) copy-start(bf16[1024]{0:T(1024)(128)(2,1)} %param.25) | copy-start | bytes 6148
  5.6 18.8 %copy-start.6 = (bf16[1024,22]{0,1:T(8,128)(2,1)S(1)}, bf16[1024,22]{0,1:T(8,128)(2,1)}, u32[]{:S(2)}) copy-start(bf16[1024,22]{0,1:T(8,128)(2,1)} %param.26) | copy-start | bytes 135172
  5.6 18.8 %copy-start.7 = (bf16[1024,22]{0,1:T(8,128)(2,1)S(1)}, bf16[1024,22]{0,1:T(8,128)(2,1)}, u32[]{:S(2)}) copy-start(bf16[1024,22]{0,1:T(8,128)(2,1)} %param.27) | copy-start | bytes 135172
  5.6 18.8 %copy-start.8 = (bf16[22,1024]{1,0:T(8,128)(2,1)S(1)}, bf16[22,1024]{1,0:T(8,128)(2,1)}, u32[]{:S(2)}) copy-start(bf16[22,1024]{1,0:T(8,128)(2,1)} %param.28) | copy-start | bytes 135172
  12.2 1.6 %collective-permute-start.1 = (bf16[16,2048]{1,0:T(8,128)(2,1)}, bf16[16,2048]{1,0:T(8,128)(2,1)S(1)}, u32[]{:S(2)}, u32[]{:S(2)}) collective-permute-start(bf16[16,2048]{1,0:T(8,128)(2,1)} %get-tuple-element.6.mix_ref), channel_id=1, source_target_pairs={{0,1},{1,0},{2,3},{3,2},{4,5},{5,4},{6,7},{7,6},{8,9},{9,8},{10,11... | collective-permute-start | bytes 196616 | tf_op jit(solution)/shard_map/ppermute | solution.py:23
  13.2 0.6 copy-start.18
  13.7 0.6 copy-start.16
  17.8 14.6 %all-to-all-start = ((bf16[8,3,2176]{2,1,0:T(4,128)(2,1)}), bf16[8,3,2176]{2,1,0:T(4,128)(2,1)S(1)}, u32[]{:S(2)}, u32[]{:S(2)}) async-start(bf16[8,3,2176]{2,1,0:T(4,128)(2,1)} %reshape.41), calls=%async_computation | async-start | bytes 278528 | tf_op jit(solution)/shard_map/all_to_all | solution.py:298
  24.6 17.6 %collective-permute-start.10 = (bf16[80,1024]{1,0:T(8,128)(2,1)S(1)}, bf16[80,1024]{1,0:T(8,128)(2,1)S(1)}, u32[]{:S(2)}, u32[]{:S(2)}) collective-permute-start(bf16[80,1024]{1,0:T(8,128)(2,1)S(1)} %concatenate.7), channel_id=1, source_target_pairs={{0,160},{32,192},{64,224},{96,0},{128,32},{160,64},{192,96},{224,1... | collective-permute-start | bytes 491528 | tf_op jit(solution)/shard_map/ppermute | solution.py:28
  29.2 19.6 %collective-permute-start.11 = (bf16[80,1024]{1,0:T(8,128)(2,1)S(1)}, bf16[80,1024]{1,0:T(8,128)(2,1)S(1)}, u32[]{:S(2)}, u32[]{:S(2)}) collective-permute-start(bf16[80,1024]{1,0:T(8,128)(2,1)S(1)} %concatenate.7), channel_id=1, source_target_pairs={{0,192},{32,224},{64,0},{96,32},{128,64},{160,96},{192,128},{224,1... | collective-permute-start | bytes 491528 | tf_op jit(solution)/shard_map/ppermute | solution.py:28
  33.9 50.6 %all-to-all-start.1 = ((bf16[16,24,2176]{2,1,0:T(8,128)(2,1)}), bf16[16,24,2176]{2,1,0:T(8,128)(2,1)S(1)}, u32[]{:S(2)}, u32[]{:S(2)}) async-start(bf16[16,24,2176]{2,1,0:T(8,128)(2,1)} %broadcast_in_dim.20), calls=%async_computation.1 | async-start | bytes 3342336 | tf_op jit(solution)/shard_map/all_to_all | solution.py:34
  40.6 38.7 %copy-start.2 = (bf16[1,2048,88]{1,2,0:T(8,128)(2,1)S(1)}, bf16[1,2048,88]{1,2,0:T(8,128)(2,1)}, u32[]{:S(2)}) copy-start(bf16[1,2048,88]{1,2,0:T(8,128)(2,1)} %param.29) | copy-start | bytes 1081348
  40.6 11.0 %collective-permute-start.12 = (bf16[80,1024]{1,0:T(8,128)(2,1)S(1)}, bf16[80,1024]{1,0:T(8,128)(2,1)S(1)}, u32[]{:S(2)}, u32[]{:S(2)}) collective-permute-start(bf16[80,1024]{1,0:T(8,128)(2,1)S(1)} %concatenate.7), channel_id=1, source_target_pairs={{0,224},{32,0},{64,32},{96,64},{128,96},{160,128},{192,160},{224,1... | collective-permute-start | bytes 491528 | tf_op jit(solution)/shard_map/ppermute | solution.py:28
  40.7 10.9 %collective-permute-start.6 = (bf16[80,1024]{1,0:T(8,128)(2,1)S(1)}, bf16[80,1024]{1,0:T(8,128)(2,1)S(1)}, u32[]{:S(2)}, u32[]{:S(2)}) collective-permute-start(bf16[80,1024]{1,0:T(8,128)(2,1)S(1)} %concatenate.7), channel_id=1, source_target_pairs={{0,32},{32,64},{64,96},{96,128},{128,160},{160,192},{192,224},{224... | collective-permute-start | bytes 491528 | tf_op jit(solution)/shard_map/ppermute | solution.py:28
  42.2 9.5 %collective-permute-start.7 = (bf16[80,1024]{1,0:T(8,128)(2,1)S(1)}, bf16[80,1024]{1,0:T(8,128)(2,1)S(1)}, u32[]{:S(2)}, u32[]{:S(2)}) collective-permute-start(bf16[80,1024]{1,0:T(8,128)(2,1)S(1)} %concatenate.7), channel_id=1, source_target_pairs={{0,64},{32,96},{64,128},{96,160},{128,192},{160,224},{192,0},{224,... | collective-permute-start | bytes 491528 | tf_op jit(solution)/shard_map/ppermute | solution.py:28
  42.2 24.9 %copy-start.9 = (bf16[80,1024]{1,0:T(8,128)(2,1)}, bf16[80,1024]{1,0:T(8,128)(2,1)S(1)}, u32[]{:S(2)}) copy-start(bf16[80,1024]{1,0:T(8,128)(2,1)S(1)} %collective-permute-done.10) | copy-start | bytes 491524
  42.2 24.9 %collective-permute-start.8 = (bf16[80,1024]{1,0:T(8,128)(2,1)S(1)}, bf16[80,1024]{1,0:T(8,128)(2,1)S(1)}, u32[]{:S(2)}, u32[]{:S(2)}) collective-permute-start(bf16[80,1024]{1,0:T(8,128)(2,1)S(1)} %concatenate.7), channel_id=1, source_target_pairs={{0,96},{32,128},{64,160},{96,192},{128,224},{160,0},{192,32},{224,... | collective-permute-start | bytes 491528 | tf_op jit(solution)/shard_map/ppermute | solution.py:28
  48.8 18.3 %copy-start.10 = (bf16[80,1024]{1,0:T(8,128)(2,1)}, bf16[80,1024]{1,0:T(8,128)(2,1)S(1)}, u32[]{:S(2)}) copy-start(bf16[80,1024]{1,0:T(8,128)(2,1)S(1)} %collective-permute-done.11) | copy-start | bytes 491524
  48.8 19.0 %collective-permute-start.9 = (bf16[80,1024]{1,0:T(8,128)(2,1)S(1)}, bf16[80,1024]{1,0:T(8,128)(2,1)}, u32[]{:S(2)}, u32[]{:S(2)}) collective-permute-start(bf16[80,1024]{1,0:T(8,128)(2,1)S(1)} %concatenate.7), channel_id=1, source_target_pairs={{0,128},{32,160},{64,192},{96,224},{128,0},{160,32},{192,64},{224,... | collective-permute-start | bytes 491528 | tf_op jit(solution)/shard_map/ppermute | solution.py:28
  51.7 15.5 %copy-start.11 = (bf16[80,1024]{1,0:T(8,128)(2,1)}, bf16[80,1024]{1,0:T(8,128)(2,1)S(1)}, u32[]{:S(2)}) copy-start(bf16[80,1024]{1,0:T(8,128)(2,1)S(1)} %collective-permute-done.12) | copy-start | bytes 491524
  51.7 15.4 %copy-start.12 = (bf16[80,1024]{1,0:T(8,128)(2,1)}, bf16[80,1024]{1,0:T(8,128)(2,1)S(1)}, u32[]{:S(2)}) copy-start(bf16[80,1024]{1,0:T(8,128)(2,1)S(1)} %collective-permute-done.6) | copy-start | bytes 491524
  51.7 15.4 %copy-start.13 = (bf16[80,1024]{1,0:T(8,128)(2,1)}, bf16[80,1024]{1,0:T(8,128)(2,1)S(1)}, u32[]{:S(2)}) copy-start(bf16[80,1024]{1,0:T(8,128)(2,1)S(1)} %collective-permute-done.7) | copy-start | bytes 491524
  67.1 0.7 copy-start.14
  74.6 9.9 %copy-start.1 = (bf16[640,1024]{1,0:T(8,128)(2,1)}, bf16[640,1024]{1,0:T(8,128)(2,1)S(1)}, u32[]{:S(2)}) copy-start(bf16[640,1024]{1,0:T(8,128)(2,1)S(1)} %concatenate.8.refs_8_) | copy-start | bytes 3932164
  74.6 9.9 %collective-permute-start.13 = (bf16[640,1024]{1,0:T(8,128)(2,1)S(1)}, bf16[640,1024]{1,0:T(8,128)(2,1)}, u32[]{:S(2)}, u32[]{:S(2)}) collective-permute-start(bf16[640,1024]{1,0:T(8,128)(2,1)S(1)} %concatenate.8.refs_8_), channel_id=1, source_target_pairs={{0,1},{1,0},{2,3},{3,2},{4,5},{5,4},{6,7},{7,6},{8,9},{9,8},{10,11... | collective-permute-start | bytes 3932168 | tf_op jit(solution)/shard_map/ppermute | solution.py:23
  79.3 3.2 %collective-permute-start.3 = (bf16[88,2048]{1,0:T(8,128)(2,1)S(1)}, bf16[88,2048]{1,0:T(8,128)(2,1)S(1)}, u32[]{:S(2)}, u32[]{:S(2)}) collective-permute-start(bf16[88,2048]{1,0:T(8,128)(2,1)S(1)} %bitcast.24), channel_id=1, source_target_pairs={{0,1},{1,0},{2,3},{3,2},{4,5},{5,4},{6,7},{7,6},{8,9},{9,8},{10,11... | collective-permute-start | bytes 1081352 | tf_op jit(solution)/shard_map/ppermute | solution.py:23
  79.4 3.6 %collective-permute-start.4 = (bf16[88,2048]{1,0:T(8,128)(2,1)}, bf16[88,2048]{1,0:T(8,128)(2,1)S(1)}, u32[]{:S(2)}, u32[]{:S(2)}) collective-permute-start(bf16[88,2048]{1,0:T(8,128)(2,1)} %bitcast.25), channel_id=1, source_target_pairs={{0,1},{1,0},{2,3},{3,2},{4,5},{5,4},{6,7},{7,6},{8,9},{9,8},{10,11... | collective-permute-start | bytes 1081352 | tf_op jit(solution)/shard_map/ppermute | solution.py:23
  79.8 3.7 %collective-permute-start.5 = (bf16[88,2048]{1,0:T(8,128)(2,1)}, bf16[88,2048]{1,0:T(8,128)(2,1)S(1)}, u32[]{:S(2)}, u32[]{:S(2)}) collective-permute-start(bf16[88,2048]{1,0:T(8,128)(2,1)} %bitcast.27), channel_id=1, source_target_pairs={{0,1},{1,0},{2,3},{3,2},{4,5},{5,4},{6,7},{7,6},{8,9},{9,8},{10,11... | collective-permute-start | bytes 1081352 | tf_op jit(solution)/shard_map/ppermute | solution.py:23
  82.5 1.0 copy-start.3
  83.0 0.7 copy-start.4
  83.7 0.7 copy-start.5
  84.5 1.2 copy-start
  126.6 8.5 %copy-start.17 = (s32[16,2]{0,1:T(2,128)S(1)}, s32[16,2]{0,1:T(2,128)}, u32[]{:S(2)}) copy-start(s32[16,2]{0,1:T(2,128)} %param.32) | copy-start | bytes 388
  127.7 16.4 %all-to-all-start.3 = ((bf16[16,3,1024]{2,1,0:T(4,128)(2,1)}), bf16[16,3,1024]{2,1,0:T(4,128)(2,1)S(1)}, u32[]{:S(2)}, u32[]{:S(2)}) async-start(bf16[16,3,1024]{2,1,0:T(4,128)(2,1)} %bitcast.18), calls=%async_computation.3 | async-start | bytes 262144 | tf_op jit(solution)/shard_map/all_to_all | solution.py:318
where the time goes:
time: 147 us
  starting transfers between devices  42.2 us (29%)
  waiting for transfers between devices  35.3 us (24%)
  blocking collectives  28.9 us (20%)
  Pallas kernels  22.2 us (15%)
  local copies, waits for them, and re-layouts  16.3 us (11%)
    all_to_all x1, blocking collectives, layer(): lax.all_to_all(partial.reshape(chips, EXPERTS * SLOTS, width), PLANE, 0,...  28.9 us
    ppermute x7, waiting for transfers between devices, along_z(): lax.ppermute(value, 'ep_0', [(i, (i + shift) % size) for i in range(size)])  19.9 us
    ppermute x7, starting transfers between devices, along_z(): lax.ppermute(value, 'ep_0', [(i, (i + shift) % size) for i in range(size)])  12.2 us
    pallas_call x1, Pallas kernels, experts_and_dense(): pl.pallas_call(lambda *refs: branch_kernel(hidden, *refs), name='branch',...  12 us
    ppermute x7, starting transfers between devices, swap(): return lax.ppermute(value, 'tp', [(0, 1), (1, 0)])  9.19 us
    all_to_all x1, waiting for transfers between devices, layer(): lax.all_to_all(send.reshape(2 * EXPERTS, SLOTS, half), ('ep_0', 'tp'), 0,...  8.2 us
    all_to_all x1, starting transfers between devices, layer(): lax.all_to_all(send.reshape(2 * EXPERTS, SLOTS, half), ('ep_0', 'tp'), 0,...  7.51 us
    all_to_all x1, starting transfers between devices, to_all(): return lax.all_to_all(copies, axis, split_axis=0, concat_axis=0, tiled=True)  6.76 us
  transfers between devices with their start and end apart: 17, of which 9 were waited for; matrix products, arithmetic and copies ran while one was open for 7% of the time, Pallas kernels for 4%

commit v1 on v0

--- a/solution.py
+++ b/solution.py
@@ -46,16 +46,31 @@
     return v / (1.0 + jnp.exp(-v))
 
 
-def branch_kernel(
-    hidden, core_ref, x_ref, g1, u1, d1, g2, u2, d2, own_ref, other_ref, out_ref, acc_ref
-):
+def branch_kernel(hidden, core_ref, x_ref, *refs):
+    weights, pieces, (out_ref, w_ref, own_ref, other_ref, acc_ref, sem) = (
+        refs[:6], refs[6:-6], refs[-6:],
+    )
     half = own_ref.shape[1]
     width = 2 * half
+    count = len(pieces) // 2
+    first = []
+    for k, weight in enumerate(weights):
+        first.append(pltpu.make_async_copy(weight, w_ref.at[k], sem.at[len(pieces) + k]))
+        first[-1].start()
+    copies = []
+    for k, piece in enumerate(pieces):
+        into = (own_ref, other_ref)[k // count]
+        place = pl.ds((k % count) * CHUNK, CHUNK)
+        copies.append(pltpu.make_async_copy(piece, into.at[place], sem.at[k]))
+        copies[-1].start()
     core = core_ref[0]
     here = pl.multiple_of(core * half, half)
     there = pl.multiple_of((1 - core) * half, half)
     total = x_ref.shape[0]
     step = total // 3
+    for copy in first:
+        copy.wait()
+    g1, u1, d1, g2, u2, d2 = (w_ref.at[k] for k in range(6))
     for start in range(0, total, step):
         band = pl.ds(start, step)
         x = x_ref[band, :width]
@@ -63,6 +78,9 @@
         h1 = (w * silu(dot_t(x, g1[...])) * dot_t(x, u1[...])).astype(BF16)
         h2 = (w * silu(dot_t(x, g2[...])) * dot_t(x, u2[...])).astype(BF16)
         acc_ref[...] = dot(h1, d1[...]) + dot(h2, d2[...])
+        if start == 0:
+            for copy in copies:
+                copy.wait()
         pre = dot_t(x_ref[band, pl.ds(here, half)], own_ref[...])
         pre = pre + dot_t(x_ref[band, pl.ds(there, half)], other_ref[...])
         logit = pre[:, hidden : hidden + 1]
@@ -77,17 +95,30 @@
         out_ref[band, :] = acc_ref[...].astype(BF16)
 
 
-def experts_and_dense(core, x, own, other, dense_own, dense_other, hidden):
-    rows, width = x.shape[0], 2 * dense_own.shape[1]
+def in_vmem(value):
+    return pltpu.with_memory_space_constraint(value, pltpu.VMEM)
+
+
+def experts_and_dense(core, x, own, other, pieces, pieces2, hidden):
+    rows, half = x.shape[0], pieces[0].shape[1]
+    width = 2 * half
     vmem = pl.BlockSpec(memory_space=pltpu.VMEM)
+    hbm = pl.BlockSpec(memory_space=pl.ANY)
+    units = len(pieces) * CHUNK
     return pl.pallas_call(
         lambda *refs: branch_kernel(hidden, *refs),
         name="branch",
-        out_shape=jax.ShapeDtypeStruct((rows, width), BF16),
-        in_specs=[pl.BlockSpec(memory_space=pltpu.SMEM)] + [vmem] * 9,
+        out_shape=pltpu.VMEM((rows, width), BF16),
+        in_specs=[pl.BlockSpec(memory_space=pltpu.SMEM)] + [vmem] + [hbm] * (6 + 2 * len(pieces)),
         out_specs=vmem,
-        scratch_shapes=[pltpu.VMEM((rows // 3, width), F32)],
-    )(core.reshape(1), x, *own, *other, dense_own, dense_other)
+        scratch_shapes=[
+            pltpu.VMEM((6, *own[0].shape), BF16),
+            pltpu.VMEM((units, half), BF16),
+            pltpu.VMEM((units, half), BF16),
+            pltpu.VMEM((rows // 3, width), F32),
+            pltpu.SemaphoreType.DMA((6 + 2 * len(pieces),)),
+        ],
+    )(core.reshape(1), in_vmem(x), *own, *other, *pieces, *pieces2)
 
 
 def mixer_kernel(
@@ -156,7 +187,7 @@
         mixer_kernel,
         name="mixer",
         out_shape=(
-            jax.ShapeDtypeStruct((rows, 2 * half), BF16),
+            pltpu.VMEM((rows, 2 * half), BF16),
             jax.ShapeDtypeStruct(state.shape, F32),
         ),
         in_specs=[pl.BlockSpec(memory_space=pltpu.SMEM)] + [vmem] * 8,
@@ -167,7 +198,10 @@
             pltpu.VMEM((rows, heads * head), F32),
             pltpu.SemaphoreType.DMA((rows // 4,)),
         ],
-    )(core.reshape(1), own, other, gain.reshape(1, 2 * half), wq, wk, wv, wo, state)
+    )(
+        core.reshape(1), in_vmem(own), in_vmem(other), gain.reshape(1, 2 * half),
+        wq, wk, wv, wo, state,
+    )
 
 
 def third(index):
@@ -223,14 +257,14 @@
         slots_kernel,
         name="slots",
         out_shape=(
-            jax.ShapeDtypeStruct((EXPERTS * SLOTS, 2 * half + 128), BF16),
-            jax.ShapeDtypeStruct((rows, half), BF16),
+            pltpu.VMEM((EXPERTS * SLOTS, 2 * half + 128), BF16),
+            pltpu.VMEM((rows, half), BF16),
         ),
         in_specs=[pl.BlockSpec(memory_space=pltpu.SMEM)] + [vmem] * 8,
         out_specs=(vmem, vmem),
     )(
-        core.reshape(1), own, other, mix, mix2, gain.reshape(1, half), gain2.reshape(1, half),
-        routes.T, route_w.astype(F32).T,
+        core.reshape(1), in_vmem(own), in_vmem(other), in_vmem(mix), in_vmem(mix2),
+        gain.reshape(1, half), in_vmem(gain2.reshape(1, half)), routes.T, route_w.T,
     )
 
 
@@ -258,7 +292,7 @@
         out_shape=jax.ShapeDtypeStruct(after.shape, BF16),
         in_specs=[vmem] * 3,
         out_specs=vmem,
-    )(home, after, routes)
+    )(in_vmem(home), in_vmem(after), routes)
 
 
 def layer(
@@ -298,9 +332,10 @@
     at_plane = lax.all_to_all(
         slot_rows.reshape(EXPERTS, SLOTS, width + 128), "ep_0", 0, 0, tiled=True
     ).reshape(EXPERTS * SLOTS, width + 128)
-    pieces = [packed] + [along_z(packed, k) for k in range(1, EXPERTS)]
-    dense_own = jnp.concatenate(pieces, axis=0)
-    dense_other = swap(dense_own)
+    pieces = [packed]
+    for shift in (4, 3, 5, 2, 6, 1, 7):
+        pieces.append(along_z(packed, shift))
+    pieces2 = [swap(piece) for piece in pieces]
     gathered = to_all(at_plane, PLANE)
     chips = gathered.shape[0]
     partial = experts_and_dense(
@@ -308,8 +343,8 @@
         gathered.reshape(-1, width + 128),
         mine,
         theirs,
-        dense_own,
-        dense_other,
+        pieces,
+        pieces2,
         hidden,
     )
     back = lax.all_to_all(partial.reshape(chips, EXPERTS * SLOTS, width), PLANE, 0, 0, tiled=True)

time: 147 us -> 134 us (0.912)
  blocking collectives: 28.9 us -> 43.3 us
  local copies, waits for them, and re-layouts: 16.3 us -> 6.03 us
  waiting for transfers between devices: 35.3 us -> 26 us
  Pallas kernels: 22.2 us -> 18.4 us
  starting transfers between devices: 42.2 us -> 38.9 us
    all_to_all x0 -> x1, blocking collectives: none -> 14.8 us  [layer(): lax.all_to_all(slot_rows.reshape(EXPERTS, SLOTS, width + 128), 'ep_0', 0,...]
    concatenate x1 -> x0, local copies, waits for them, and re-layouts: 6.75 us -> none  [layer(): dense_own = jnp.concatenate(pieces, axis=0)]
    ppermute x7, waiting for transfers between devices: 19.9 us -> 13.2 us  [along_z(): lax.ppermute(value, 'ep_0', [(i, (i + shift) % size) for i in range(size)])]
    all_to_all x1 -> x0, starting transfers between devices: 6.48 us -> none  [layer(): lax.all_to_all(slot_rows.reshape(EXPERTS, SLOTS, width + 128), 'ep_0', 0,...]
    ppermute x7 -> x14, starting transfers between devices: 9.19 us -> 13.5 us  [swap(): return lax.ppermute(value, 'tp', [(0, 1), (1, 0)])]
    all_to_all x1 -> x0, waiting for transfers between devices: 2.11 us -> none  [layer(): lax.all_to_all(slot_rows.reshape(EXPERTS, SLOTS, width + 128), 'ep_0', 0,...]
    pallas_call x1, Pallas kernels: 12 us -> 9.88 us  [experts_and_dense(): pl.pallas_call(lambda *refs: branch_kernel(hidden, *refs), name='branch',...]
    pallas_call x2, Pallas kernels: 8.41 us -> 6.85 us  [the longest x1 5.86 us: mixer(): pl.pallas_call(mixer_kernel, name='mixer', out_shape=(pltpu.VMEM((rows, 2...]
  transfers between devices with their start and end apart: 17 -> 23, of which waited for: 9 -> 8; matrix products, arithmetic and copies ran while one was open for 7% -> 1% of each run, Pallas kernels for 4% -> 0%
where the time goes in v1:
time: 134 us
  blocking collectives  43.3 us (32%)
  starting transfers between devices  38.9 us (29%)
  waiting for transfers between devices  26 us (19%)
  Pallas kernels  18.4 us (14%)
  local copies, waits for them, and re-layouts  6.03 us (4%)
    all_to_all x1, blocking collectives, layer(): lax.all_to_all(partial.reshape(chips, EXPERTS * SLOTS, width), PLANE, 0,...  28.5 us
    all_to_all x1, blocking collectives, layer(): lax.all_to_all(slot_rows.reshape(EXPERTS, SLOTS, width + 128), 'ep_0', 0,...  14.8 us
    ppermute x14, starting transfers between devices, swap(): return lax.ppermute(value, 'tp', [(0, 1), (1, 0)])  13.5 us
    ppermute x7, waiting for transfers between devices, along_z(): lax.ppermute(value, 'ep_0', [(i, (i + shift) % size) for i in range(size)])  13.2 us
    ppermute x7, starting transfers between devices, along_z(): lax.ppermute(value, 'ep_0', [(i, (i + shift) % size) for i in range(size)])  12 us
    pallas_call x1, Pallas kernels, experts_and_dense(): pl.pallas_call(lambda *refs: branch_kernel(hidden, *refs), name='branch',...  9.88 us
    all_to_all x1, waiting for transfers between devices, layer(): lax.all_to_all(send.reshape(2 * EXPERTS, SLOTS, half), ('ep_0', 'tp'), 0,...  8.21 us
    all_to_all x1, starting transfers between devices, to_all(): return lax.all_to_all(copies, axis, split_axis=0, concat_axis=0, tiled=True)  6.9 us
  transfers between devices with their start and end apart: 23, of which 8 were waited for; matrix products, arithmetic and copies ran while one was open for 1% of the time, Pallas kernels for 0%

profile of v1, /device:TPU:1, one launch (start us, length us, event | category | flops | bytes accessed | tf_op | source)
XLA Modules:
  0.0 133.8 jit_solution(4559894190099605423)
XLA Ops:
  0.6 3.3 %collective-permute-start = (bf16[16,1024]{1,0:T(8,128)(2,1)}, bf16[16,1024]{1,0:T(8,128)(2,1)S(1)}, u32[]{:S(2)}, u32[]{:S(2)}) collective-permute-start(bf16[16,1024]{1,0:T(8,128)(2,1)} %x_ref.3), channel_id=1, source_target_pairs={{0,1},{1,0},{2,3},{3,2},{4,5},{5,4},{6,7},{7,6},{8,9},{9,8},{10,11... | collective-permute-start | bytes 98312 | tf_op jit(solution)/shard_map/ppermute | solution.py:23
  3.9 1.1 collective-permute-done.y_ref
  5.0 0.8 copy-done
  5.8 5.9 %mixer.1 = (bf16[16,2048]{1,0:T(8,128)(2,1)S(1)}, f32[16,2,128,128]{3,2,1,0:T(8,128)}) custom-call(s32[1]{0:T(128)} %bitcast.core_ref.refs_0_, bf16[16,1024]{1,0:T(8,128)(2,1)S(1)} %copy-done, bf16[16,1024]{1,0:T(8,128)(2,1)S(1)} %collective-permute-done.y_ref, f32[1,2048]{1,0:T(1,128)} %bitcast.31, bf16[2048,256]{1,0:T(8,128)(2,1)} %wq.1, ...), custom_call_target="tpu_custom_call" | custom-call | tf_op jit(solution)/shard_map/mixer/pallas_call | solution.py:186
  11.6 0.4 collective-permute-start.1
  12.1 0.2 collective-permute-start.2
  12.2 1.0 collective-permute-done.2
  13.2 1.0 slots.1
  14.3 14.8 %all_to_all.20 = bf16[8,3,2176]{2,1,0:T(4,128)(2,1)S(1)} all-to-all(bf16[8,3,2176]{2,1,0:T(4,128)(2,1)S(1)} %reshape.41), channel_id=1, replica_groups=mesh['ep_0'=8,'ep_1'=4,'ep_2'=4,'tp'=2] {'ep_0'}, dimensions={0} | all-to-all | bytes 208896 | tf_op jit(solution)/shard_map/all_to_all | solution.py:332
  29.1 0.1 broadcast_in_dim.19
  29.1 1.3 broadcast_in_dim.20
  30.5 6.9 %all-to-all-start.1 = ((bf16[16,24,2176]{2,1,0:T(8,128)(2,1)}), bf16[16,24,2176]{2,1,0:T(8,128)(2,1)S(1)}, u32[]{:S(2)}, u32[]{:S(2)}) async-start(bf16[16,24,2176]{2,1,0:T(8,128)(2,1)} %broadcast_in_dim.20), calls=%async_computation.1 | async-start | bytes 3342336 | tf_op jit(solution)/shard_map/all_to_all | solution.py:34
  37.5 0.2 concatenate.3.refs_8_
  37.7 1.1 collective-permute-start.6
  38.8 1.1 collective-permute-start.7
  40.0 3.3 %collective-permute-start.8 = (bf16[80,1024]{1,0:T(8,128)(2,1)S(1)}, bf16[80,1024]{1,0:T(8,128)(2,1)S(1)}, u32[]{:S(2)}, u32[]{:S(2)}) collective-permute-start(bf16[80,1024]{1,0:T(8,128)(2,1)S(1)} %concatenate.3.refs_8_), channel_id=1, source_target_pairs={{0,160},{32,192},{64,224},{96,0},{128,32},{160,64},{192,96},{224,1... | collective-permute-start | bytes 491528 | tf_op jit(solution)/shard_map/ppermute | solution.py:28
  43.3 1.9 %collective-permute-start.9 = (bf16[80,1024]{1,0:T(8,128)(2,1)S(1)}, bf16[80,1024]{1,0:T(8,128)(2,1)S(1)}, u32[]{:S(2)}, u32[]{:S(2)}) collective-permute-start(bf16[80,1024]{1,0:T(8,128)(2,1)S(1)} %concatenate.3.refs_8_), channel_id=1, source_target_pairs={{0,64},{32,96},{64,128},{96,160},{128,192},{160,224},{192,0},{224,... | collective-permute-start | bytes 491528 | tf_op jit(solution)/shard_map/ppermute | solution.py:28
  45.2 1.7 %collective-permute-start.10 = (bf16[80,1024]{1,0:T(8,128)(2,1)S(1)}, bf16[80,1024]{1,0:T(8,128)(2,1)S(1)}, u32[]{:S(2)}, u32[]{:S(2)}) collective-permute-start(bf16[80,1024]{1,0:T(8,128)(2,1)S(1)} %concatenate.3.refs_8_), channel_id=1, source_target_pairs={{0,192},{32,224},{64,0},{96,32},{128,64},{160,96},{192,128},{224,1... | collective-permute-start | bytes 491528 | tf_op jit(solution)/shard_map/ppermute | solution.py:28
  46.9 2.9 %collective-permute-start.11 = (bf16[80,1024]{1,0:T(8,128)(2,1)S(1)}, bf16[80,1024]{1,0:T(8,128)(2,1)S(1)}, u32[]{:S(2)}, u32[]{:S(2)}) collective-permute-start(bf16[80,1024]{1,0:T(8,128)(2,1)S(1)} %concatenate.3.refs_8_), channel_id=1, source_target_pairs={{0,32},{32,64},{64,96},{96,128},{128,160},{160,192},{192,224},{224... | collective-permute-start | bytes 491528 | tf_op jit(solution)/shard_map/ppermute | solution.py:28
  49.8 12.1 %collective-permute-done.7.refs_10_ = bf16[80,1024]{1,0:T(8,128)(2,1)S(1)} collective-permute-done((bf16[80,1024]{1,0:T(8,128)(2,1)S(1)}, bf16[80,1024]{1,0:T(8,128)(2,1)S(1)}, u32[]{:S(2)}, u32[]{:S(2)}) %collective-permute-start.7) | collective-permute-done | bytes 163872 | tf_op jit(solution)/shard_map/ppermute | solution.py:28
  61.9 3.2 %collective-permute-start.13 = (bf16[80,1024]{1,0:T(8,128)(2,1)S(1)}, bf16[80,1024]{1,0:T(8,128)(2,1)S(1)}, u32[]{:S(2)}, u32[]{:S(2)}) collective-permute-start(bf16[80,1024]{1,0:T(8,128)(2,1)S(1)} %concatenate.3.refs_8_), channel_id=1, source_target_pairs={{0,1},{1,0},{2,3},{3,2},{4,5},{5,4},{6,7},{7,6},{8,9},{9,8},{10,11... | collective-permute-start | bytes 491528 | tf_op jit(solution)/shard_map/ppermute | solution.py:23
  65.1 3.7 %collective-permute-start.14 = (bf16[80,1024]{1,0:T(8,128)(2,1)S(1)}, bf16[80,1024]{1,0:T(8,128)(2,1)S(1)}, u32[]{:S(2)}, u32[]{:S(2)}) collective-permute-start(bf16[80,1024]{1,0:T(8,128)(2,1)S(1)} %collective-permute-done.6.refs_9_), channel_id=1, source_target_pairs={{0,1},{1,0},{2,3},{3,2},{4,5},{5,4},{6,7},{7,6},{8,9},{9,8},{10,11... | collective-permute-start | bytes 491528 | tf_op jit(solution)/shard_map/ppermute | solution.py:23
  68.9 0.1 collective-permute-start.15
  69.0 1.1 collective-permute-done.11.refs_14_
  70.1 0.5 collective-permute-start.16
  70.6 0.3 collective-permute-start.3
  70.9 0.7 copy-done.14
  71.6 0.5 collective-permute-start.4
  72.1 0.1 collective-permute-start.5
  72.2 0.5 collective-permute-start.17
  72.7 0.1 collective-permute-start.18
  72.8 1.3 collective-permute-done.17.refs_20_
  74.1 0.4 collective-permute-start.19
  74.5 0.2 collective-permute-start.20
  74.7 0.8 collective-permute-done.19.refs_22_
  75.5 0.4 collective-permute-done.20.refs_23_
  76.0 0.2 copy-done.20
  76.2 0.4 copy-done.21
  76.6 0.7 copy-done.6
  77.3 9.9 %branch.1 = bf16[384,2048]{1,0:T(8,128)(2,1)S(1)} custom-call(s32[1]{0:T(128)} %bitcast.core_ref.refs_0_, bf16[384,2176]{1,0:T(8,128)(2,1)S(1)} %bitcast.19, bf16[88,2048]{1,0:T(8,128)(2,1)} %bitcast.23, bf16[88,2048]{1,0:T(8,128)(2,1)} %bitcast.25, bf16[88,2048]{1,0:T(8,128)(2,1)} %bitcast.27, bf16[88,2048]{1,0:T(8,128)(2,1)} %copy-done.5, ...), custom_call_target="tpu_custom_call" | custom-call | tf_op jit(solution)/shard_map/branch/pallas_call | solution.py:108
  87.2 28.5 %all_to_all.21 = bf16[16,24,2048]{2,1,0:T(8,128)(2,1)S(1)} all-to-all(bf16[16,24,2048]{2,1,0:T(8,128)(2,1)S(1)} %bitcast.20), channel_id=1, replica_groups=mesh['ep_0'=8,'ep_1'=4,'ep_2'=4,'tp'=2] {'ep_1','ep_2'}, dimensions={0} | all-to-all | bytes 3145728 | tf_op jit(solution)/shard_map/all_to_all | solution.py:350
  115.8 0.3 reduce_sum.12
  116.1 0.7 copy.27
  116.8 6.4 %all-to-all-start.3 = ((bf16[16,3,1024]{2,1,0:T(4,128)(2,1)}), bf16[16,3,1024]{2,1,0:T(4,128)(2,1)S(1)}, u32[]{:S(2)}, u32[]{:S(2)}) async-start(bf16[16,3,1024]{2,1,0:T(4,128)(2,1)} %bitcast.18), calls=%async_computation.3 | async-start | bytes 262144 | tf_op jit(solution)/shard_map/all_to_all | solution.py:353
  123.2 0.7 copy.26.routes_ref
  123.9 8.2 %all-to-all-done.3 = bf16[16,3,1024]{2,1,0:T(4,128)(2,1)S(1)} async-done(((bf16[16,3,1024]{2,1,0:T(4,128)(2,1)}), bf16[16,3,1024]{2,1,0:T(4,128)(2,1)S(1)}, u32[]{:S(2)}, u32[]{:S(2)}) %all-to-all-start.3) | async-done | bytes 98336 | tf_op jit(solution)/shard_map/all_to_all | solution.py:353
  132.1 0.1 reshape.46.home_ref
  132.1 1.6 %home.1 = bf16[16,1024]{1,0:T(8,128)(2,1)} custom-call(bf16[48,1024]{1,0:T(8,128)(2,1)S(1)} %reshape.46.home_ref, bf16[16,1024]{1,0:T(8,128)(2,1)S(1)} %get-tuple-element.8.after_ref, s32[16,2]{1,0:T(8,128)} %copy.26.routes_ref), custom_call_target="tpu_custom_call" | custom-call | tf_op jit(solution)/shard_map/home/pallas_call | solution.py:289
  (73 shorter events, 0.3 us)
Async XLA Ops:
  0.6 4.4 %collective-permute-start = (bf16[16,1024]{1,0:T(8,128)(2,1)}, bf16[16,1024]{1,0:T(8,128)(2,1)S(1)}, u32[]{:S(2)}, u32[]{:S(2)}) collective-permute-start(bf16[16,1024]{1,0:T(8,128)(2,1)} %x_ref.3), channel_id=1, source_target_pairs={{0,1},{1,0},{2,3},{3,2},{4,5},{5,4},{6,7},{7,6},{8,9},{9,8},{10,11... | collective-permute-start | bytes 98312 | tf_op jit(solution)/shard_map/ppermute | solution.py:23
  5.0 0.8 copy-start
  5.7 6.3 %copy-start.26 = (f32[1024]{0:T(1024)S(1)}, f32[1024]{0:T(1024)}, u32[]{:S(2)}) copy-start(f32[1024]{0:T(1024)} %param.24) | copy-start | bytes 12292
  11.6 1.6 %collective-permute-start.1 = (bf16[16,2048]{1,0:T(8,128)(2,1)S(1)}, bf16[16,2048]{1,0:T(8,128)(2,1)S(1)}, u32[]{:S(2)}, u32[]{:S(2)}) collective-permute-start(bf16[16,2048]{1,0:T(8,128)(2,1)S(1)} %get-tuple-element.6.mix_ref), channel_id=1, source_target_pairs={{0,1},{1,0},{2,3},{3,2},{4,5},{5,4},{6,7},{7,6},{8,9},{9,8},{10,11... | collective-permute-start | bytes 196616 | tf_op jit(solution)/shard_map/ppermute | solution.py:23
  12.1 1.2 collective-permute-start.2
  30.5 7.0 %copy-start.27 = (bf16[1024]{0:T(1024)(128)(2,1)S(1)}, bf16[1024]{0:T(1024)(128)(2,1)}, u32[]{:S(2)}) copy-start(bf16[1024]{0:T(1024)(128)(2,1)} %param.25) | copy-start | bytes 6148
  30.5 7.0 %copy-start.22 = (bf16[1024,22]{0,1:T(8,128)(2,1)S(1)}, bf16[1024,22]{0,1:T(8,128)(2,1)}, u32[]{:S(2)}) copy-start(bf16[1024,22]{0,1:T(8,128)(2,1)} %param.26) | copy-start | bytes 135172
  30.5 7.0 %copy-start.23 = (bf16[1024,22]{0,1:T(8,128)(2,1)S(1)}, bf16[1024,22]{0,1:T(8,128)(2,1)}, u32[]{:S(2)}) copy-start(bf16[1024,22]{0,1:T(8,128)(2,1)} %param.27) | copy-start | bytes 135172
  30.5 7.0 %copy-start.24 = (bf16[22,1024]{1,0:T(8,128)(2,1)S(1)}, bf16[22,1024]{1,0:T(8,128)(2,1)}, u32[]{:S(2)}) copy-start(bf16[22,1024]{1,0:T(8,128)(2,1)} %param.28) | copy-start | bytes 135172
  30.5 40.1 %copy-start.2 = (bf16[1,2048,88]{1,2,0:T(8,128)(2,1)S(1)}, bf16[1,2048,88]{1,2,0:T(8,128)(2,1)}, u32[]{:S(2)}) copy-start(bf16[1,2048,88]{1,2,0:T(8,128)(2,1)} %param.29) | copy-start | bytes 1081348
  30.5 41.1 %copy-start.3 = (bf16[1,2048,88]{1,2,0:T(8,128)(2,1)S(1)}, bf16[1,2048,88]{1,2,0:T(8,128)(2,1)}, u32[]{:S(2)}) copy-start(bf16[1,2048,88]{1,2,0:T(8,128)(2,1)} %param.30) | copy-start | bytes 1081348
  30.5 41.6 %copy-start.4 = (bf16[1,88,2048]{2,1,0:T(8,128)(2,1)S(1)}, bf16[1,88,2048]{2,1,0:T(8,128)(2,1)}, u32[]{:S(2)}) copy-start(bf16[1,88,2048]{2,1,0:T(8,128)(2,1)} %param.31) | copy-start | bytes 1081348
  30.5 46.8 %all-to-all-start.1 = ((bf16[16,24,2176]{2,1,0:T(8,128)(2,1)}), bf16[16,24,2176]{2,1,0:T(8,128)(2,1)S(1)}, u32[]{:S(2)}, u32[]{:S(2)}) async-start(bf16[16,24,2176]{2,1,0:T(8,128)(2,1)} %broadcast_in_dim.20), calls=%async_computation.1 | async-start | bytes 3342336 | tf_op jit(solution)/shard_map/all_to_all | solution.py:34
  37.7 39.6 %copy-start.1 = (bf16[80,1024]{1,0:T(8,128)(2,1)}, bf16[80,1024]{1,0:T(8,128)(2,1)S(1)}, u32[]{:S(2)}) copy-start(bf16[80,1024]{1,0:T(8,128)(2,1)S(1)} %concatenate.3.refs_8_) | copy-start | bytes 491524
  37.7 9.1 %collective-permute-start.6 = (bf16[80,1024]{1,0:T(8,128)(2,1)S(1)}, bf16[80,1024]{1,0:T(8,128)(2,1)S(1)}, u32[]{:S(2)}, u32[]{:S(2)}) collective-permute-start(bf16[80,1024]{1,0:T(8,128)(2,1)S(1)} %concatenate.3.refs_8_), channel_id=1, source_target_pairs={{0,128},{32,160},{64,192},{96,224},{128,0},{160,32},{192,64},{224,... | collective-permute-start | bytes 491528 | tf_op jit(solution)/shard_map/ppermute | solution.py:28
  38.8 23.1 %collective-permute-start.7 = (bf16[80,1024]{1,0:T(8,128)(2,1)S(1)}, bf16[80,1024]{1,0:T(8,128)(2,1)S(1)}, u32[]{:S(2)}, u32[]{:S(2)}) collective-permute-start(bf16[80,1024]{1,0:T(8,128)(2,1)S(1)} %concatenate.3.refs_8_), channel_id=1, source_target_pairs={{0,96},{32,128},{64,160},{96,192},{128,224},{160,0},{192,32},{224,... | collective-permute-start | bytes 491528 | tf_op jit(solution)/shard_map/ppermute | solution.py:28
  40.0 21.9 %collective-permute-start.8 = (bf16[80,1024]{1,0:T(8,128)(2,1)S(1)}, bf16[80,1024]{1,0:T(8,128)(2,1)S(1)}, u32[]{:S(2)}, u32[]{:S(2)}) collective-permute-start(bf16[80,1024]{1,0:T(8,128)(2,1)S(1)} %concatenate.3.refs_8_), channel_id=1, source_target_pairs={{0,160},{32,192},{64,224},{96,0},{128,32},{160,64},{192,96},{224,1... | collective-permute-start | bytes 491528 | tf_op jit(solution)/shard_map/ppermute | solution.py:28
  43.3 21.8 %collective-permute-start.9 = (bf16[80,1024]{1,0:T(8,128)(2,1)S(1)}, bf16[80,1024]{1,0:T(8,128)(2,1)S(1)}, u32[]{:S(2)}, u32[]{:S(2)}) collective-permute-start(bf16[80,1024]{1,0:T(8,128)(2,1)S(1)} %concatenate.3.refs_8_), channel_id=1, source_target_pairs={{0,64},{32,96},{64,128},{96,160},{128,192},{160,224},{192,0},{224,... | collective-permute-start | bytes 491528 | tf_op jit(solution)/shard_map/ppermute | solution.py:28
  45.2 23.7 %collective-permute-start.10 = (bf16[80,1024]{1,0:T(8,128)(2,1)S(1)}, bf16[80,1024]{1,0:T(8,128)(2,1)S(1)}, u32[]{:S(2)}, u32[]{:S(2)}) collective-permute-start(bf16[80,1024]{1,0:T(8,128)(2,1)S(1)} %concatenate.3.refs_8_), channel_id=1, source_target_pairs={{0,192},{32,224},{64,0},{96,32},{128,64},{160,96},{192,128},{224,1... | collective-permute-start | bytes 491528 | tf_op jit(solution)/shard_map/ppermute | solution.py:28
  46.9 29.0 %copy-start.7 = (bf16[80,1024]{1,0:T(8,128)(2,1)}, bf16[80,1024]{1,0:T(8,128)(2,1)S(1)}, u32[]{:S(2)}) copy-start(bf16[80,1024]{1,0:T(8,128)(2,1)S(1)} %collective-permute-done.6.refs_9_) | copy-start | bytes 491524
  46.9 23.2 %collective-permute-start.11 = (bf16[80,1024]{1,0:T(8,128)(2,1)S(1)}, bf16[80,1024]{1,0:T(8,128)(2,1)S(1)}, u32[]{:S(2)}, u32[]{:S(2)}) collective-permute-start(bf16[80,1024]{1,0:T(8,128)(2,1)S(1)} %concatenate.3.refs_8_), channel_id=1, source_target_pairs={{0,32},{32,64},{64,96},{96,128},{128,160},{160,192},{192,224},{224... | collective-permute-start | bytes 491528 | tf_op jit(solution)/shard_map/ppermute | solution.py:28
  61.9 14.0 %copy-start.8 = (bf16[80,1024]{1,0:T(8,128)(2,1)}, bf16[80,1024]{1,0:T(8,128)(2,1)S(1)}, u32[]{:S(2)}) copy-start(bf16[80,1024]{1,0:T(8,128)(2,1)S(1)} %collective-permute-done.7.refs_10_) | copy-start | bytes 491524
  61.9 8.7 %collective-permute-start.12 = (bf16[80,1024]{1,0:T(8,128)(2,1)S(1)}, bf16[80,1024]{1,0:T(8,128)(2,1)S(1)}, u32[]{:S(2)}, u32[]{:S(2)}) collective-permute-start(bf16[80,1024]{1,0:T(8,128)(2,1)S(1)} %concatenate.3.refs_8_), channel_id=1, source_target_pairs={{0,224},{32,0},{64,32},{96,64},{128,96},{160,128},{192,160},{224,1... | collective-permute-start | bytes 491528 | tf_op jit(solution)/shard_map/ppermute | solution.py:28
  61.9 14.0 %copy-start.9 = (bf16[80,1024]{1,0:T(8,128)(2,1)}, bf16[80,1024]{1,0:T(8,128)(2,1)S(1)}, u32[]{:S(2)}) copy-start(bf16[80,1024]{1,0:T(8,128)(2,1)S(1)} %collective-permute-done.8.refs_11_) | copy-start | bytes 491524
  61.9 9.0 %collective-permute-start.13 = (bf16[80,1024]{1,0:T(8,128)(2,1)S(1)}, bf16[80,1024]{1,0:T(8,128)(2,1)S(1)}, u32[]{:S(2)}, u32[]{:S(2)}) collective-permute-start(bf16[80,1024]{1,0:T(8,128)(2,1)S(1)} %concatenate.3.refs_8_), channel_id=1, source_target_pairs={{0,1},{1,0},{2,3},{3,2},{4,5},{5,4},{6,7},{7,6},{8,9},{9,8},{10,11... | collective-permute-start | bytes 491528 | tf_op jit(solution)/shard_map/ppermute | solution.py:23
  65.1 10.8 %copy-start.10 = (bf16[80,1024]{1,0:T(8,128)(2,1)}, bf16[80,1024]{1,0:T(8,128)(2,1)S(1)}, u32[]{:S(2)}) copy-start(bf16[80,1024]{1,0:T(8,128)(2,1)S(1)} %collective-permute-done.9.refs_12_) | copy-start | bytes 491524
  65.1 6.9 %collective-permute-start.14 = (bf16[80,1024]{1,0:T(8,128)(2,1)S(1)}, bf16[80,1024]{1,0:T(8,128)(2,1)S(1)}, u32[]{:S(2)}, u32[]{:S(2)}) collective-permute-start(bf16[80,1024]{1,0:T(8,128)(2,1)S(1)} %collective-permute-done.6.refs_9_), channel_id=1, source_target_pairs={{0,1},{1,0},{2,3},{3,2},{4,5},{5,4},{6,7},{7,6},{8,9},{9,8},{10,11... | collective-permute-start | bytes 491528 | tf_op jit(solution)/shard_map/ppermute | solution.py:23
  68.9 7.1 %copy-start.11 = (bf16[80,1024]{1,0:T(8,128)(2,1)}, bf16[80,1024]{1,0:T(8,128)(2,1)S(1)}, u32[]{:S(2)}) copy-start(bf16[80,1024]{1,0:T(8,128)(2,1)S(1)} %collective-permute-done.10.refs_13_) | copy-start | bytes 491524
  68.9 3.3 %collective-permute-start.15 = (bf16[80,1024]{1,0:T(8,128)(2,1)S(1)}, bf16[80,1024]{1,0:T(8,128)(2,1)S(1)}, u32[]{:S(2)}, u32[]{:S(2)}) collective-permute-start(bf16[80,1024]{1,0:T(8,128)(2,1)S(1)} %collective-permute-done.7.refs_10_), channel_id=1, source_target_pairs={{0,1},{1,0},{2,3},{3,2},{4,5},{5,4},{6,7},{7,6},{8,9},{9,8},{10,11... | collective-permute-start | bytes 491528 | tf_op jit(solution)/shard_map/ppermute | solution.py:23
  70.1 5.9 %copy-start.12 = (bf16[80,1024]{1,0:T(8,128)(2,1)}, bf16[80,1024]{1,0:T(8,128)(2,1)S(1)}, u32[]{:S(2)}) copy-start(bf16[80,1024]{1,0:T(8,128)(2,1)S(1)} %collective-permute-done.11.refs_14_) | copy-start | bytes 491524
  70.1 2.6 %collective-permute-start.16 = (bf16[80,1024]{1,0:T(8,128)(2,1)S(1)}, bf16[80,1024]{1,0:T(8,128)(2,1)S(1)}, u32[]{:S(2)}, u32[]{:S(2)}) collective-permute-start(bf16[80,1024]{1,0:T(8,128)(2,1)S(1)} %collective-permute-done.8.refs_11_), channel_id=1, source_target_pairs={{0,1},{1,0},{2,3},{3,2},{4,5},{5,4},{6,7},{7,6},{8,9},{9,8},{10,11... | collective-permute-start | bytes 491528 | tf_op jit(solution)/shard_map/ppermute | solution.py:23
  70.6 5.4 %copy-start.13 = (bf16[80,1024]{1,0:T(8,128)(2,1)}, bf16[80,1024]{1,0:T(8,128)(2,1)S(1)}, u32[]{:S(2)}) copy-start(bf16[80,1024]{1,0:T(8,128)(2,1)S(1)} %collective-permute-done.12.refs_15_) | copy-start | bytes 491524
  70.6 5.3 %collective-permute-start.3 = (bf16[88,2048]{1,0:T(8,128)(2,1)S(1)}, bf16[88,2048]{1,0:T(8,128)(2,1)S(1)}, u32[]{:S(2)}, u32[]{:S(2)}) collective-permute-start(bf16[88,2048]{1,0:T(8,128)(2,1)S(1)} %bitcast.24), channel_id=1, source_target_pairs={{0,1},{1,0},{2,3},{3,2},{4,5},{5,4},{6,7},{7,6},{8,9},{9,8},{10,11... | collective-permute-start | bytes 1081352 | tf_op jit(solution)/shard_map/ppermute | solution.py:23
  71.6 4.3 %collective-permute-start.4 = (bf16[88,2048]{1,0:T(8,128)(2,1)S(1)}, bf16[88,2048]{1,0:T(8,128)(2,1)S(1)}, u32[]{:S(2)}, u32[]{:S(2)}) collective-permute-start(bf16[88,2048]{1,0:T(8,128)(2,1)S(1)} %bitcast.26), channel_id=1, source_target_pairs={{0,1},{1,0},{2,3},{3,2},{4,5},{5,4},{6,7},{7,6},{8,9},{9,8},{10,11... | collective-permute-start | bytes 1081352 | tf_op jit(solution)/shard_map/ppermute | solution.py:23
  72.1 3.9 %copy-start.15 = (bf16[80,1024]{1,0:T(8,128)(2,1)}, bf16[80,1024]{1,0:T(8,128)(2,1)S(1)}, u32[]{:S(2)}) copy-start(bf16[80,1024]{1,0:T(8,128)(2,1)S(1)} %collective-permute-done.14.refs_17_) | copy-start | bytes 491524
  72.1 5.3 %collective-permute-start.5 = (bf16[88,2048]{1,0:T(8,128)(2,1)S(1)}, bf16[88,2048]{1,0:T(8,128)(2,1)}, u32[]{:S(2)}, u32[]{:S(2)}) collective-permute-start(bf16[88,2048]{1,0:T(8,128)(2,1)S(1)} %bitcast.28), channel_id=1, source_target_pairs={{0,1},{1,0},{2,3},{3,2},{4,5},{5,4},{6,7},{7,6},{8,9},{9,8},{10,11... | collective-permute-start | bytes 1081352 | tf_op jit(solution)/shard_map/ppermute | solution.py:23
  72.2 3.8 %copy-start.16 = (bf16[80,1024]{1,0:T(8,128)(2,1)}, bf16[80,1024]{1,0:T(8,128)(2,1)S(1)}, u32[]{:S(2)}) copy-start(bf16[80,1024]{1,0:T(8,128)(2,1)S(1)} %collective-permute-done.15.refs_18_) | copy-start | bytes 491524
  72.2 1.9 %collective-permute-start.17 = (bf16[80,1024]{1,0:T(8,128)(2,1)S(1)}, bf16[80,1024]{1,0:T(8,128)(2,1)S(1)}, u32[]{:S(2)}, u32[]{:S(2)}) collective-permute-start(bf16[80,1024]{1,0:T(8,128)(2,1)S(1)} %collective-permute-done.9.refs_12_), channel_id=1, source_target_pairs={{0,1},{1,0},{2,3},{3,2},{4,5},{5,4},{6,7},{7,6},{8,9},{9,8},{10,11... | collective-permute-start | bytes 491528 | tf_op jit(solution)/shard_map/ppermute | solution.py:23
  72.7 3.3 %copy-start.17 = (bf16[80,1024]{1,0:T(8,128)(2,1)}, bf16[80,1024]{1,0:T(8,128)(2,1)S(1)}, u32[]{:S(2)}) copy-start(bf16[80,1024]{1,0:T(8,128)(2,1)S(1)} %collective-permute-done.16.refs_19_) | copy-start | bytes 491524
  72.7 1.8 %collective-permute-start.18 = (bf16[80,1024]{1,0:T(8,128)(2,1)S(1)}, bf16[80,1024]{1,0:T(8,128)(2,1)S(1)}, u32[]{:S(2)}, u32[]{:S(2)}) collective-permute-start(bf16[80,1024]{1,0:T(8,128)(2,1)S(1)} %collective-permute-done.10.refs_13_), channel_id=1, source_target_pairs={{0,1},{1,0},{2,3},{3,2},{4,5},{5,4},{6,7},{7,6},{8,9},{9,8},{10,11... | collective-permute-start | bytes 491528 | tf_op jit(solution)/shard_map/ppermute | solution.py:23
  74.1 1.9 %copy-start.18 = (bf16[80,1024]{1,0:T(8,128)(2,1)}, bf16[80,1024]{1,0:T(8,128)(2,1)S(1)}, u32[]{:S(2)}) copy-start(bf16[80,1024]{1,0:T(8,128)(2,1)S(1)} %collective-permute-done.17.refs_20_) | copy-start | bytes 491524
  74.1 1.4 %collective-permute-start.19 = (bf16[80,1024]{1,0:T(8,128)(2,1)S(1)}, bf16[80,1024]{1,0:T(8,128)(2,1)S(1)}, u32[]{:S(2)}, u32[]{:S(2)}) collective-permute-start(bf16[80,1024]{1,0:T(8,128)(2,1)S(1)} %collective-permute-done.11.refs_14_), channel_id=1, source_target_pairs={{0,1},{1,0},{2,3},{3,2},{4,5},{5,4},{6,7},{7,6},{8,9},{9,8},{10,11... | collective-permute-start | bytes 491528 | tf_op jit(solution)/shard_map/ppermute | solution.py:23
  74.5 1.5 %copy-start.19 = (bf16[80,1024]{1,0:T(8,128)(2,1)}, bf16[80,1024]{1,0:T(8,128)(2,1)S(1)}, u32[]{:S(2)}) copy-start(bf16[80,1024]{1,0:T(8,128)(2,1)S(1)} %collective-permute-done.18.refs_21_) | copy-start | bytes 491524
  74.5 1.4 %collective-permute-start.20 = (bf16[80,1024]{1,0:T(8,128)(2,1)S(1)}, bf16[80,1024]{1,0:T(8,128)(2,1)S(1)}, u32[]{:S(2)}, u32[]{:S(2)}) collective-permute-start(bf16[80,1024]{1,0:T(8,128)(2,1)S(1)} %collective-permute-done.12.refs_15_), channel_id=1, source_target_pairs={{0,1},{1,0},{2,3},{3,2},{4,5},{5,4},{6,7},{7,6},{8,9},{9,8},{10,11... | collective-permute-start | bytes 491528 | tf_op jit(solution)/shard_map/ppermute | solution.py:23
  75.9 1.4 %copy-start.5 = (bf16[88,2048]{1,0:T(8,128)(2,1)}, bf16[88,2048]{1,0:T(8,128)(2,1)S(1)}, u32[]{:S(2)}) copy-start(bf16[88,2048]{1,0:T(8,128)(2,1)S(1)} %collective-permute-done.3.refs_5_) | copy-start | bytes 1081348
  76.6 0.7 copy-start.6
  115.8 7.4 %copy-start.25 = (s32[16,2]{0,1:T(2,128)S(1)}, s32[16,2]{0,1:T(2,128)}, u32[]{:S(2)}) copy-start(s32[16,2]{0,1:T(2,128)} %param.32) | copy-start | bytes 388
  116.8 15.3 %all-to-all-start.3 = ((bf16[16,3,1024]{2,1,0:T(4,128)(2,1)}), bf16[16,3,1024]{2,1,0:T(4,128)(2,1)S(1)}, u32[]{:S(2)}, u32[]{:S(2)}) async-start(bf16[16,3,1024]{2,1,0:T(4,128)(2,1)} %bitcast.18), calls=%async_computation.3 | async-start | bytes 262144 | tf_op jit(solution)/shard_map/all_to_all | solution.py:353
  (3 other events, 2.0 us)

commit v2 on v1

--- a/solution.py
+++ b/solution.py
@@ -12,6 +12,10 @@
 EP = ("ep_0", "ep_1", "ep_2")
 PLANE = ("ep_1", "ep_2")
 PAD = 24
+ROWS = 24
+LIVE = 20
+MAIN = 1792
+TAIL = 256
 CHUNK = 80
 
 epsilon = 1e-06
@@ -28,12 +32,6 @@
     return lax.ppermute(value, "ep_0", [(i, (i + shift) % size) for i in range(size)])
 
 
-def to_all(value, axis):
-    size = lax.axis_size(axis)
-    copies = jnp.broadcast_to(value[None], (size, *value.shape))
-    return lax.all_to_all(copies, axis, split_axis=0, concat_axis=0, tiled=True)
-
-
 def dot(a, b):
     return jnp.dot(a, b, preferred_element_type=F32)
 
@@ -46,53 +44,101 @@
     return v / (1.0 + jnp.exp(-v))
 
 
+def divided(index, by):
+    return {3: (index * 43) >> 7, 5: (index * 13) >> 6, 24: (index * 171) >> 12}[by]
+
+
+def iota2(shape, dim):
+    return lax.broadcasted_iota(jnp.int32, shape, dim)
+
+
+def one_hot(mask):
+    return mask.astype(F32).astype(BF16)
+
+
+def tail_maps(size, group):
+    shape = (size, size)
+    row, col = iota2(shape, 0), iota2(shape, 1)
+    chunk = divided(row, ROWS)
+    place = row - ROWS * chunk
+    unpack = (place < LIVE) & (place >> 2 == group) & (col == ROWS * chunk + LIVE + (place & 3))
+    pack = (place >= LIVE) & (col == ROWS * chunk + 4 * group + place - LIVE)
+    return one_hot(unpack), one_hot(pack)
+
+
 def branch_kernel(hidden, core_ref, x_ref, *refs):
-    weights, pieces, (out_ref, w_ref, own_ref, other_ref, acc_ref, sem) = (
-        refs[:6], refs[6:-6], refs[-6:],
+    weights, pieces, (out_ref, full_ref, up_ref, down_ref, own_ref, other_ref, acc_ref, sem) = (
+        refs[:6], refs[6:-8], refs[-8:],
     )
     half = own_ref.shape[1]
-    width = 2 * half
     count = len(pieces) // 2
-    first = []
-    for k, weight in enumerate(weights):
-        first.append(pltpu.make_async_copy(weight, w_ref.at[k], sem.at[len(pieces) + k]))
-        first[-1].start()
+    units = weights[0].shape[0]
+    lanes = up_ref.shape[0] // 4
     copies = []
+
+    def fetch(source, into):
+        copies.append(pltpu.make_async_copy(source, into, sem.at[len(copies)]))
+        copies[-1].start()
+
+    for k, place in enumerate((0, 2, None, 1, 3, None)):
+        if place is not None:
+            fetch(weights[k], up_ref.at[pl.ds(place * lanes, units)])
+    for k, place in ((2, 0), (5, 1)):
+        fetch(weights[k], down_ref.at[pl.ds(place * lanes, units)])
     for k, piece in enumerate(pieces):
         into = (own_ref, other_ref)[k // count]
-        place = pl.ds((k % count) * CHUNK, CHUNK)
-        copies.append(pltpu.make_async_copy(piece, into.at[place], sem.at[k]))
-        copies[-1].start()
+        fetch(piece, into.at[pl.ds((k % count) * CHUNK, CHUNK)])
     core = core_ref[0]
     here = pl.multiple_of(core * half, half)
     there = pl.multiple_of((1 - core) * half, half)
     total = x_ref.shape[0]
-    step = total // 3
-    for copy in first:
-        copy.wait()
-    g1, u1, d1, g2, u2, d2 = (w_ref.at[k] for k in range(6))
+    step = total // 2
+    groups = LIVE // 4
+    maps = [tail_maps(step, g) for g in range(groups)]
+    lane = iota2((step, 128), 1)
     for start in range(0, total, step):
         band = pl.ds(start, step)
-        x = x_ref[band, :width]
-        w = x_ref[band, width : width + 1].astype(F32)
-        h1 = (w * silu(dot_t(x, g1[...])) * dot_t(x, u1[...])).astype(BF16)
-        h2 = (w * silu(dot_t(x, g2[...])) * dot_t(x, u2[...])).astype(BF16)
-        acc_ref[...] = dot(h1, d1[...]) + dot(h2, d2[...])
+        tail = jnp.zeros((step, TAIL), F32)
+        w = jnp.zeros((step, 128), F32)
+        for g in range(groups):
+            tail = tail + dot(maps[g][0], x_ref[band, g * TAIL : (g + 1) * TAIL])
+            w = w + jnp.where(
+                lane == g, dot(maps[g][0], x_ref[band, groups * TAIL : groups * TAIL + 128]), 0.0
+            )
+        w = jnp.sum(w, axis=1, keepdims=True)
+        full_ref[:, :MAIN] = x_ref[band, :]
+        full_ref[:, MAIN:] = tail.astype(BF16)
         if start == 0:
-            for copy in copies:
+            for copy in copies[:6]:
                 copy.wait()
-        pre = dot_t(x_ref[band, pl.ds(here, half)], own_ref[...])
-        pre = pre + dot_t(x_ref[band, pl.ds(there, half)], other_ref[...])
+            for k in range(2):
+                down_ref[k * lanes + units : (k + 1) * lanes, :] = jnp.zeros(
+                    (lanes - units, 2 * half), BF16
+                )
+        pre = dot_t(full_ref[...], up_ref[...])
+        h = w * silu(pre[:, : 2 * lanes]) * pre[:, 2 * lanes :]
+        h = jnp.where((iota2(h.shape, 1) & (lanes - 1)) < units, h, 0.0).astype(BF16)
+        acc_ref[...] = dot(h, down_ref[...])
+        if start == 0:
+            for copy in copies[6:]:
+                copy.wait()
+        pre = dot_t(full_ref[:, pl.ds(here, half)], own_ref[...])
+        pre = pre + dot_t(full_ref[:, pl.ds(there, half)], other_ref[...])
         logit = pre[:, hidden : hidden + 1]
         gate = pltpu.roll(pre, 2 * PAD, 1)
         up = pltpu.roll(pre, PAD, 1)
-        unit = lax.broadcasted_iota(jnp.int32, pre.shape, 1) % CHUNK
+        unit = iota2(pre.shape, 1) % CHUNK
         live = (unit >= 2 * PAD) & (unit < 2 * PAD + hidden)
         scale = 0.5 / (1.0 + jnp.exp(-logit))
+        live = live & (w > 0.0)
         hd = jnp.where(live, scale * silu(gate) * up, 0.0).astype(BF16)
         acc_ref[:, pl.ds(here, half)] += dot(hd, own_ref[...])
         acc_ref[:, pl.ds(there, half)] += dot(hd, other_ref[...])
-        out_ref[band, :] = acc_ref[...].astype(BF16)
+        tail = acc_ref[:, MAIN:].astype(BF16)
+        for g in range(groups):
+            part = slice(g * TAIL, (g + 1) * TAIL)
+            out_ref[band, part] = (acc_ref[:, part] + dot(maps[g][1], tail)).astype(BF16)
+        out_ref[band, groups * TAIL :] = acc_ref[:, groups * TAIL : MAIN].astype(BF16)
 
 
 def in_vmem(value):
@@ -108,17 +154,96 @@
     return pl.pallas_call(
         lambda *refs: branch_kernel(hidden, *refs),
         name="branch",
-        out_shape=pltpu.VMEM((rows, width), BF16),
-        in_specs=[pl.BlockSpec(memory_space=pltpu.SMEM)] + [vmem] + [hbm] * (6 + 2 * len(pieces)),
+        out_shape=pltpu.VMEM((rows, MAIN), BF16),
+        in_specs=[pl.BlockSpec(memory_space=pltpu.SMEM), vmem] + [hbm] * (6 + 2 * len(pieces)),
         out_specs=vmem,
         scratch_shapes=[
-            pltpu.VMEM((6, *own[0].shape), BF16),
+            pltpu.VMEM((rows // 2, width), BF16),
+            pltpu.VMEM((4 * 128, width), BF16),
+            pltpu.VMEM((2 * 128, width), BF16),
             pltpu.VMEM((units, half), BF16),
             pltpu.VMEM((units, half), BF16),
-            pltpu.VMEM((rows // 3, width), F32),
+            pltpu.VMEM((rows // 2, width), F32),
             pltpu.SemaphoreType.DMA((6 + 2 * len(pieces),)),
         ],
     )(core.reshape(1), in_vmem(x), *own, *other, *pieces, *pieces2)
+
+
+def slot_source(core, row):
+    pair = divided(row, 5)
+    place = row - 5 * pair
+    crossed = place + jnp.where(place < SLOTS, SLOTS, -SLOTS)
+    return 6 * pair + jnp.where(core == 0, place, crossed)
+
+
+def spread_kernel(core_ref, x_ref, out_ref, rows_ref):
+    core = core_ref[0]
+    for k in range(x_ref.shape[0]):
+        rows_ref[k * SLOTS : (k + 1) * SLOTS, :] = x_ref[k].astype(F32)
+    x = rows_ref[...].astype(BF16)
+    width = MAIN + TAIL
+    shape = (ROWS, ROWS)
+    row, col = iota2(shape, 0), iota2(shape, 1)
+    main = dot(one_hot((row < LIVE) & (col == slot_source(core, row))), x[:, :MAIN])
+    groups = LIVE // 4
+    lane = iota2((ROWS, 128), 1)
+    weight = jnp.zeros((ROWS, 128), F32)
+    parts = []
+    for g in range(groups):
+        pick = one_hot((row >= LIVE) & (col == slot_source(core, 4 * g + row - LIVE)))
+        parts.append(main[:, g * TAIL : (g + 1) * TAIL] + dot(pick, x[:, MAIN:width]))
+        weight = weight + jnp.where(lane == g, dot(pick, x[:, width:]), 0.0)
+    parts.append(main[:, groups * TAIL : groups * TAIL + 128] + weight)
+    parts.append(main[:, groups * TAIL + 128 :])
+    packed = jnp.concatenate(parts, axis=1).astype(BF16)
+    for k in range(out_ref.shape[0]):
+        out_ref[k] = packed
+
+
+def spread(core, x, chips):
+    vmem = pl.BlockSpec(memory_space=pltpu.VMEM)
+    return pl.pallas_call(
+        spread_kernel,
+        name="spread",
+        out_shape=pltpu.VMEM((chips, ROWS, MAIN), BF16),
+        in_specs=[pl.BlockSpec(memory_space=pltpu.SMEM), vmem],
+        out_specs=vmem,
+        scratch_shapes=[pltpu.VMEM((EXPERTS * SLOTS, x.shape[2]), F32)],
+    )(core.reshape(1), in_vmem(x))
+
+
+def collect_kernel(core_ref, x_ref, out_ref, rows_ref):
+    core = core_ref[0]
+    half = out_ref.shape[2]
+    total = x_ref[0].astype(F32)
+    for k in range(1, x_ref.shape[0]):
+        total = total + x_ref[k].astype(F32)
+    total = total.astype(BF16)
+    shape = (ROWS, ROWS)
+    row, col = iota2(shape, 0), iota2(shape, 1)
+    rows_ref[:, :MAIN] = dot(one_hot((col < LIVE) & (row == slot_source(core, col))), total)
+    tail = jnp.zeros((ROWS, TAIL), F32)
+    for g in range(LIVE // 4):
+        pick = one_hot((col >= LIVE) & (row == slot_source(core, 4 * g + col - LIVE)))
+        tail = tail + dot(pick, total[:, g * TAIL : (g + 1) * TAIL])
+    rows_ref[:, MAIN:] = tail
+    for k in range(out_ref.shape[0]):
+        at = k // 2 * SLOTS
+        part = rows_ref[at : at + SLOTS, k % 2 * half : (k % 2 + 1) * half]
+        out_ref[k] = part.astype(BF16)
+
+
+def collect(core, x):
+    vmem = pl.BlockSpec(memory_space=pltpu.VMEM)
+    half = (MAIN + TAIL) // 2
+    return pl.pallas_call(
+        collect_kernel,
+        name="collect",
+        out_shape=pltpu.VMEM((2 * EXPERTS, SLOTS, half), BF16),
+        in_specs=[pl.BlockSpec(memory_space=pltpu.SMEM), vmem],
+        out_specs=vmem,
+        scratch_shapes=[pltpu.VMEM((ROWS, MAIN + TAIL), F32)],
+    )(core.reshape(1), in_vmem(x))
 
 
 def mixer_kernel(
@@ -204,8 +329,8 @@
     )
 
 
-def third(index):
-    return (index * 11) >> 5
+def first_slot(odd, core):
+    return jnp.where(odd == core, 0, SLOTS)
 
 
 def slots_kernel(
@@ -213,7 +338,7 @@
     slot_ref, after_ref,
 ):
     rows, half = x_ref.shape
-    core = core_ref[0]
+    core, odd = core_ref[0], core_ref[1]
     here = pl.multiple_of(core * half, half)
     there = pl.multiple_of((1 - core) * half, half)
 
@@ -231,68 +356,74 @@
     y = (y * scale * gain2_ref[...]).astype(BF16)
 
     shape = (EXPERTS * SLOTS, rows)
-    slot = lax.broadcasted_iota(jnp.int32, shape, 0)
-    expert = third(slot)
-    slot = slot - SLOTS * expert + SLOTS * core
+    slot = iota2(shape, 0)
+    expert = divided(slot, 3)
+    slot = slot - SLOTS * expert + first_slot(odd, core)
     first = (routes_ref[0:1, :] == expert).astype(F32)
     second = (routes_ref[1:2, :] == expert).astype(F32)
     member = first + second
-    earlier = lax.broadcasted_iota(jnp.int32, (rows, rows), 0) < lax.broadcasted_iota(
-        jnp.int32, (rows, rows), 1
-    )
-    place = dot(member.astype(BF16), earlier.astype(F32).astype(BF16))
+    earlier = iota2((rows, rows), 0) < iota2((rows, rows), 1)
+    place = dot(member.astype(BF16), one_hot(earlier))
     select = jnp.where(place == slot.astype(F32), member, 0.0)
     weight = first * weights_ref[0:1, :].astype(F32) + second * weights_ref[1:2, :].astype(F32)
     weight = jnp.sum(select * weight, axis=1, keepdims=True)
+    weight = jnp.broadcast_to(weight, (EXPERTS * SLOTS, 128))
     select = select.astype(BF16)
-    slot_ref[:, pl.ds(here, half)] = dot(select, x).astype(BF16)
-    slot_ref[:, pl.ds(there, half)] = dot(select, y).astype(BF16)
-    slot_ref[:, 2 * half :] = jnp.broadcast_to(weight, (EXPERTS * SLOTS, 128)).astype(BF16)
-
-
-def to_slots(core, own, other, mix, mix2, gain, gain2, routes, route_w):
+    x, y = dot(select, x), dot(select, y)
+    for k in range(EXPERTS):
+        part = slice(k * SLOTS, (k + 1) * SLOTS)
+        slot_ref[k, :, pl.ds(here, half)] = x[part].astype(BF16)
+        slot_ref[k, :, pl.ds(there, half)] = y[part].astype(BF16)
+        slot_ref[k, :, 2 * half :] = weight[part].astype(BF16)
+
+
+def to_slots(place, own, other, mix, mix2, gain, gain2, routes, route_w):
     rows, half = own.shape
     vmem = pl.BlockSpec(memory_space=pltpu.VMEM)
     return pl.pallas_call(
         slots_kernel,
         name="slots",
         out_shape=(
-            pltpu.VMEM((EXPERTS * SLOTS, 2 * half + 128), BF16),
+            pltpu.VMEM((EXPERTS, SLOTS, 2 * half + 128), BF16),
             pltpu.VMEM((rows, half), BF16),
         ),
         in_specs=[pl.BlockSpec(memory_space=pltpu.SMEM)] + [vmem] * 8,
         out_specs=(vmem, vmem),
     )(
-        core.reshape(1), in_vmem(own), in_vmem(other), in_vmem(mix), in_vmem(mix2),
+        place, in_vmem(own), in_vmem(other), in_vmem(mix), in_vmem(mix2),
         gain.reshape(1, half), in_vmem(gain2.reshape(1, half)), routes.T, route_w.T,
     )
 
 
-def home_kernel(home_ref, after_ref, routes_ref, out_ref):
+def home_kernel(core_ref, home_ref, after_ref, routes_ref, out_ref, rows_ref):
+    odd = core_ref[1]
     rows = after_ref.shape[0]
-    shape = (rows, home_ref.shape[0])
-    slot = lax.broadcasted_iota(jnp.int32, shape, 1)
-    expert = third(slot >> 1)
-    slot = slot - 2 * SLOTS * expert
+    count = home_ref.shape[0]
+    for k in range(count):
+        rows_ref[k * SLOTS : (k + 1) * SLOTS, :] = home_ref[k].astype(F32)
+    shape = (rows, count * SLOTS)
+    slot = iota2(shape, 1)
+    source = divided(slot, 3)
+    expert = source >> 1
+    slot = slot - SLOTS * source + first_slot(odd, source & 1)
     member = (routes_ref[:, 0:1] == expert).astype(F32) + (routes_ref[:, 1:2] == expert).astype(F32)
-    earlier = lax.broadcasted_iota(jnp.int32, (rows, rows), 1) < lax.broadcasted_iota(
-        jnp.int32, (rows, rows), 0
-    )
-    place = dot(earlier.astype(F32).astype(BF16), member.astype(BF16))
+    earlier = iota2((rows, rows), 1) < iota2((rows, rows), 0)
+    place = dot(one_hot(earlier), member.astype(BF16))
     select = jnp.where(place == slot.astype(F32), member, 0.0).astype(BF16)
-    total = after_ref[...].astype(F32) + dot(select, home_ref[...])
+    total = after_ref[...].astype(F32) + dot(select, rows_ref[...].astype(BF16))
     out_ref[...] = total.astype(BF16)
 
 
-def at_home(home, after, routes):
+def at_home(place, home, after, routes):
     vmem = pl.BlockSpec(memory_space=pltpu.VMEM)
     return pl.pallas_call(
         home_kernel,
         name="home",
         out_shape=jax.ShapeDtypeStruct(after.shape, BF16),
-        in_specs=[vmem] * 3,
+        in_specs=[pl.BlockSpec(memory_space=pltpu.SMEM)] + [vmem] * 3,
         out_specs=vmem,
-    )(in_vmem(home), in_vmem(after), routes)
+        scratch_shapes=[pltpu.VMEM((home.shape[0] * SLOTS, home.shape[2]), F32)],
+    )(place, in_vmem(home), in_vmem(after), routes)
 
 
 def layer(
@@ -301,7 +432,6 @@
 ):
     core = lax.axis_index("tp")
     half = tokens.shape[1]
-    width = 2 * half
     hidden = dense_gate.shape[1]
 
     def fill(size):
@@ -326,34 +456,25 @@
 
     mix, new_state = mixer(core, tokens, other_x, norm_mix, w_query, w_key, w_value, w_out, state)
     mix2 = swap(mix)
+    place = jnp.stack([core, lax.axis_index("ep_0") % 2])
     slot_rows, after = to_slots(
-        core, tokens, other_x, mix, mix2, norm_ffn, other_gain, routes, route_w
-    )
-    at_plane = lax.all_to_all(
-        slot_rows.reshape(EXPERTS, SLOTS, width + 128), "ep_0", 0, 0, tiled=True
-    ).reshape(EXPERTS * SLOTS, width + 128)
+        place, tokens, other_x, mix, mix2, norm_ffn, other_gain, routes, route_w
+    )
+    at_plane = lax.all_to_all(slot_rows, "ep_0", 0, 0, tiled=True)
     pieces = [packed]
     for shift in (4, 3, 5, 2, 6, 1, 7):
         pieces.append(along_z(packed, shift))
     pieces2 = [swap(piece) for piece in pieces]
-    gathered = to_all(at_plane, PLANE)
-    chips = gathered.shape[0]
+    chips = lax.axis_size(PLANE)
+    copies = spread(core, at_plane, chips)
+    gathered = lax.all_to_all(copies, PLANE, 0, 0, tiled=True)
     partial = experts_and_dense(
-        core,
-        gathered.reshape(-1, width + 128),
-        mine,
-        theirs,
-        pieces,
-        pieces2,
-        hidden,
-    )
-    back = lax.all_to_all(partial.reshape(chips, EXPERTS * SLOTS, width), PLANE, 0, 0, tiled=True)
-    summed = jnp.sum(back.astype(F32), axis=0).astype(BF16)
-    send = summed.reshape(EXPERTS, SLOTS, 2, half).transpose(0, 2, 1, 3)
-    home = lax.all_to_all(
-        send.reshape(2 * EXPERTS, SLOTS, half), ("ep_0", "tp"), 0, 0, tiled=True
-    ).reshape(2 * EXPERTS * SLOTS, half)
-    return (at_home(home, after, routes), new_state)
+        core, gathered.reshape(chips * ROWS, MAIN), mine, theirs, pieces, pieces2, hidden
+    )
+    back = lax.all_to_all(partial.reshape(chips, ROWS, MAIN), PLANE, 0, 0, tiled=True)
+    send = collect(core, back)
+    home = lax.all_to_all(send, ("ep_0", "tp"), 0, 0, tiled=True)
+    return (at_home(place, home, after, routes), new_state)
 
 
 def solution(mesh):

time: 134 us -> 131 us (0.978)
  starting transfers between devices: 38.9 us -> 36.2 us
  local copies, waits for them, and re-layouts: 6.03 us -> 3.74 us
  blocking collectives: 43.3 us -> 41.2 us
  Pallas kernels: 18.4 us -> 20.1 us
  waiting for transfers between devices: 26 us -> 27.6 us
    ppermute x7, starting transfers between devices: 12 us -> 9.44 us  [along_z(): lax.ppermute(value, 'ep_0', [(i, (i + shift) % size) for i in range(size)])]
    pallas_call x0 -> x2, Pallas kernels: none -> 2.43 us  [the longest x1 1.42 us: spread(): pl.pallas_call(spread_kernel, name='spread', out_shape=pltpu.VMEM((chips,...]
    ppermute x7, waiting for transfers between devices: 13.2 us -> 15.6 us  [along_z(): lax.ppermute(value, 'ep_0', [(i, (i + shift) % size) for i in range(size)])]
    all_to_all x2, blocking collectives: 43.3 us -> 41.2 us  [the longest x1 26.8 us: layer(): lax.all_to_all(partial.reshape(chips, ROWS, MAIN), PLANE, 0, 0, tiled=True)]
    broadcast_in_dim x2 -> x0, local copies, waits for them, and re-layouts: 1.4 us -> none  [to_all(): copies = jnp.broadcast_to(value[None], (size, *value.shape))]
    unnamed x57 -> x55, local copies, waits for them, and re-layouts: 3.5 us -> 3.51 us
  transfers between devices with their start and end apart: 23 -> 23, of which waited for: 8 -> 8; matrix products, arithmetic and copies ran while one was open for 1% -> 1% of each run, Pallas kernels for 0% -> 4%
where the time goes in v2:
time: 131 us; the launch traced here: 130 us
  blocking collectives  41.2 us (31%)
  starting transfers between devices  36.2 us (28%)
  waiting for transfers between devices  27.6 us (21%)
  Pallas kernels  20.1 us (15%)
  local copies, waits for them, and re-layouts  3.74 us (3%)
    all_to_all x1, blocking collectives, layer(): lax.all_to_all(partial.reshape(chips, ROWS, MAIN), PLANE, 0, 0, tiled=True)  26.8 us
    ppermute x7, waiting for transfers between devices, along_z(): lax.ppermute(value, 'ep_0', [(i, (i + shift) % size) for i in range(size)])  15.6 us
    all_to_all x1, blocking collectives, layer(): at_plane = lax.all_to_all(slot_rows, 'ep_0', 0, 0, tiled=True)  14.4 us
    ppermute x14, starting transfers between devices, swap(): return lax.ppermute(value, 'tp', [(0, 1), (1, 0)])  13.5 us
    ppermute x7, starting transfers between devices, along_z(): lax.ppermute(value, 'ep_0', [(i, (i + shift) % size) for i in range(size)])  9.44 us
    pallas_call x1, Pallas kernels, experts_and_dense(): pl.pallas_call(lambda *refs: branch_kernel(hidden, *refs), name='branch',...  9 us
    all_to_all x1, waiting for transfers between devices, layer(): home = lax.all_to_all(send, ('ep_0', 'tp'), 0, 0, tiled=True)  8.19 us
    all_to_all x1, starting transfers between devices, layer(): gathered = lax.all_to_all(copies, PLANE, 0, 0, tiled=True)  6.88 us
  transfers between devices with their start and end apart: 23, of which 8 were waited for; matrix products, arithmetic and copies ran while one was open for 1% of the time, Pallas kernels for 4%

profile of v2, /device:TPU:1, one launch (start us, length us, event | category | flops | bytes accessed | tf_op | source)
XLA Modules:
  0.0 130.4 jit_solution(677311537441467384)
XLA Ops:
  0.6 3.3 %collective-permute-start = (bf16[16,1024]{1,0:T(8,128)(2,1)}, bf16[16,1024]{1,0:T(8,128)(2,1)S(1)}, u32[]{:S(2)}, u32[]{:S(2)}) collective-permute-start(bf16[16,1024]{1,0:T(8,128)(2,1)} %x_ref.3), channel_id=1, source_target_pairs={{0,1},{1,0},{2,3},{3,2},{4,5},{5,4},{6,7},{7,6},{8,9},{9,8},{10,11... | collective-permute-start | bytes 98312 | tf_op jit(solution)/shard_map/ppermute | solution.py:27
  3.9 0.1 collective-permute-start.2
  4.0 1.0 collective-permute-done.y_ref
  5.0 0.8 copy-done
  5.7 5.9 %mixer.1 = (bf16[16,2048]{1,0:T(8,128)(2,1)S(1)}, f32[16,2,128,128]{3,2,1,0:T(8,128)}) custom-call(s32[1]{0:T(128)} %bitcast.core_ref.refs_0_, bf16[16,1024]{1,0:T(8,128)(2,1)S(1)} %copy-done, bf16[16,1024]{1,0:T(8,128)(2,1)S(1)} %collective-permute-done.y_ref, f32[1,2048]{1,0:T(1,128)} %bitcast.29, bf16[2048,256]{1,0:T(8,128)(2,1)} %wq.1, ...), custom_call_target="tpu_custom_call" | custom-call | tf_op jit(solution)/shard_map/mixer/pallas_call | solution.py:311
  11.6 0.4 collective-permute-start.1
  12.0 0.7 pad_add_fusion.core_ref
  12.7 0.2 collective-permute-done.1.mix2_ref
  13.0 1.1 slots.1
  14.1 14.4 %all_to_all.20.x_ref = bf16[8,3,2176]{2,1,0:T(4,128)(2,1)S(1)} all-to-all(bf16[8,3,2176]{2,1,0:T(4,128)(2,1)S(1)} %get-tuple-element.7), channel_id=1, replica_groups=mesh['ep_0'=8,'ep_1'=4,'ep_2'=4,'tp'=2] {'ep_0'}, dimensions={0} | all-to-all | bytes 208896 | tf_op jit(solution)/shard_map/all_to_all | solution.py:463
  28.5 1.4 %spread.1 = bf16[16,24,1792]{2,1,0:T(8,128)(2,1)} custom-call(s32[1]{0:T(128)} %bitcast.core_ref.refs_0_, bf16[8,3,2176]{2,1,0:T(4,128)(2,1)S(1)} %all_to_all.20.x_ref), custom_call_target="tpu_custom_call" | custom-call | tf_op jit(solution)/shard_map/spread/pallas_call | solution.py:205
  30.0 0.0 copy-start.3
  30.0 0.0 copy-start.4
  30.0 6.9 %all-to-all-start.1 = ((bf16[16,24,1792]{2,1,0:T(8,128)(2,1)}), bf16[16,24,1792]{2,1,0:T(8,128)(2,1)S(1)}, u32[]{:S(2)}, u32[]{:S(2)}) async-start(bf16[16,24,1792]{2,1,0:T(8,128)(2,1)} %spread.1), calls=%async_computation.1 | async-start | bytes 2752512 | tf_op jit(solution)/shard_map/all_to_all | solution.py:470
  37.0 0.2 concatenate.3.refs_8_
  37.2 1.1 collective-permute-start.6
  38.3 1.4 %collective-permute-start.7 = (bf16[80,1024]{1,0:T(8,128)(2,1)S(1)}, bf16[80,1024]{1,0:T(8,128)(2,1)S(1)}, u32[]{:S(2)}, u32[]{:S(2)}) collective-permute-start(bf16[80,1024]{1,0:T(8,128)(2,1)S(1)} %concatenate.3.refs_8_), channel_id=1, source_target_pairs={{0,96},{32,128},{64,160},{96,192},{128,224},{160,0},{192,32},{224,... | collective-permute-start | bytes 491528 | tf_op jit(solution)/shard_map/ppermute | solution.py:32
  39.8 3.1 %collective-permute-start.8 = (bf16[80,1024]{1,0:T(8,128)(2,1)S(1)}, bf16[80,1024]{1,0:T(8,128)(2,1)S(1)}, u32[]{:S(2)}, u32[]{:S(2)}) collective-permute-start(bf16[80,1024]{1,0:T(8,128)(2,1)S(1)} %concatenate.3.refs_8_), channel_id=1, source_target_pairs={{0,160},{32,192},{64,224},{96,0},{128,32},{160,64},{192,96},{224,1... | collective-permute-start | bytes 491528 | tf_op jit(solution)/shard_map/ppermute | solution.py:32
  42.8 2.2 %collective-permute-start.9 = (bf16[80,1024]{1,0:T(8,128)(2,1)S(1)}, bf16[80,1024]{1,0:T(8,128)(2,1)S(1)}, u32[]{:S(2)}, u32[]{:S(2)}) collective-permute-start(bf16[80,1024]{1,0:T(8,128)(2,1)S(1)} %concatenate.3.refs_8_), channel_id=1, source_target_pairs={{0,64},{32,96},{64,128},{96,160},{128,192},{160,224},{192,0},{224,... | collective-permute-start | bytes 491528 | tf_op jit(solution)/shard_map/ppermute | solution.py:32
  45.0 1.4 %collective-permute-start.10 = (bf16[80,1024]{1,0:T(8,128)(2,1)S(1)}, bf16[80,1024]{1,0:T(8,128)(2,1)S(1)}, u32[]{:S(2)}, u32[]{:S(2)}) collective-permute-start(bf16[80,1024]{1,0:T(8,128)(2,1)S(1)} %concatenate.3.refs_8_), channel_id=1, source_target_pairs={{0,192},{32,224},{64,0},{96,32},{128,64},{160,96},{192,128},{224,1... | collective-permute-start | bytes 491528 | tf_op jit(solution)/shard_map/ppermute | solution.py:32
  46.4 0.3 collective-permute-start.11
  46.7 14.7 %collective-permute-done.7.refs_10_ = bf16[80,1024]{1,0:T(8,128)(2,1)S(1)} collective-permute-done((bf16[80,1024]{1,0:T(8,128)(2,1)S(1)}, bf16[80,1024]{1,0:T(8,128)(2,1)S(1)}, u32[]{:S(2)}, u32[]{:S(2)}) %collective-permute-start.7) | collective-permute-done | bytes 163872 | tf_op jit(solution)/shard_map/ppermute | solution.py:32
  61.4 4.2 %collective-permute-start.13 = (bf16[80,1024]{1,0:T(8,128)(2,1)S(1)}, bf16[80,1024]{1,0:T(8,128)(2,1)S(1)}, u32[]{:S(2)}, u32[]{:S(2)}) collective-permute-start(bf16[80,1024]{1,0:T(8,128)(2,1)S(1)} %concatenate.3.refs_8_), channel_id=1, source_target_pairs={{0,1},{1,0},{2,3},{3,2},{4,5},{5,4},{6,7},{7,6},{8,9},{9,8},{10,11... | collective-permute-start | bytes 491528 | tf_op jit(solution)/shard_map/ppermute | solution.py:27
  65.6 2.6 %collective-permute-start.14 = (bf16[80,1024]{1,0:T(8,128)(2,1)S(1)}, bf16[80,1024]{1,0:T(8,128)(2,1)S(1)}, u32[]{:S(2)}, u32[]{:S(2)}) collective-permute-start(bf16[80,1024]{1,0:T(8,128)(2,1)S(1)} %collective-permute-done.6.refs_9_), channel_id=1, source_target_pairs={{0,1},{1,0},{2,3},{3,2},{4,5},{5,4},{6,7},{7,6},{8,9},{9,8},{10,11... | collective-permute-start | bytes 491528 | tf_op jit(solution)/shard_map/ppermute | solution.py:27
  68.2 0.1 collective-permute-start.15
  68.3 0.9 collective-permute-done.11.refs_14_
  69.2 0.7 collective-permute-start.16
  69.9 0.3 collective-permute-start.3
  70.3 0.7 copy-done.14
  70.9 0.4 collective-permute-start.4
  71.4 0.2 collective-permute-start.5
  71.5 0.4 collective-permute-start.17
  72.0 0.1 collective-permute-start.18
  72.1 1.3 %collective-permute-done.17.refs_20_ = bf16[80,1024]{1,0:T(8,128)(2,1)S(1)} collective-permute-done((bf16[80,1024]{1,0:T(8,128)(2,1)S(1)}, bf16[80,1024]{1,0:T(8,128)(2,1)S(1)}, u32[]{:S(2)}, u32[]{:S(2)}) %collective-permute-start.17) | collective-permute-done | bytes 163872 | tf_op jit(solution)/shard_map/ppermute | solution.py:27
  73.4 0.4 collective-permute-start.19
  73.8 0.2 collective-permute-start.20
  74.0 0.8 collective-permute-done.19.refs_22_
  74.8 0.4 collective-permute-done.20.refs_23_
  75.3 0.2 copy-done.20
  75.5 0.4 copy-done.21
  75.9 0.7 copy-done.6
  76.6 9.0 %branch.1 = bf16[384,1792]{1,0:T(8,128)(2,1)S(1)} custom-call(s32[1]{0:T(128)} %bitcast.core_ref.refs_0_, bf16[384,1792]{1,0:T(8,128)(2,1)S(1)} %bitcast.18, bf16[88,2048]{1,0:T(8,128)(2,1)} %bitcast.21, bf16[88,2048]{1,0:T(8,128)(2,1)} %bitcast.23, bf16[88,2048]{1,0:T(8,128)(2,1)} %bitcast.25, bf16[88,2048]{1,0:T(8,128)(2,1)} %copy-done.5, ...), custom_call_target="tpu_custom_call" | custom-call | tf_op jit(solution)/shard_map/branch/pallas_call | solution.py:154
  85.6 26.8 %all_to_all.21.x_ref = bf16[16,24,1792]{2,1,0:T(8,128)(2,1)S(1)} all-to-all(bf16[16,24,1792]{2,1,0:T(8,128)(2,1)S(1)} %bitcast.19), channel_id=1, replica_groups=mesh['ep_0'=8,'ep_1'=4,'ep_2'=4,'tp'=2] {'ep_1','ep_2'}, dimensions={0} | all-to-all | bytes 2752512 | tf_op jit(solution)/shard_map/all_to_all | solution.py:474
  112.4 1.0 collect.1
  113.4 6.5 %all-to-all-start.3 = ((bf16[16,3,1024]{2,1,0:T(4,128)(2,1)}), bf16[16,3,1024]{2,1,0:T(4,128)(2,1)S(1)}, u32[]{:S(2)}, u32[]{:S(2)}) async-start(bf16[16,3,1024]{2,1,0:T(4,128)(2,1)} %collect.1), calls=%async_computation.3 | async-start | bytes 262144 | tf_op jit(solution)/shard_map/all_to_all | solution.py:476
  119.9 0.7 copy.19.routes_ref
  120.6 8.2 %all-to-all-done.3.home_ref = bf16[16,3,1024]{2,1,0:T(4,128)(2,1)S(1)} async-done(((bf16[16,3,1024]{2,1,0:T(4,128)(2,1)}), bf16[16,3,1024]{2,1,0:T(4,128)(2,1)S(1)}, u32[]{:S(2)}, u32[]{:S(2)}) %all-to-all-start.3) | async-done | bytes 98336 | tf_op jit(solution)/shard_map/all_to_all | solution.py:476
  128.8 1.6 %home.1 = bf16[16,1024]{1,0:T(8,128)(2,1)} custom-call(s32[2]{0:T(128)} %pad_add_fusion.core_ref, bf16[16,3,1024]{2,1,0:T(4,128)(2,1)S(1)} %all-to-all-done.3.home_ref, bf16[16,1024]{1,0:T(8,128)(2,1)S(1)} %get-tuple-element.8.after_ref, s32[16,2]{1,0:T(8,128)} %copy.19.routes_ref), custom_call_target="tpu_custom_call" | custom-call | tf_op jit(solution)/shard_map/home/pallas_call | solution.py:419
  (67 shorter events, 0.2 us)
Async XLA Ops:
  0.6 4.4 %collective-permute-start = (bf16[16,1024]{1,0:T(8,128)(2,1)}, bf16[16,1024]{1,0:T(8,128)(2,1)S(1)}, u32[]{:S(2)}, u32[]{:S(2)}) collective-permute-start(bf16[16,1024]{1,0:T(8,128)(2,1)} %x_ref.3), channel_id=1, source_target_pairs={{0,1},{1,0},{2,3},{3,2},{4,5},{5,4},{6,7},{7,6},{8,9},{9,8},{10,11... | collective-permute-start | bytes 98312 | tf_op jit(solution)/shard_map/ppermute | solution.py:27
  3.9 8.8 %collective-permute-start.2 = (f32[1024]{0:T(1024)}, f32[1024]{0:T(1024)S(1)}, u32[]{:S(2)}, u32[]{:S(2)}) collective-permute-start(f32[1024]{0:T(1024)} %param.24), channel_id=1, source_target_pairs={{0,1},{1,0},{2,3},{3,2},{4,5},{5,4},{6,7},{7,6},{8,9},{9,8},{10,11... | collective-permute-start | bytes 12296 | tf_op jit(solution)/shard_map/ppermute | solution.py:27
  5.0 0.8 copy-start
  11.6 1.3 %collective-permute-start.1 = (bf16[16,2048]{1,0:T(8,128)(2,1)S(1)}, bf16[16,2048]{1,0:T(8,128)(2,1)S(1)}, u32[]{:S(2)}, u32[]{:S(2)}) collective-permute-start(bf16[16,2048]{1,0:T(8,128)(2,1)S(1)} %get-tuple-element.6.mix_ref), channel_id=1, source_target_pairs={{0,1},{1,0},{2,3},{3,2},{4,5},{5,4},{6,7},{7,6},{8,9},{9,8},{10,11... | collective-permute-start | bytes 196616 | tf_op jit(solution)/shard_map/ppermute | solution.py:27
  29.9 6.9 %copy-start.26 = (bf16[1024]{0:T(1024)(128)(2,1)S(1)}, bf16[1024]{0:T(1024)(128)(2,1)}, u32[]{:S(2)}) copy-start(bf16[1024]{0:T(1024)(128)(2,1)} %param.25) | copy-start | bytes 6148
  29.9 7.0 %copy-start.22 = (bf16[1024,22]{0,1:T(8,128)(2,1)S(1)}, bf16[1024,22]{0,1:T(8,128)(2,1)}, u32[]{:S(2)}) copy-start(bf16[1024,22]{0,1:T(8,128)(2,1)} %param.26) | copy-start | bytes 135172
  30.0 7.0 %copy-start.23 = (bf16[1024,22]{0,1:T(8,128)(2,1)S(1)}, bf16[1024,22]{0,1:T(8,128)(2,1)}, u32[]{:S(2)}) copy-start(bf16[1024,22]{0,1:T(8,128)(2,1)} %param.27) | copy-start | bytes 135172
  30.0 7.0 %copy-start.24 = (bf16[22,1024]{1,0:T(8,128)(2,1)S(1)}, bf16[22,1024]{1,0:T(8,128)(2,1)}, u32[]{:S(2)}) copy-start(bf16[22,1024]{1,0:T(8,128)(2,1)} %param.28) | copy-start | bytes 135172
  30.0 39.9 %copy-start.2 = (bf16[1,2048,88]{1,2,0:T(8,128)(2,1)S(1)}, bf16[1,2048,88]{1,2,0:T(8,128)(2,1)}, u32[]{:S(2)}) copy-start(bf16[1,2048,88]{1,2,0:T(8,128)(2,1)} %param.29) | copy-start | bytes 1081348
  30.0 41.0 %copy-start.3 = (bf16[1,2048,88]{1,2,0:T(8,128)(2,1)S(1)}, bf16[1,2048,88]{1,2,0:T(8,128)(2,1)}, u32[]{:S(2)}) copy-start(bf16[1,2048,88]{1,2,0:T(8,128)(2,1)} %param.30) | copy-start | bytes 1081348
  30.0 41.4 %copy-start.4 = (bf16[1,88,2048]{2,1,0:T(8,128)(2,1)S(1)}, bf16[1,88,2048]{2,1,0:T(8,128)(2,1)}, u32[]{:S(2)}) copy-start(bf16[1,88,2048]{2,1,0:T(8,128)(2,1)} %param.31) | copy-start | bytes 1081348
  30.0 46.6 %all-to-all-start.1 = ((bf16[16,24,1792]{2,1,0:T(8,128)(2,1)}), bf16[16,24,1792]{2,1,0:T(8,128)(2,1)S(1)}, u32[]{:S(2)}, u32[]{:S(2)}) async-start(bf16[16,24,1792]{2,1,0:T(8,128)(2,1)} %spread.1), calls=%async_computation.1 | async-start | bytes 2752512 | tf_op jit(solution)/shard_map/all_to_all | solution.py:470
  37.2 39.4 %copy-start.1 = (bf16[80,1024]{1,0:T(8,128)(2,1)}, bf16[80,1024]{1,0:T(8,128)(2,1)S(1)}, u32[]{:S(2)}) copy-start(bf16[80,1024]{1,0:T(8,128)(2,1)S(1)} %concatenate.3.refs_8_) | copy-start | bytes 491524
  37.2 9.2 %collective-permute-start.6 = (bf16[80,1024]{1,0:T(8,128)(2,1)S(1)}, bf16[80,1024]{1,0:T(8,128)(2,1)S(1)}, u32[]{:S(2)}, u32[]{:S(2)}) collective-permute-start(bf16[80,1024]{1,0:T(8,128)(2,1)S(1)} %concatenate.3.refs_8_), channel_id=1, source_target_pairs={{0,128},{32,160},{64,192},{96,224},{128,0},{160,32},{192,64},{224,... | collective-permute-start | bytes 491528 | tf_op jit(solution)/shard_map/ppermute | solution.py:32
  38.3 23.0 %collective-permute-start.7 = (bf16[80,1024]{1,0:T(8,128)(2,1)S(1)}, bf16[80,1024]{1,0:T(8,128)(2,1)S(1)}, u32[]{:S(2)}, u32[]{:S(2)}) collective-permute-start(bf16[80,1024]{1,0:T(8,128)(2,1)S(1)} %concatenate.3.refs_8_), channel_id=1, source_target_pairs={{0,96},{32,128},{64,160},{96,192},{128,224},{160,0},{192,32},{224,... | collective-permute-start | bytes 491528 | tf_op jit(solution)/shard_map/ppermute | solution.py:32
  39.8 21.6 %collective-permute-start.8 = (bf16[80,1024]{1,0:T(8,128)(2,1)S(1)}, bf16[80,1024]{1,0:T(8,128)(2,1)S(1)}, u32[]{:S(2)}, u32[]{:S(2)}) collective-permute-start(bf16[80,1024]{1,0:T(8,128)(2,1)S(1)} %concatenate.3.refs_8_), channel_id=1, source_target_pairs={{0,160},{32,192},{64,224},{96,0},{128,32},{160,64},{192,96},{224,1... | collective-permute-start | bytes 491528 | tf_op jit(solution)/shard_map/ppermute | solution.py:32
  42.8 22.8 %collective-permute-start.9 = (bf16[80,1024]{1,0:T(8,128)(2,1)S(1)}, bf16[80,1024]{1,0:T(8,128)(2,1)S(1)}, u32[]{:S(2)}, u32[]{:S(2)}) collective-permute-start(bf16[80,1024]{1,0:T(8,128)(2,1)S(1)} %concatenate.3.refs_8_), channel_id=1, source_target_pairs={{0,64},{32,96},{64,128},{96,160},{128,192},{160,224},{192,0},{224,... | collective-permute-start | bytes 491528 | tf_op jit(solution)/shard_map/ppermute | solution.py:32
  45.0 23.2 %collective-permute-start.10 = (bf16[80,1024]{1,0:T(8,128)(2,1)S(1)}, bf16[80,1024]{1,0:T(8,128)(2,1)S(1)}, u32[]{:S(2)}, u32[]{:S(2)}) collective-permute-start(bf16[80,1024]{1,0:T(8,128)(2,1)S(1)} %concatenate.3.refs_8_), channel_id=1, source_target_pairs={{0,192},{32,224},{64,0},{96,32},{128,64},{160,96},{192,128},{224,1... | collective-permute-start | bytes 491528 | tf_op jit(solution)/shard_map/ppermute | solution.py:32
  46.4 30.2 %copy-start.7 = (bf16[80,1024]{1,0:T(8,128)(2,1)}, bf16[80,1024]{1,0:T(8,128)(2,1)S(1)}, u32[]{:S(2)}) copy-start(bf16[80,1024]{1,0:T(8,128)(2,1)S(1)} %collective-permute-done.6.refs_9_) | copy-start | bytes 491524
  46.4 22.8 %collective-permute-start.11 = (bf16[80,1024]{1,0:T(8,128)(2,1)S(1)}, bf16[80,1024]{1,0:T(8,128)(2,1)S(1)}, u32[]{:S(2)}, u32[]{:S(2)}) collective-permute-start(bf16[80,1024]{1,0:T(8,128)(2,1)S(1)} %concatenate.3.refs_8_), channel_id=1, source_target_pairs={{0,32},{32,64},{64,96},{96,128},{128,160},{160,192},{192,224},{224... | collective-permute-start | bytes 491528 | tf_op jit(solution)/shard_map/ppermute | solution.py:32
  61.4 15.3 %copy-start.8 = (bf16[80,1024]{1,0:T(8,128)(2,1)}, bf16[80,1024]{1,0:T(8,128)(2,1)S(1)}, u32[]{:S(2)}) copy-start(bf16[80,1024]{1,0:T(8,128)(2,1)S(1)} %collective-permute-done.7.refs_10_) | copy-start | bytes 491524
  61.4 8.5 %collective-permute-start.12 = (bf16[80,1024]{1,0:T(8,128)(2,1)S(1)}, bf16[80,1024]{1,0:T(8,128)(2,1)S(1)}, u32[]{:S(2)}, u32[]{:S(2)}) collective-permute-start(bf16[80,1024]{1,0:T(8,128)(2,1)S(1)} %concatenate.3.refs_8_), channel_id=1, source_target_pairs={{0,224},{32,0},{64,32},{96,64},{128,96},{160,128},{192,160},{224,1... | collective-permute-start | bytes 491528 | tf_op jit(solution)/shard_map/ppermute | solution.py:32
  61.4 13.8 %copy-start.9 = (bf16[80,1024]{1,0:T(8,128)(2,1)}, bf16[80,1024]{1,0:T(8,128)(2,1)S(1)}, u32[]{:S(2)}) copy-start(bf16[80,1024]{1,0:T(8,128)(2,1)S(1)} %collective-permute-done.8.refs_11_) | copy-start | bytes 491524
  61.4 8.9 %collective-permute-start.13 = (bf16[80,1024]{1,0:T(8,128)(2,1)S(1)}, bf16[80,1024]{1,0:T(8,128)(2,1)S(1)}, u32[]{:S(2)}, u32[]{:S(2)}) collective-permute-start(bf16[80,1024]{1,0:T(8,128)(2,1)S(1)} %concatenate.3.refs_8_), channel_id=1, source_target_pairs={{0,1},{1,0},{2,3},{3,2},{4,5},{5,4},{6,7},{7,6},{8,9},{9,8},{10,11... | collective-permute-start | bytes 491528 | tf_op jit(solution)/shard_map/ppermute | solution.py:27
  65.6 9.6 %copy-start.10 = (bf16[80,1024]{1,0:T(8,128)(2,1)}, bf16[80,1024]{1,0:T(8,128)(2,1)S(1)}, u32[]{:S(2)}) copy-start(bf16[80,1024]{1,0:T(8,128)(2,1)S(1)} %collective-permute-done.9.refs_12_) | copy-start | bytes 491524
  65.6 5.7 %collective-permute-start.14 = (bf16[80,1024]{1,0:T(8,128)(2,1)S(1)}, bf16[80,1024]{1,0:T(8,128)(2,1)S(1)}, u32[]{:S(2)}, u32[]{:S(2)}) collective-permute-start(bf16[80,1024]{1,0:T(8,128)(2,1)S(1)} %collective-permute-done.6.refs_9_), channel_id=1, source_target_pairs={{0,1},{1,0},{2,3},{3,2},{4,5},{5,4},{6,7},{7,6},{8,9},{9,8},{10,11... | collective-permute-start | bytes 491528 | tf_op jit(solution)/shard_map/ppermute | solution.py:27
  68.2 7.0 %copy-start.11 = (bf16[80,1024]{1,0:T(8,128)(2,1)}, bf16[80,1024]{1,0:T(8,128)(2,1)S(1)}, u32[]{:S(2)}) copy-start(bf16[80,1024]{1,0:T(8,128)(2,1)S(1)} %collective-permute-done.10.refs_13_) | copy-start | bytes 491524
  68.2 3.4 %collective-permute-start.15 = (bf16[80,1024]{1,0:T(8,128)(2,1)S(1)}, bf16[80,1024]{1,0:T(8,128)(2,1)S(1)}, u32[]{:S(2)}, u32[]{:S(2)}) collective-permute-start(bf16[80,1024]{1,0:T(8,128)(2,1)S(1)} %collective-permute-done.7.refs_10_), channel_id=1, source_target_pairs={{0,1},{1,0},{2,3},{3,2},{4,5},{5,4},{6,7},{7,6},{8,9},{9,8},{10,11... | collective-permute-start | bytes 491528 | tf_op jit(solution)/shard_map/ppermute | solution.py:27
  69.2 6.0 %copy-start.12 = (bf16[80,1024]{1,0:T(8,128)(2,1)}, bf16[80,1024]{1,0:T(8,128)(2,1)S(1)}, u32[]{:S(2)}) copy-start(bf16[80,1024]{1,0:T(8,128)(2,1)S(1)} %collective-permute-done.11.refs_14_) | copy-start | bytes 491524
  69.2 2.7 %collective-permute-start.16 = (bf16[80,1024]{1,0:T(8,128)(2,1)S(1)}, bf16[80,1024]{1,0:T(8,128)(2,1)S(1)}, u32[]{:S(2)}, u32[]{:S(2)}) collective-permute-start(bf16[80,1024]{1,0:T(8,128)(2,1)S(1)} %collective-permute-done.8.refs_11_), channel_id=1, source_target_pairs={{0,1},{1,0},{2,3},{3,2},{4,5},{5,4},{6,7},{7,6},{8,9},{9,8},{10,11... | collective-permute-start | bytes 491528 | tf_op jit(solution)/shard_map/ppermute | solution.py:27
  69.9 5.3 %copy-start.13 = (bf16[80,1024]{1,0:T(8,128)(2,1)}, bf16[80,1024]{1,0:T(8,128)(2,1)S(1)}, u32[]{:S(2)}) copy-start(bf16[80,1024]{1,0:T(8,128)(2,1)S(1)} %collective-permute-done.12.refs_15_) | copy-start | bytes 491524
  69.9 5.3 %collective-permute-start.3 = (bf16[88,2048]{1,0:T(8,128)(2,1)S(1)}, bf16[88,2048]{1,0:T(8,128)(2,1)S(1)}, u32[]{:S(2)}, u32[]{:S(2)}) collective-permute-start(bf16[88,2048]{1,0:T(8,128)(2,1)S(1)} %bitcast.22), channel_id=1, source_target_pairs={{0,1},{1,0},{2,3},{3,2},{4,5},{5,4},{6,7},{7,6},{8,9},{9,8},{10,11... | collective-permute-start | bytes 1081352 | tf_op jit(solution)/shard_map/ppermute | solution.py:27
  70.9 4.3 %collective-permute-start.4 = (bf16[88,2048]{1,0:T(8,128)(2,1)S(1)}, bf16[88,2048]{1,0:T(8,128)(2,1)S(1)}, u32[]{:S(2)}, u32[]{:S(2)}) collective-permute-start(bf16[88,2048]{1,0:T(8,128)(2,1)S(1)} %bitcast.24), channel_id=1, source_target_pairs={{0,1},{1,0},{2,3},{3,2},{4,5},{5,4},{6,7},{7,6},{8,9},{9,8},{10,11... | collective-permute-start | bytes 1081352 | tf_op jit(solution)/shard_map/ppermute | solution.py:27
  71.4 3.9 %copy-start.15 = (bf16[80,1024]{1,0:T(8,128)(2,1)}, bf16[80,1024]{1,0:T(8,128)(2,1)S(1)}, u32[]{:S(2)}) copy-start(bf16[80,1024]{1,0:T(8,128)(2,1)S(1)} %collective-permute-done.14.refs_17_) | copy-start | bytes 491524
  71.4 5.2 %collective-permute-start.5 = (bf16[88,2048]{1,0:T(8,128)(2,1)S(1)}, bf16[88,2048]{1,0:T(8,128)(2,1)}, u32[]{:S(2)}, u32[]{:S(2)}) collective-permute-start(bf16[88,2048]{1,0:T(8,128)(2,1)S(1)} %bitcast.26), channel_id=1, source_target_pairs={{0,1},{1,0},{2,3},{3,2},{4,5},{5,4},{6,7},{7,6},{8,9},{9,8},{10,11... | collective-permute-start | bytes 1081352 | tf_op jit(solution)/shard_map/ppermute | solution.py:27
  71.5 3.7 %copy-start.16 = (bf16[80,1024]{1,0:T(8,128)(2,1)}, bf16[80,1024]{1,0:T(8,128)(2,1)S(1)}, u32[]{:S(2)}) copy-start(bf16[80,1024]{1,0:T(8,128)(2,1)S(1)} %collective-permute-done.15.refs_18_) | copy-start | bytes 491524
  71.5 1.9 %collective-permute-start.17 = (bf16[80,1024]{1,0:T(8,128)(2,1)S(1)}, bf16[80,1024]{1,0:T(8,128)(2,1)S(1)}, u32[]{:S(2)}, u32[]{:S(2)}) collective-permute-start(bf16[80,1024]{1,0:T(8,128)(2,1)S(1)} %collective-permute-done.9.refs_12_), channel_id=1, source_target_pairs={{0,1},{1,0},{2,3},{3,2},{4,5},{5,4},{6,7},{7,6},{8,9},{9,8},{10,11... | collective-permute-start | bytes 491528 | tf_op jit(solution)/shard_map/ppermute | solution.py:27
  72.0 3.3 %copy-start.17 = (bf16[80,1024]{1,0:T(8,128)(2,1)}, bf16[80,1024]{1,0:T(8,128)(2,1)S(1)}, u32[]{:S(2)}) copy-start(bf16[80,1024]{1,0:T(8,128)(2,1)S(1)} %collective-permute-done.16.refs_19_) | copy-start | bytes 491524
  72.0 1.8 %collective-permute-start.18 = (bf16[80,1024]{1,0:T(8,128)(2,1)S(1)}, bf16[80,1024]{1,0:T(8,128)(2,1)S(1)}, u32[]{:S(2)}, u32[]{:S(2)}) collective-permute-start(bf16[80,1024]{1,0:T(8,128)(2,1)S(1)} %collective-permute-done.10.refs_13_), channel_id=1, source_target_pairs={{0,1},{1,0},{2,3},{3,2},{4,5},{5,4},{6,7},{7,6},{8,9},{9,8},{10,11... | collective-permute-start | bytes 491528 | tf_op jit(solution)/shard_map/ppermute | solution.py:27
  73.4 1.9 %copy-start.18 = (bf16[80,1024]{1,0:T(8,128)(2,1)}, bf16[80,1024]{1,0:T(8,128)(2,1)S(1)}, u32[]{:S(2)}) copy-start(bf16[80,1024]{1,0:T(8,128)(2,1)S(1)} %collective-permute-done.17.refs_20_) | copy-start | bytes 491524
  73.4 1.4 %collective-permute-start.19 = (bf16[80,1024]{1,0:T(8,128)(2,1)S(1)}, bf16[80,1024]{1,0:T(8,128)(2,1)S(1)}, u32[]{:S(2)}, u32[]{:S(2)}) collective-permute-start(bf16[80,1024]{1,0:T(8,128)(2,1)S(1)} %collective-permute-done.11.refs_14_), channel_id=1, source_target_pairs={{0,1},{1,0},{2,3},{3,2},{4,5},{5,4},{6,7},{7,6},{8,9},{9,8},{10,11... | collective-permute-start | bytes 491528 | tf_op jit(solution)/shard_map/ppermute | solution.py:27
  73.8 1.5 %copy-start.19 = (bf16[80,1024]{1,0:T(8,128)(2,1)}, bf16[80,1024]{1,0:T(8,128)(2,1)S(1)}, u32[]{:S(2)}) copy-start(bf16[80,1024]{1,0:T(8,128)(2,1)S(1)} %collective-permute-done.18.refs_21_) | copy-start | bytes 491524
  73.8 1.4 %collective-permute-start.20 = (bf16[80,1024]{1,0:T(8,128)(2,1)S(1)}, bf16[80,1024]{1,0:T(8,128)(2,1)S(1)}, u32[]{:S(2)}, u32[]{:S(2)}) collective-permute-start(bf16[80,1024]{1,0:T(8,128)(2,1)S(1)} %collective-permute-done.12.refs_15_), channel_id=1, source_target_pairs={{0,1},{1,0},{2,3},{3,2},{4,5},{5,4},{6,7},{7,6},{8,9},{9,8},{10,11... | collective-permute-start | bytes 491528 | tf_op jit(solution)/shard_map/ppermute | solution.py:27
  75.2 0.7 copy-start.21
  75.2 1.4 %copy-start.5 = (bf16[88,2048]{1,0:T(8,128)(2,1)}, bf16[88,2048]{1,0:T(8,128)(2,1)S(1)}, u32[]{:S(2)}) copy-start(bf16[88,2048]{1,0:T(8,128)(2,1)S(1)} %collective-permute-done.3.refs_5_) | copy-start | bytes 1081348
  75.9 0.7 copy-start.6
  112.4 7.5 %copy-start.25 = (s32[16,2]{0,1:T(2,128)S(1)}, s32[16,2]{0,1:T(2,128)}, u32[]{:S(2)}) copy-start(s32[16,2]{0,1:T(2,128)} %param.32) | copy-start | bytes 388
  113.4 15.3 %all-to-all-start.3 = ((bf16[16,3,1024]{2,1,0:T(4,128)(2,1)}), bf16[16,3,1024]{2,1,0:T(4,128)(2,1)S(1)}, u32[]{:S(2)}, u32[]{:S(2)}) async-start(bf16[16,3,1024]{2,1,0:T(4,128)(2,1)} %collect.1), calls=%async_computation.3 | async-start | bytes 262144 | tf_op jit(solution)/shard_map/all_to_all | solution.py:476
  (2 other events, 1.3 us)

commit v3 on v2

--- a/solution.py
+++ b/solution.py
@@ -16,6 +16,7 @@
 LIVE = 20
 MAIN = 1792
 TAIL = 256
+SENT = 72
 CHUNK = 80
 
 epsilon = 1e-06
@@ -87,17 +88,18 @@
         fetch(weights[k], down_ref.at[pl.ds(place * lanes, units)])
     for k, piece in enumerate(pieces):
         into = (own_ref, other_ref)[k // count]
-        fetch(piece, into.at[pl.ds((k % count) * CHUNK, CHUNK)])
+        fetch(piece, into.at[pl.ds((k % count) * CHUNK, SENT)])
     core = core_ref[0]
     here = pl.multiple_of(core * half, half)
     there = pl.multiple_of((1 - core) * half, half)
     total = x_ref.shape[0]
     step = total // 2
+    bands = [pl.ds(start, step) for start in range(0, total, step)]
     groups = LIVE // 4
     maps = [tail_maps(step, g) for g in range(groups)]
     lane = iota2((step, 128), 1)
-    for start in range(0, total, step):
-        band = pl.ds(start, step)
+    weight = []
+    for band in bands:
         tail = jnp.zeros((step, TAIL), F32)
         w = jnp.zeros((step, 128), F32)
         for g in range(groups):
@@ -105,40 +107,42 @@
             w = w + jnp.where(
                 lane == g, dot(maps[g][0], x_ref[band, groups * TAIL : groups * TAIL + 128]), 0.0
             )
-        w = jnp.sum(w, axis=1, keepdims=True)
-        full_ref[:, :MAIN] = x_ref[band, :]
-        full_ref[:, MAIN:] = tail.astype(BF16)
-        if start == 0:
-            for copy in copies[:6]:
-                copy.wait()
-            for k in range(2):
-                down_ref[k * lanes + units : (k + 1) * lanes, :] = jnp.zeros(
-                    (lanes - units, 2 * half), BF16
-                )
-        pre = dot_t(full_ref[...], up_ref[...])
-        h = w * silu(pre[:, : 2 * lanes]) * pre[:, 2 * lanes :]
-        h = jnp.where((iota2(h.shape, 1) & (lanes - 1)) < units, h, 0.0).astype(BF16)
-        acc_ref[...] = dot(h, down_ref[...])
-        if start == 0:
-            for copy in copies[6:]:
-                copy.wait()
-        pre = dot_t(full_ref[:, pl.ds(here, half)], own_ref[...])
-        pre = pre + dot_t(full_ref[:, pl.ds(there, half)], other_ref[...])
-        logit = pre[:, hidden : hidden + 1]
-        gate = pltpu.roll(pre, 2 * PAD, 1)
-        up = pltpu.roll(pre, PAD, 1)
-        unit = iota2(pre.shape, 1) % CHUNK
-        live = (unit >= 2 * PAD) & (unit < 2 * PAD + hidden)
-        scale = 0.5 / (1.0 + jnp.exp(-logit))
-        live = live & (w > 0.0)
-        hd = jnp.where(live, scale * silu(gate) * up, 0.0).astype(BF16)
-        acc_ref[:, pl.ds(here, half)] += dot(hd, own_ref[...])
-        acc_ref[:, pl.ds(there, half)] += dot(hd, other_ref[...])
-        tail = acc_ref[:, MAIN:].astype(BF16)
+        weight.append(jnp.sum(w, axis=1, keepdims=True))
+        full_ref[band, :MAIN] = x_ref[band, :]
+        full_ref[band, MAIN:] = tail.astype(BF16)
+    w = jnp.concatenate(weight, axis=0)
+    for copy in copies[:6]:
+        copy.wait()
+    for k in range(2):
+        down_ref[k * lanes + units : (k + 1) * lanes, :] = jnp.zeros(
+            (lanes - units, 2 * half), BF16
+        )
+    pre = dot_t(full_ref[...], up_ref[...])
+    h = w * silu(pre[:, : 2 * lanes]) * pre[:, 2 * lanes :]
+    h = jnp.where((iota2(h.shape, 1) & (lanes - 1)) < units, h, 0.0).astype(BF16)
+    acc_ref[...] = dot(h, down_ref[...])
+    for copy in copies[6:]:
+        copy.wait()
+    for ref in (own_ref, other_ref):
+        for k in range(count):
+            ref[k * CHUNK + SENT : (k + 1) * CHUNK, :] = jnp.zeros((CHUNK - SENT, half), BF16)
+    pre = dot_t(full_ref[:, pl.ds(here, half)], own_ref[...])
+    pre = pre + dot_t(full_ref[:, pl.ds(there, half)], other_ref[...])
+    logit = pre[:, hidden : hidden + 1]
+    gate = pltpu.roll(pre, 2 * PAD, 1)
+    up = pltpu.roll(pre, PAD, 1)
+    unit = iota2(pre.shape, 1) % CHUNK
+    live = (unit >= 2 * PAD) & (unit < 2 * PAD + hidden) & (w > 0.0)
+    scale = 0.5 / (1.0 + jnp.exp(-logit))
+    hd = jnp.where(live, scale * silu(gate) * up, 0.0).astype(BF16)
+    acc_ref[:, pl.ds(here, half)] += dot(hd, own_ref[...])
+    acc_ref[:, pl.ds(there, half)] += dot(hd, other_ref[...])
+    for band in bands:
+        tail = acc_ref[band, MAIN:].astype(BF16)
         for g in range(groups):
             part = slice(g * TAIL, (g + 1) * TAIL)
-            out_ref[band, part] = (acc_ref[:, part] + dot(maps[g][1], tail)).astype(BF16)
-        out_ref[band, groups * TAIL :] = acc_ref[:, groups * TAIL : MAIN].astype(BF16)
+            out_ref[band, part] = (acc_ref[band, part] + dot(maps[g][1], tail)).astype(BF16)
+        out_ref[band, groups * TAIL :] = acc_ref[band, groups * TAIL : MAIN].astype(BF16)
 
 
 def in_vmem(value):
@@ -158,12 +162,12 @@
         in_specs=[pl.BlockSpec(memory_space=pltpu.SMEM), vmem] + [hbm] * (6 + 2 * len(pieces)),
         out_specs=vmem,
         scratch_shapes=[
-            pltpu.VMEM((rows // 2, width), BF16),
+            pltpu.VMEM((rows, width), BF16),
             pltpu.VMEM((4 * 128, width), BF16),
             pltpu.VMEM((2 * 128, width), BF16),
             pltpu.VMEM((units, half), BF16),
             pltpu.VMEM((units, half), BF16),
-            pltpu.VMEM((rows // 2, width), F32),
+            pltpu.VMEM((rows, width), F32),
             pltpu.SemaphoreType.DMA((6 + 2 * len(pieces),)),
         ],
     )(core.reshape(1), in_vmem(x), *own, *other, *pieces, *pieces2)
@@ -247,11 +251,16 @@
 
 
 def mixer_kernel(
-    core_ref, x_ref, y_ref, gain_ref, wq, wk, wv, wo, state_ref, mix_ref, new_hbm,
-    new_ref, turn_ref, read_ref, sem,
+    core_ref, x_ref, y_ref, gain_ref, wq_hbm, wk_hbm, wv_hbm, wo_hbm, state_hbm, mix_ref, new_hbm,
+    wq, wk, wv, wo, state_ref, new_ref, turn_ref, read_ref, sem, load_sem,
 ):
     rows, half = x_ref.shape
     heads, head = state_ref.shape[1], state_ref.shape[2]
+    loads = []
+    pairs = ((wq_hbm, wq), (wk_hbm, wk), (wv_hbm, wv), (state_hbm, state_ref), (wo_hbm, wo))
+    for k, (source, into) in enumerate(pairs):
+        loads.append(pltpu.make_async_copy(source, into, load_sem.at[k]))
+        loads[-1].start()
     core = core_ref[0]
     here = pl.multiple_of(core * half, half)
     there = pl.multiple_of((1 - core) * half, half)
@@ -266,8 +275,11 @@
         both = dot(x, ref[pl.ds(here, half), :]) + dot(y, ref[pl.ds(there, half), :])
         return both.astype(BF16).astype(F32)
 
+    loads[0].wait()
     query = project(wq)
+    loads[1].wait()
     key = project(wk) * head ** (-0.5)
+    loads[2].wait()
     value = project(wv)
     turn_ref[0] = query.T
     turn_ref[1] = key.T
@@ -275,6 +287,7 @@
         jnp.where(core == 0, 1.0 - 2.0 ** (-3 - 2 * h), 1.0 - 2.0 ** (-3 - 2 * (h + heads)))
         for h in range(heads)
     ]
+    loads[3].wait()
     group = 4
     copies = []
     for s in range(rows):
@@ -296,6 +309,7 @@
         centre = jnp.mean(read, axis=1, keepdims=True)
         spread = jnp.mean(jnp.square(read - centre), axis=1, keepdims=True)
         outs.append(((read - centre) * lax.rsqrt(spread + epsilon)).astype(BF16))
+    loads[4].wait()
     mix = jnp.zeros(mix_ref.shape, F32)
     for h in range(heads):
         mix = mix + dot(outs[h], wo[h * head : (h + 1) * head, :])
@@ -308,6 +322,7 @@
     rows, half = own.shape
     heads, head = state.shape[1], state.shape[2]
     vmem = pl.BlockSpec(memory_space=pltpu.VMEM)
+    hbm = pl.BlockSpec(memory_space=pl.ANY)
     return pl.pallas_call(
         mixer_kernel,
         name="mixer",
@@ -315,13 +330,19 @@
             pltpu.VMEM((rows, 2 * half), BF16),
             jax.ShapeDtypeStruct(state.shape, F32),
         ),
-        in_specs=[pl.BlockSpec(memory_space=pltpu.SMEM)] + [vmem] * 8,
-        out_specs=(vmem, pl.BlockSpec(memory_space=pl.ANY)),
+        in_specs=[pl.BlockSpec(memory_space=pltpu.SMEM)] + [vmem] * 3 + [hbm] * 5,
+        out_specs=(vmem, hbm),
         scratch_shapes=[
+            pltpu.VMEM(wq.shape, BF16),
+            pltpu.VMEM(wk.shape, BF16),
+            pltpu.VMEM(wv.shape, BF16),
+            pltpu.VMEM(wo.shape, BF16),
+            pltpu.VMEM(state.shape, F32),
             pltpu.VMEM(state.shape, F32),
             pltpu.VMEM((2, heads * head, rows), F32),
             pltpu.VMEM((rows, heads * head), F32),
             pltpu.SemaphoreType.DMA((rows // 4,)),
+            pltpu.SemaphoreType.DMA((5,)),
         ],
     )(
         core.reshape(1), in_vmem(own), in_vmem(other), gain.reshape(1, 2 * half),
@@ -447,7 +468,7 @@
             dense_up.T,
             fill(PAD - hidden),
             dense_down,
-            fill(CHUNK - 2 * PAD - hidden),
+            fill(SENT - 2 * PAD - hidden),
         ],
         axis=0,
     )

time: 131 us -> 126 us (0.962)
  Pallas kernels: 20.1 us -> 17.9 us
  waiting for transfers between devices: 27.6 us -> 25.6 us
    ppermute x7, waiting for transfers between devices: 15.6 us -> 13.6 us  [along_z(): lax.ppermute(value, 'ep_0', [(i, (i + shift) % size) for i in range(size)])]
    pallas_call x1, Pallas kernels: 9 us -> 7.36 us  [experts_and_dense(): pl.pallas_call(lambda *refs: branch_kernel(hidden, *refs), name='branch',...]
where the time goes in v3:
time: 126 us; the launch traced here: 125 us
  blocking collectives  41.1 us (33%)
  starting transfers between devices  35.5 us (28%)
  waiting for transfers between devices  25.6 us (20%)
  Pallas kernels  17.9 us (14%)
  local copies, waits for them, and re-layouts  3.6 us (3%)
    all_to_all x1, blocking collectives, layer(): lax.all_to_all(partial.reshape(chips, ROWS, MAIN), PLANE, 0, 0, tiled=True)  26.7 us
    all_to_all x1, blocking collectives, layer(): at_plane = lax.all_to_all(slot_rows, 'ep_0', 0, 0, tiled=True)  14.4 us
    ppermute x7, waiting for transfers between devices, along_z(): lax.ppermute(value, 'ep_0', [(i, (i + shift) % size) for i in range(size)])  13.6 us
    ppermute x14, starting transfers between devices, swap(): return lax.ppermute(value, 'tp', [(0, 1), (1, 0)])  12.8 us
    ppermute x7, starting transfers between devices, along_z(): lax.ppermute(value, 'ep_0', [(i, (i + shift) % size) for i in range(size)])  9.43 us
    all_to_all x1, waiting for transfers between devices, layer(): home = lax.all_to_all(send, ('ep_0', 'tp'), 0, 0, tiled=True)  8.19 us
    pallas_call x1, Pallas kernels, experts_and_dense(): pl.pallas_call(lambda *refs: branch_kernel(hidden, *refs), name='branch',...  7.36 us
    all_to_all x1, starting transfers between devices, layer(): gathered = lax.all_to_all(copies, PLANE, 0, 0, tiled=True)  6.9 us
  transfers between devices with their start and end apart: 23, of which 8 were waited for; matrix products, arithmetic and copies ran while one was open for 1% of the time, Pallas kernels for 4%

profile of v3, /device:TPU:1, one launch (start us, length us, event | category | flops | bytes accessed | tf_op | source)
XLA Modules:
  0.0 125.2 jit_solution(3950204683606652447)
XLA Ops:
  0.6 3.3 %collective-permute-start = (bf16[16,1024]{1,0:T(8,128)(2,1)}, bf16[16,1024]{1,0:T(8,128)(2,1)S(1)}, u32[]{:S(2)}, u32[]{:S(2)}) collective-permute-start(bf16[16,1024]{1,0:T(8,128)(2,1)} %x_ref.3), channel_id=1, source_target_pairs={{0,1},{1,0},{2,3},{3,2},{4,5},{5,4},{6,7},{7,6},{8,9},{9,8},{10,11... | collective-permute-start | bytes 98312 | tf_op jit(solution)/shard_map/ppermute | solution.py:28
  3.9 0.1 collective-permute-start.2
  4.0 1.0 collective-permute-done.y_ref
  5.0 0.8 copy-done
  5.7 5.3 %mixer.1 = (bf16[16,2048]{1,0:T(8,128)(2,1)S(1)}, f32[16,2,128,128]{3,2,1,0:T(8,128)}) custom-call(s32[1]{0:T(128)} %bitcast.core_ref.refs_0_, bf16[16,1024]{1,0:T(8,128)(2,1)S(1)} %copy-done, bf16[16,1024]{1,0:T(8,128)(2,1)S(1)} %collective-permute-done.y_ref, f32[1,2048]{1,0:T(1,128)} %bitcast.29, bf16[2048,256]{1,0:T(8,128)(2,1)} %wq_hbm.1, ...), custom_call_target="tpu_custom_call" | custom-call | tf_op jit(solution)/shard_map/mixer/pallas_call | solution.py:326
  11.0 0.4 collective-permute-start.1
  11.5 0.6 pad_add_fusion.core_ref
  12.1 0.3 collective-permute-done.1.mix2_ref
  12.4 1.1 slots.1
  13.5 14.4 %all_to_all.20.x_ref = bf16[8,3,2176]{2,1,0:T(4,128)(2,1)S(1)} all-to-all(bf16[8,3,2176]{2,1,0:T(4,128)(2,1)S(1)} %get-tuple-element.7), channel_id=1, replica_groups=mesh['ep_0'=8,'ep_1'=4,'ep_2'=4,'tp'=2] {'ep_0'}, dimensions={0} | all-to-all | bytes 208896 | tf_op jit(solution)/shard_map/all_to_all | solution.py:484
  27.9 1.4 %spread.1 = bf16[16,24,1792]{2,1,0:T(8,128)(2,1)} custom-call(s32[1]{0:T(128)} %bitcast.core_ref.refs_0_, bf16[8,3,2176]{2,1,0:T(4,128)(2,1)S(1)} %all_to_all.20.x_ref), custom_call_target="tpu_custom_call" | custom-call | tf_op jit(solution)/shard_map/spread/pallas_call | solution.py:209
  29.4 0.0 copy-start.2
  29.4 0.0 copy-start.3
  29.4 6.9 %all-to-all-start.1 = ((bf16[16,24,1792]{2,1,0:T(8,128)(2,1)}), bf16[16,24,1792]{2,1,0:T(8,128)(2,1)S(1)}, u32[]{:S(2)}, u32[]{:S(2)}) async-start(bf16[16,24,1792]{2,1,0:T(8,128)(2,1)} %spread.1), calls=%async_computation.1 | async-start | bytes 2752512 | tf_op jit(solution)/shard_map/all_to_all | solution.py:491
  36.4 0.1 concatenate.3.refs_8_
  36.5 1.1 collective-permute-start.6
  37.6 1.4 %collective-permute-start.7 = (bf16[72,1024]{1,0:T(8,128)(2,1)S(1)}, bf16[72,1024]{1,0:T(8,128)(2,1)S(1)}, u32[]{:S(2)}, u32[]{:S(2)}) collective-permute-start(bf16[72,1024]{1,0:T(8,128)(2,1)S(1)} %concatenate.3.refs_8_), channel_id=1, source_target_pairs={{0,96},{32,128},{64,160},{96,192},{128,224},{160,0},{192,32},{224,... | collective-permute-start | bytes 442376 | tf_op jit(solution)/shard_map/ppermute | solution.py:33
  39.0 3.1 %collective-permute-start.8 = (bf16[72,1024]{1,0:T(8,128)(2,1)S(1)}, bf16[72,1024]{1,0:T(8,128)(2,1)S(1)}, u32[]{:S(2)}, u32[]{:S(2)}) collective-permute-start(bf16[72,1024]{1,0:T(8,128)(2,1)S(1)} %concatenate.3.refs_8_), channel_id=1, source_target_pairs={{0,160},{32,192},{64,224},{96,0},{128,32},{160,64},{192,96},{224,1... | collective-permute-start | bytes 442376 | tf_op jit(solution)/shard_map/ppermute | solution.py:33
  42.1 2.2 %collective-permute-start.9 = (bf16[72,1024]{1,0:T(8,128)(2,1)S(1)}, bf16[72,1024]{1,0:T(8,128)(2,1)S(1)}, u32[]{:S(2)}, u32[]{:S(2)}) collective-permute-start(bf16[72,1024]{1,0:T(8,128)(2,1)S(1)} %concatenate.3.refs_8_), channel_id=1, source_target_pairs={{0,64},{32,96},{64,128},{96,160},{128,192},{160,224},{192,0},{224,... | collective-permute-start | bytes 442376 | tf_op jit(solution)/shard_map/ppermute | solution.py:33
  44.3 1.4 %collective-permute-start.10 = (bf16[72,1024]{1,0:T(8,128)(2,1)S(1)}, bf16[72,1024]{1,0:T(8,128)(2,1)S(1)}, u32[]{:S(2)}, u32[]{:S(2)}) collective-permute-start(bf16[72,1024]{1,0:T(8,128)(2,1)S(1)} %concatenate.3.refs_8_), channel_id=1, source_target_pairs={{0,192},{32,224},{64,0},{96,32},{128,64},{160,96},{192,128},{224,1... | collective-permute-start | bytes 442376 | tf_op jit(solution)/shard_map/ppermute | solution.py:33
  45.7 0.3 collective-permute-start.11
  45.9 13.0 %collective-permute-done.7.refs_10_ = bf16[72,1024]{1,0:T(8,128)(2,1)S(1)} collective-permute-done((bf16[72,1024]{1,0:T(8,128)(2,1)S(1)}, bf16[72,1024]{1,0:T(8,128)(2,1)S(1)}, u32[]{:S(2)}, u32[]{:S(2)}) %collective-permute-start.7) | collective-permute-done | bytes 147488 | tf_op jit(solution)/shard_map/ppermute | solution.py:33
  59.0 4.0 %collective-permute-start.13 = (bf16[72,1024]{1,0:T(8,128)(2,1)S(1)}, bf16[72,1024]{1,0:T(8,128)(2,1)S(1)}, u32[]{:S(2)}, u32[]{:S(2)}) collective-permute-start(bf16[72,1024]{1,0:T(8,128)(2,1)S(1)} %concatenate.3.refs_8_), channel_id=1, source_target_pairs={{0,1},{1,0},{2,3},{3,2},{4,5},{5,4},{6,7},{7,6},{8,9},{9,8},{10,11... | collective-permute-start | bytes 442376 | tf_op jit(solution)/shard_map/ppermute | solution.py:28
  63.0 1.9 %collective-permute-start.14 = (bf16[72,1024]{1,0:T(8,128)(2,1)S(1)}, bf16[72,1024]{1,0:T(8,128)(2,1)S(1)}, u32[]{:S(2)}, u32[]{:S(2)}) collective-permute-start(bf16[72,1024]{1,0:T(8,128)(2,1)S(1)} %collective-permute-done.6.refs_9_), channel_id=1, source_target_pairs={{0,1},{1,0},{2,3},{3,2},{4,5},{5,4},{6,7},{7,6},{8,9},{9,8},{10,11... | collective-permute-start | bytes 442376 | tf_op jit(solution)/shard_map/ppermute | solution.py:28
  65.0 0.1 collective-permute-start.15
  65.1 0.6 collective-permute-done.11.refs_14_
  65.7 0.8 collective-permute-start.16
  66.5 0.4 collective-permute-start.3
  66.9 0.7 copy-done.14
  67.6 0.4 collective-permute-start.4
  68.0 0.2 collective-permute-start.5
  68.2 0.4 collective-permute-start.17
  68.6 0.1 collective-permute-start.18
  68.7 1.3 %collective-permute-done.17.refs_20_ = bf16[72,1024]{1,0:T(8,128)(2,1)S(1)} collective-permute-done((bf16[72,1024]{1,0:T(8,128)(2,1)S(1)}, bf16[72,1024]{1,0:T(8,128)(2,1)S(1)}, u32[]{:S(2)}, u32[]{:S(2)}) %collective-permute-start.17) | collective-permute-done | bytes 147488 | tf_op jit(solution)/shard_map/ppermute | solution.py:28
  70.0 0.4 collective-permute-start.19
  70.4 0.2 collective-permute-start.20
  70.6 0.8 collective-permute-done.19.refs_22_
  71.4 0.4 collective-permute-done.20.refs_23_
  71.8 0.2 copy-done.20
  72.0 0.4 copy-done.21
  72.4 0.7 copy-done.6
  73.2 7.4 %branch.1 = bf16[384,1792]{1,0:T(8,128)(2,1)S(1)} custom-call(s32[1]{0:T(128)} %bitcast.core_ref.refs_0_, bf16[384,1792]{1,0:T(8,128)(2,1)S(1)} %bitcast.18, bf16[88,2048]{1,0:T(8,128)(2,1)} %bitcast.21, bf16[88,2048]{1,0:T(8,128)(2,1)} %bitcast.23, bf16[88,2048]{1,0:T(8,128)(2,1)} %bitcast.25, bf16[88,2048]{1,0:T(8,128)(2,1)} %copy-done.5, ...), custom_call_target="tpu_custom_call" | custom-call | tf_op jit(solution)/shard_map/branch/pallas_call | solution.py:158
  80.6 26.7 %all_to_all.21.x_ref = bf16[16,24,1792]{2,1,0:T(8,128)(2,1)S(1)} all-to-all(bf16[16,24,1792]{2,1,0:T(8,128)(2,1)S(1)} %bitcast.19), channel_id=1, replica_groups=mesh['ep_0'=8,'ep_1'=4,'ep_2'=4,'tp'=2] {'ep_1','ep_2'}, dimensions={0} | all-to-all | bytes 2752512 | tf_op jit(solution)/shard_map/all_to_all | solution.py:495
  107.3 1.0 collect.1
  108.3 6.3 %all-to-all-start.3 = ((bf16[16,3,1024]{2,1,0:T(4,128)(2,1)}), bf16[16,3,1024]{2,1,0:T(4,128)(2,1)S(1)}, u32[]{:S(2)}, u32[]{:S(2)}) async-start(bf16[16,3,1024]{2,1,0:T(4,128)(2,1)} %collect.1), calls=%async_computation.3 | async-start | bytes 262144 | tf_op jit(solution)/shard_map/all_to_all | solution.py:497
  114.6 0.7 copy.19.routes_ref
  115.3 8.2 %all-to-all-done.3.home_ref = bf16[16,3,1024]{2,1,0:T(4,128)(2,1)S(1)} async-done(((bf16[16,3,1024]{2,1,0:T(4,128)(2,1)}), bf16[16,3,1024]{2,1,0:T(4,128)(2,1)S(1)}, u32[]{:S(2)}, u32[]{:S(2)}) %all-to-all-start.3) | async-done | bytes 98336 | tf_op jit(solution)/shard_map/all_to_all | solution.py:497
  123.5 1.6 %home.1 = bf16[16,1024]{1,0:T(8,128)(2,1)} custom-call(s32[2]{0:T(128)} %pad_add_fusion.core_ref, bf16[16,3,1024]{2,1,0:T(4,128)(2,1)S(1)} %all-to-all-done.3.home_ref, bf16[16,1024]{1,0:T(8,128)(2,1)S(1)} %get-tuple-element.8.after_ref, s32[16,2]{1,0:T(8,128)} %copy.19.routes_ref), custom_call_target="tpu_custom_call" | custom-call | tf_op jit(solution)/shard_map/home/pallas_call | solution.py:440
  (66 shorter events, 0.1 us)
Async XLA Ops:
  0.6 4.4 %collective-permute-start = (bf16[16,1024]{1,0:T(8,128)(2,1)}, bf16[16,1024]{1,0:T(8,128)(2,1)S(1)}, u32[]{:S(2)}, u32[]{:S(2)}) collective-permute-start(bf16[16,1024]{1,0:T(8,128)(2,1)} %x_ref.3), channel_id=1, source_target_pairs={{0,1},{1,0},{2,3},{3,2},{4,5},{5,4},{6,7},{7,6},{8,9},{9,8},{10,11... | collective-permute-start | bytes 98312 | tf_op jit(solution)/shard_map/ppermute | solution.py:28
  3.9 8.2 %collective-permute-start.2 = (f32[1024]{0:T(1024)}, f32[1024]{0:T(1024)S(1)}, u32[]{:S(2)}, u32[]{:S(2)}) collective-permute-start(f32[1024]{0:T(1024)} %param.24), channel_id=1, source_target_pairs={{0,1},{1,0},{2,3},{3,2},{4,5},{5,4},{6,7},{7,6},{8,9},{9,8},{10,11... | collective-permute-start | bytes 12296 | tf_op jit(solution)/shard_map/ppermute | solution.py:28
  5.0 0.8 copy-start
  11.0 1.3 %collective-permute-start.1 = (bf16[16,2048]{1,0:T(8,128)(2,1)S(1)}, bf16[16,2048]{1,0:T(8,128)(2,1)S(1)}, u32[]{:S(2)}, u32[]{:S(2)}) collective-permute-start(bf16[16,2048]{1,0:T(8,128)(2,1)S(1)} %get-tuple-element.6.mix_ref), channel_id=1, source_target_pairs={{0,1},{1,0},{2,3},{3,2},{4,5},{5,4},{6,7},{7,6},{8,9},{9,8},{10,11... | collective-permute-start | bytes 196616 | tf_op jit(solution)/shard_map/ppermute | solution.py:28
  29.4 7.0 %copy-start.26 = (bf16[1024]{0:T(1024)(128)(2,1)S(1)}, bf16[1024]{0:T(1024)(128)(2,1)}, u32[]{:S(2)}) copy-start(bf16[1024]{0:T(1024)(128)(2,1)} %param.25) | copy-start | bytes 6148
  29.4 7.0 %copy-start.22 = (bf16[1024,22]{0,1:T(8,128)(2,1)S(1)}, bf16[1024,22]{0,1:T(8,128)(2,1)}, u32[]{:S(2)}) copy-start(bf16[1024,22]{0,1:T(8,128)(2,1)} %param.26) | copy-start | bytes 135172
  29.4 7.0 %copy-start.23 = (bf16[1024,22]{0,1:T(8,128)(2,1)S(1)}, bf16[1024,22]{0,1:T(8,128)(2,1)}, u32[]{:S(2)}) copy-start(bf16[1024,22]{0,1:T(8,128)(2,1)} %param.27) | copy-start | bytes 135172
  29.4 7.0 %copy-start.24 = (bf16[22,1024]{1,0:T(8,128)(2,1)S(1)}, bf16[22,1024]{1,0:T(8,128)(2,1)}, u32[]{:S(2)}) copy-start(bf16[22,1024]{1,0:T(8,128)(2,1)} %param.28) | copy-start | bytes 135172
  29.4 37.1 %copy-start.2 = (bf16[1,2048,88]{1,2,0:T(8,128)(2,1)S(1)}, bf16[1,2048,88]{1,2,0:T(8,128)(2,1)}, u32[]{:S(2)}) copy-start(bf16[1,2048,88]{1,2,0:T(8,128)(2,1)} %param.29) | copy-start | bytes 1081348
  29.4 38.2 %copy-start.3 = (bf16[1,2048,88]{1,2,0:T(8,128)(2,1)S(1)}, bf16[1,2048,88]{1,2,0:T(8,128)(2,1)}, u32[]{:S(2)}) copy-start(bf16[1,2048,88]{1,2,0:T(8,128)(2,1)} %param.30) | copy-start | bytes 1081348
  29.4 38.6 %copy-start.4 = (bf16[1,88,2048]{2,1,0:T(8,128)(2,1)S(1)}, bf16[1,88,2048]{2,1,0:T(8,128)(2,1)}, u32[]{:S(2)}) copy-start(bf16[1,88,2048]{2,1,0:T(8,128)(2,1)} %param.31) | copy-start | bytes 1081348
  29.4 43.7 %all-to-all-start.1 = ((bf16[16,24,1792]{2,1,0:T(8,128)(2,1)}), bf16[16,24,1792]{2,1,0:T(8,128)(2,1)S(1)}, u32[]{:S(2)}, u32[]{:S(2)}) async-start(bf16[16,24,1792]{2,1,0:T(8,128)(2,1)} %spread.1), calls=%async_computation.1 | async-start | bytes 2752512 | tf_op jit(solution)/shard_map/all_to_all | solution.py:491
  36.5 36.7 %copy-start.1 = (bf16[72,1024]{1,0:T(8,128)(2,1)}, bf16[72,1024]{1,0:T(8,128)(2,1)S(1)}, u32[]{:S(2)}) copy-start(bf16[72,1024]{1,0:T(8,128)(2,1)S(1)} %concatenate.3.refs_8_) | copy-start | bytes 442372
  36.5 9.2 %collective-permute-start.6 = (bf16[72,1024]{1,0:T(8,128)(2,1)S(1)}, bf16[72,1024]{1,0:T(8,128)(2,1)S(1)}, u32[]{:S(2)}, u32[]{:S(2)}) collective-permute-start(bf16[72,1024]{1,0:T(8,128)(2,1)S(1)} %concatenate.3.refs_8_), channel_id=1, source_target_pairs={{0,128},{32,160},{64,192},{96,224},{128,0},{160,32},{192,64},{224,... | collective-permute-start | bytes 442376 | tf_op jit(solution)/shard_map/ppermute | solution.py:33
  37.6 21.3 %collective-permute-start.7 = (bf16[72,1024]{1,0:T(8,128)(2,1)S(1)}, bf16[72,1024]{1,0:T(8,128)(2,1)S(1)}, u32[]{:S(2)}, u32[]{:S(2)}) collective-permute-start(bf16[72,1024]{1,0:T(8,128)(2,1)S(1)} %concatenate.3.refs_8_), channel_id=1, source_target_pairs={{0,96},{32,128},{64,160},{96,192},{128,224},{160,0},{192,32},{224,... | collective-permute-start | bytes 442376 | tf_op jit(solution)/shard_map/ppermute | solution.py:33
  39.0 19.9 %collective-permute-start.8 = (bf16[72,1024]{1,0:T(8,128)(2,1)S(1)}, bf16[72,1024]{1,0:T(8,128)(2,1)S(1)}, u32[]{:S(2)}, u32[]{:S(2)}) collective-permute-start(bf16[72,1024]{1,0:T(8,128)(2,1)S(1)} %concatenate.3.refs_8_), channel_id=1, source_target_pairs={{0,160},{32,192},{64,224},{96,0},{128,32},{160,64},{192,96},{224,1... | collective-permute-start | bytes 442376 | tf_op jit(solution)/shard_map/ppermute | solution.py:33
  42.1 20.9 %collective-permute-start.9 = (bf16[72,1024]{1,0:T(8,128)(2,1)S(1)}, bf16[72,1024]{1,0:T(8,128)(2,1)S(1)}, u32[]{:S(2)}, u32[]{:S(2)}) collective-permute-start(bf16[72,1024]{1,0:T(8,128)(2,1)S(1)} %concatenate.3.refs_8_), channel_id=1, source_target_pairs={{0,64},{32,96},{64,128},{96,160},{128,192},{160,224},{192,0},{224,... | collective-permute-start | bytes 442376 | tf_op jit(solution)/shard_map/ppermute | solution.py:33
  44.3 20.7 %collective-permute-start.10 = (bf16[72,1024]{1,0:T(8,128)(2,1)S(1)}, bf16[72,1024]{1,0:T(8,128)(2,1)S(1)}, u32[]{:S(2)}, u32[]{:S(2)}) collective-permute-start(bf16[72,1024]{1,0:T(8,128)(2,1)S(1)} %concatenate.3.refs_8_), channel_id=1, source_target_pairs={{0,192},{32,224},{64,0},{96,32},{128,64},{160,96},{192,128},{224,1... | collective-permute-start | bytes 442376 | tf_op jit(solution)/shard_map/ppermute | solution.py:33
  45.7 27.5 %copy-start.7 = (bf16[72,1024]{1,0:T(8,128)(2,1)}, bf16[72,1024]{1,0:T(8,128)(2,1)S(1)}, u32[]{:S(2)}) copy-start(bf16[72,1024]{1,0:T(8,128)(2,1)S(1)} %collective-permute-done.6.refs_9_) | copy-start | bytes 442372
  45.7 20.0 %collective-permute-start.11 = (bf16[72,1024]{1,0:T(8,128)(2,1)S(1)}, bf16[72,1024]{1,0:T(8,128)(2,1)S(1)}, u32[]{:S(2)}, u32[]{:S(2)}) collective-permute-start(bf16[72,1024]{1,0:T(8,128)(2,1)S(1)} %concatenate.3.refs_8_), channel_id=1, source_target_pairs={{0,32},{32,64},{64,96},{96,128},{128,160},{160,192},{192,224},{224... | collective-permute-start | bytes 442376 | tf_op jit(solution)/shard_map/ppermute | solution.py:33
  59.0 14.2 %copy-start.8 = (bf16[72,1024]{1,0:T(8,128)(2,1)}, bf16[72,1024]{1,0:T(8,128)(2,1)S(1)}, u32[]{:S(2)}) copy-start(bf16[72,1024]{1,0:T(8,128)(2,1)S(1)} %collective-permute-done.7.refs_10_) | copy-start | bytes 442372
  59.0 7.6 %collective-permute-start.12 = (bf16[72,1024]{1,0:T(8,128)(2,1)S(1)}, bf16[72,1024]{1,0:T(8,128)(2,1)S(1)}, u32[]{:S(2)}, u32[]{:S(2)}) collective-permute-start(bf16[72,1024]{1,0:T(8,128)(2,1)S(1)} %concatenate.3.refs_8_), channel_id=1, source_target_pairs={{0,224},{32,0},{64,32},{96,64},{128,96},{160,128},{192,160},{224,1... | collective-permute-start | bytes 442376 | tf_op jit(solution)/shard_map/ppermute | solution.py:33
  59.0 14.2 %copy-start.9 = (bf16[72,1024]{1,0:T(8,128)(2,1)}, bf16[72,1024]{1,0:T(8,128)(2,1)S(1)}, u32[]{:S(2)}) copy-start(bf16[72,1024]{1,0:T(8,128)(2,1)S(1)} %collective-permute-done.8.refs_11_) | copy-start | bytes 442372
  59.0 7.9 %collective-permute-start.13 = (bf16[72,1024]{1,0:T(8,128)(2,1)S(1)}, bf16[72,1024]{1,0:T(8,128)(2,1)S(1)}, u32[]{:S(2)}, u32[]{:S(2)}) collective-permute-start(bf16[72,1024]{1,0:T(8,128)(2,1)S(1)} %concatenate.3.refs_8_), channel_id=1, source_target_pairs={{0,1},{1,0},{2,3},{3,2},{4,5},{5,4},{6,7},{7,6},{8,9},{9,8},{10,11... | collective-permute-start | bytes 442376 | tf_op jit(solution)/shard_map/ppermute | solution.py:28
  63.0 8.7 %copy-start.10 = (bf16[72,1024]{1,0:T(8,128)(2,1)}, bf16[72,1024]{1,0:T(8,128)(2,1)S(1)}, u32[]{:S(2)}) copy-start(bf16[72,1024]{1,0:T(8,128)(2,1)S(1)} %collective-permute-done.9.refs_12_) | copy-start | bytes 442372
  63.0 4.9 %collective-permute-start.14 = (bf16[72,1024]{1,0:T(8,128)(2,1)S(1)}, bf16[72,1024]{1,0:T(8,128)(2,1)S(1)}, u32[]{:S(2)}, u32[]{:S(2)}) collective-permute-start(bf16[72,1024]{1,0:T(8,128)(2,1)S(1)} %collective-permute-done.6.refs_9_), channel_id=1, source_target_pairs={{0,1},{1,0},{2,3},{3,2},{4,5},{5,4},{6,7},{7,6},{8,9},{9,8},{10,11... | collective-permute-start | bytes 442376 | tf_op jit(solution)/shard_map/ppermute | solution.py:28
  65.0 6.8 %copy-start.11 = (bf16[72,1024]{1,0:T(8,128)(2,1)}, bf16[72,1024]{1,0:T(8,128)(2,1)S(1)}, u32[]{:S(2)}) copy-start(bf16[72,1024]{1,0:T(8,128)(2,1)S(1)} %collective-permute-done.10.refs_13_) | copy-start | bytes 442372
  65.0 3.2 %collective-permute-start.15 = (bf16[72,1024]{1,0:T(8,128)(2,1)S(1)}, bf16[72,1024]{1,0:T(8,128)(2,1)S(1)}, u32[]{:S(2)}, u32[]{:S(2)}) collective-permute-start(bf16[72,1024]{1,0:T(8,128)(2,1)S(1)} %collective-permute-done.7.refs_10_), channel_id=1, source_target_pairs={{0,1},{1,0},{2,3},{3,2},{4,5},{5,4},{6,7},{7,6},{8,9},{9,8},{10,11... | collective-permute-start | bytes 442376 | tf_op jit(solution)/shard_map/ppermute | solution.py:28
  65.7 6.1 %copy-start.12 = (bf16[72,1024]{1,0:T(8,128)(2,1)}, bf16[72,1024]{1,0:T(8,128)(2,1)S(1)}, u32[]{:S(2)}) copy-start(bf16[72,1024]{1,0:T(8,128)(2,1)S(1)} %collective-permute-done.11.refs_14_) | copy-start | bytes 442372
  65.7 2.9 %collective-permute-start.16 = (bf16[72,1024]{1,0:T(8,128)(2,1)S(1)}, bf16[72,1024]{1,0:T(8,128)(2,1)S(1)}, u32[]{:S(2)}, u32[]{:S(2)}) collective-permute-start(bf16[72,1024]{1,0:T(8,128)(2,1)S(1)} %collective-permute-done.8.refs_11_), channel_id=1, source_target_pairs={{0,1},{1,0},{2,3},{3,2},{4,5},{5,4},{6,7},{7,6},{8,9},{9,8},{10,11... | collective-permute-start | bytes 442376 | tf_op jit(solution)/shard_map/ppermute | solution.py:28
  66.5 5.3 %copy-start.13 = (bf16[72,1024]{1,0:T(8,128)(2,1)}, bf16[72,1024]{1,0:T(8,128)(2,1)S(1)}, u32[]{:S(2)}) copy-start(bf16[72,1024]{1,0:T(8,128)(2,1)S(1)} %collective-permute-done.12.refs_15_) | copy-start | bytes 442372
  66.5 5.2 %collective-permute-start.3 = (bf16[88,2048]{1,0:T(8,128)(2,1)S(1)}, bf16[88,2048]{1,0:T(8,128)(2,1)S(1)}, u32[]{:S(2)}, u32[]{:S(2)}) collective-permute-start(bf16[88,2048]{1,0:T(8,128)(2,1)S(1)} %bitcast.22), channel_id=1, source_target_pairs={{0,1},{1,0},{2,3},{3,2},{4,5},{5,4},{6,7},{7,6},{8,9},{9,8},{10,11... | collective-permute-start | bytes 1081352 | tf_op jit(solution)/shard_map/ppermute | solution.py:28
  67.6 4.2 %collective-permute-start.4 = (bf16[88,2048]{1,0:T(8,128)(2,1)S(1)}, bf16[88,2048]{1,0:T(8,128)(2,1)S(1)}, u32[]{:S(2)}, u32[]{:S(2)}) collective-permute-start(bf16[88,2048]{1,0:T(8,128)(2,1)S(1)} %bitcast.24), channel_id=1, source_target_pairs={{0,1},{1,0},{2,3},{3,2},{4,5},{5,4},{6,7},{7,6},{8,9},{9,8},{10,11... | collective-permute-start | bytes 1081352 | tf_op jit(solution)/shard_map/ppermute | solution.py:28
  68.0 3.8 %copy-start.15 = (bf16[72,1024]{1,0:T(8,128)(2,1)}, bf16[72,1024]{1,0:T(8,128)(2,1)S(1)}, u32[]{:S(2)}) copy-start(bf16[72,1024]{1,0:T(8,128)(2,1)S(1)} %collective-permute-done.14.refs_17_) | copy-start | bytes 442372
  68.0 5.2 %collective-permute-start.5 = (bf16[88,2048]{1,0:T(8,128)(2,1)S(1)}, bf16[88,2048]{1,0:T(8,128)(2,1)}, u32[]{:S(2)}, u32[]{:S(2)}) collective-permute-start(bf16[88,2048]{1,0:T(8,128)(2,1)S(1)} %bitcast.26), channel_id=1, source_target_pairs={{0,1},{1,0},{2,3},{3,2},{4,5},{5,4},{6,7},{7,6},{8,9},{9,8},{10,11... | collective-permute-start | bytes 1081352 | tf_op jit(solution)/shard_map/ppermute | solution.py:28
  68.2 3.6 %copy-start.16 = (bf16[72,1024]{1,0:T(8,128)(2,1)}, bf16[72,1024]{1,0:T(8,128)(2,1)S(1)}, u32[]{:S(2)}) copy-start(bf16[72,1024]{1,0:T(8,128)(2,1)S(1)} %collective-permute-done.15.refs_18_) | copy-start | bytes 442372
  68.2 1.8 %collective-permute-start.17 = (bf16[72,1024]{1,0:T(8,128)(2,1)S(1)}, bf16[72,1024]{1,0:T(8,128)(2,1)S(1)}, u32[]{:S(2)}, u32[]{:S(2)}) collective-permute-start(bf16[72,1024]{1,0:T(8,128)(2,1)S(1)} %collective-permute-done.9.refs_12_), channel_id=1, source_target_pairs={{0,1},{1,0},{2,3},{3,2},{4,5},{5,4},{6,7},{7,6},{8,9},{9,8},{10,11... | collective-permute-start | bytes 442376 | tf_op jit(solution)/shard_map/ppermute | solution.py:28
  68.6 3.2 %copy-start.17 = (bf16[72,1024]{1,0:T(8,128)(2,1)}, bf16[72,1024]{1,0:T(8,128)(2,1)S(1)}, u32[]{:S(2)}) copy-start(bf16[72,1024]{1,0:T(8,128)(2,1)S(1)} %collective-permute-done.16.refs_19_) | copy-start | bytes 442372
  68.6 1.8 %collective-permute-start.18 = (bf16[72,1024]{1,0:T(8,128)(2,1)S(1)}, bf16[72,1024]{1,0:T(8,128)(2,1)S(1)}, u32[]{:S(2)}, u32[]{:S(2)}) collective-permute-start(bf16[72,1024]{1,0:T(8,128)(2,1)S(1)} %collective-permute-done.10.refs_13_), channel_id=1, source_target_pairs={{0,1},{1,0},{2,3},{3,2},{4,5},{5,4},{6,7},{7,6},{8,9},{9,8},{10,11... | collective-permute-start | bytes 442376 | tf_op jit(solution)/shard_map/ppermute | solution.py:28
  70.0 1.8 %copy-start.18 = (bf16[72,1024]{1,0:T(8,128)(2,1)}, bf16[72,1024]{1,0:T(8,128)(2,1)S(1)}, u32[]{:S(2)}) copy-start(bf16[72,1024]{1,0:T(8,128)(2,1)S(1)} %collective-permute-done.17.refs_20_) | copy-start | bytes 442372
  70.0 1.4 %collective-permute-start.19 = (bf16[72,1024]{1,0:T(8,128)(2,1)S(1)}, bf16[72,1024]{1,0:T(8,128)(2,1)S(1)}, u32[]{:S(2)}, u32[]{:S(2)}) collective-permute-start(bf16[72,1024]{1,0:T(8,128)(2,1)S(1)} %collective-permute-done.11.refs_14_), channel_id=1, source_target_pairs={{0,1},{1,0},{2,3},{3,2},{4,5},{5,4},{6,7},{7,6},{8,9},{9,8},{10,11... | collective-permute-start | bytes 442376 | tf_op jit(solution)/shard_map/ppermute | solution.py:28
  70.4 1.5 %copy-start.19 = (bf16[72,1024]{1,0:T(8,128)(2,1)}, bf16[72,1024]{1,0:T(8,128)(2,1)S(1)}, u32[]{:S(2)}) copy-start(bf16[72,1024]{1,0:T(8,128)(2,1)S(1)} %collective-permute-done.18.refs_21_) | copy-start | bytes 442372
  70.4 1.4 %collective-permute-start.20 = (bf16[72,1024]{1,0:T(8,128)(2,1)S(1)}, bf16[72,1024]{1,0:T(8,128)(2,1)S(1)}, u32[]{:S(2)}, u32[]{:S(2)}) collective-permute-start(bf16[72,1024]{1,0:T(8,128)(2,1)S(1)} %collective-permute-done.12.refs_15_), channel_id=1, source_target_pairs={{0,1},{1,0},{2,3},{3,2},{4,5},{5,4},{6,7},{7,6},{8,9},{9,8},{10,11... | collective-permute-start | bytes 442376 | tf_op jit(solution)/shard_map/ppermute | solution.py:28
  71.7 0.7 copy-start.21
  71.8 1.4 %copy-start.5 = (bf16[88,2048]{1,0:T(8,128)(2,1)}, bf16[88,2048]{1,0:T(8,128)(2,1)S(1)}, u32[]{:S(2)}) copy-start(bf16[88,2048]{1,0:T(8,128)(2,1)S(1)} %collective-permute-done.3.refs_5_) | copy-start | bytes 1081348
  72.4 0.7 copy-start.6
  107.3 7.4 %copy-start.25 = (s32[16,2]{0,1:T(2,128)S(1)}, s32[16,2]{0,1:T(2,128)}, u32[]{:S(2)}) copy-start(s32[16,2]{0,1:T(2,128)} %param.32) | copy-start | bytes 388
  108.3 15.2 %all-to-all-start.3 = ((bf16[16,3,1024]{2,1,0:T(4,128)(2,1)}), bf16[16,3,1024]{2,1,0:T(4,128)(2,1)S(1)}, u32[]{:S(2)}, u32[]{:S(2)}) async-start(bf16[16,3,1024]{2,1,0:T(4,128)(2,1)} %collect.1), calls=%async_computation.3 | async-start | bytes 262144 | tf_op jit(solution)/shard_map/all_to_all | solution.py:497
  (2 other events, 1.3 us)

commit v4 on v3

--- a/solution.py
+++ b/solution.py
@@ -251,19 +251,20 @@
 
 
 def mixer_kernel(
-    core_ref, x_ref, y_ref, gain_ref, wq_hbm, wk_hbm, wv_hbm, wo_hbm, state_hbm, mix_ref, new_hbm,
-    wq, wk, wv, wo, state_ref, new_ref, turn_ref, read_ref, sem, load_sem,
+    core_ref, x_hbm, y_ref, gain_ref, wq_hbm, wk_hbm, wv_hbm, wo_hbm, state_hbm, mix_ref, new_hbm,
+    x_ref, wq, wk, wv, wo, state_ref, new_ref, turn_ref, read_ref, sem, load_sem,
 ):
     rows, half = x_ref.shape
     heads, head = state_ref.shape[1], state_ref.shape[2]
     loads = []
-    pairs = ((wq_hbm, wq), (wk_hbm, wk), (wv_hbm, wv), (state_hbm, state_ref), (wo_hbm, wo))
+    pairs = ((x_hbm, x_ref), (wq_hbm, wq), (wk_hbm, wk), (wv_hbm, wv), (state_hbm, state_ref), (wo_hbm, wo))
     for k, (source, into) in enumerate(pairs):
         loads.append(pltpu.make_async_copy(source, into, load_sem.at[k]))
         loads[-1].start()
     core = core_ref[0]
     here = pl.multiple_of(core * half, half)
     there = pl.multiple_of((1 - core) * half, half)
+    loads[0].wait()
     x = x_ref[...].astype(F32)
     y = y_ref[...].astype(F32)
     total = jnp.sum(x * x, axis=1, keepdims=True) + jnp.sum(y * y, axis=1, keepdims=True)
@@ -275,11 +276,11 @@
         both = dot(x, ref[pl.ds(here, half), :]) + dot(y, ref[pl.ds(there, half), :])
         return both.astype(BF16).astype(F32)
 
-    loads[0].wait()
+    loads[1].wait()
     query = project(wq)
-    loads[1].wait()
+    loads[2].wait()
     key = project(wk) * head ** (-0.5)
-    loads[2].wait()
+    loads[3].wait()
     value = project(wv)
     turn_ref[0] = query.T
     turn_ref[1] = key.T
@@ -287,7 +288,7 @@
         jnp.where(core == 0, 1.0 - 2.0 ** (-3 - 2 * h), 1.0 - 2.0 ** (-3 - 2 * (h + heads)))
         for h in range(heads)
     ]
-    loads[3].wait()
+    loads[4].wait()
     group = 4
     copies = []
     for s in range(rows):
@@ -309,7 +310,7 @@
         centre = jnp.mean(read, axis=1, keepdims=True)
         spread = jnp.mean(jnp.square(read - centre), axis=1, keepdims=True)
         outs.append(((read - centre) * lax.rsqrt(spread + epsilon)).astype(BF16))
-    loads[4].wait()
+    loads[5].wait()
     mix = jnp.zeros(mix_ref.shape, F32)
     for h in range(heads):
         mix = mix + dot(outs[h], wo[h * head : (h + 1) * head, :])
@@ -330,9 +331,10 @@
             pltpu.VMEM((rows, 2 * half), BF16),
             jax.ShapeDtypeStruct(state.shape, F32),
         ),
-        in_specs=[pl.BlockSpec(memory_space=pltpu.SMEM)] + [vmem] * 3 + [hbm] * 5,
+        in_specs=[pl.BlockSpec(memory_space=pltpu.SMEM), hbm, vmem, vmem] + [hbm] * 5,
         out_specs=(vmem, hbm),
         scratch_shapes=[
+            pltpu.VMEM(own.shape, BF16),
             pltpu.VMEM(wq.shape, BF16),
             pltpu.VMEM(wk.shape, BF16),
             pltpu.VMEM(wv.shape, BF16),
@@ -342,10 +344,10 @@
             pltpu.VMEM((2, heads * head, rows), F32),
             pltpu.VMEM((rows, heads * head), F32),
             pltpu.SemaphoreType.DMA((rows // 4,)),
-            pltpu.SemaphoreType.DMA((5,)),
+            pltpu.SemaphoreType.DMA((6,)),
         ],
     )(
-        core.reshape(1), in_vmem(own), in_vmem(other), gain.reshape(1, 2 * half),
+        core.reshape(1), own, in_vmem(other), gain.reshape(1, 2 * half),
         wq, wk, wv, wo, state,
     )
 
@@ -355,11 +357,11 @@
 
 
 def slots_kernel(
-    core_ref, x_ref, y_ref, mix_ref, mix2_ref, gain_ref, gain2_ref, routes_ref, weights_ref,
+    core_ref, z_ref, x_ref, y_ref, mix_ref, mix2_ref, gain_ref, gain2_ref, routes_ref, weights_ref,
     slot_ref, after_ref,
 ):
     rows, half = x_ref.shape
-    core, odd = core_ref[0], core_ref[1]
+    core, odd = core_ref[0], z_ref[0] & 1
     here = pl.multiple_of(core * half, half)
     there = pl.multiple_of((1 - core) * half, half)
 
@@ -408,16 +410,16 @@
             pltpu.VMEM((EXPERTS, SLOTS, 2 * half + 128), BF16),
             pltpu.VMEM((rows, half), BF16),
         ),
-        in_specs=[pl.BlockSpec(memory_space=pltpu.SMEM)] + [vmem] * 8,
+        in_specs=[pl.BlockSpec(memory_space=pltpu.SMEM)] * 2 + [vmem] * 8,
         out_specs=(vmem, vmem),
     )(
-        place, in_vmem(own), in_vmem(other), in_vmem(mix), in_vmem(mix2),
+        place[0].reshape(1), place[1].reshape(1), in_vmem(own), in_vmem(other), in_vmem(mix), in_vmem(mix2),
         gain.reshape(1, half), in_vmem(gain2.reshape(1, half)), routes.T, route_w.T,
     )
 
 
-def home_kernel(core_ref, home_ref, after_ref, routes_ref, out_ref, rows_ref):
-    odd = core_ref[1]
+def home_kernel(z_ref, home_ref, after_ref, routes_ref, out_ref, rows_ref):
+    odd = z_ref[0] & 1
     rows = after_ref.shape[0]
     count = home_ref.shape[0]
     for k in range(count):
@@ -444,7 +446,7 @@
         in_specs=[pl.BlockSpec(memory_space=pltpu.SMEM)] + [vmem] * 3,
         out_specs=vmem,
         scratch_shapes=[pltpu.VMEM((home.shape[0] * SLOTS, home.shape[2]), F32)],
-    )(place, in_vmem(home), in_vmem(after), routes)
+    )(place[1].reshape(1), in_vmem(home), in_vmem(after), routes)
 
 
 def layer(
@@ -477,14 +479,15 @@
 
     mix, new_state = mixer(core, tokens, other_x, norm_mix, w_query, w_key, w_value, w_out, state)
     mix2 = swap(mix)
-    place = jnp.stack([core, lax.axis_index("ep_0") % 2])
+    place = (core, lax.axis_index("ep_0"))
     slot_rows, after = to_slots(
         place, tokens, other_x, mix, mix2, norm_ffn, other_gain, routes, route_w
     )
     at_plane = lax.all_to_all(slot_rows, "ep_0", 0, 0, tiled=True)
     pieces = [packed]
-    for shift in (4, 3, 5, 2, 6, 1, 7):
+    for shift in (3, -3, -2, 2, 1, -1):
         pieces.append(along_z(packed, shift))
+    pieces.append(along_z(pieces[2], -1))
     pieces2 = [swap(piece) for piece in pieces]
     chips = lax.axis_size(PLANE)
     copies = spread(core, at_plane, chips)

time: 126 us -> 120 us (0.952)
  waiting for transfers between devices: 25.6 us -> 20.5 us
    ppermute x7, waiting for transfers between devices: 13.6 us -> 8.24 us  [along_z(): lax.ppermute(value, 'ep_0', [(i, (i + shift) % size) for i in range(size)])]
    ppermute x14, starting transfers between devices: 12.8 us -> 14.4 us  [swap(): return lax.ppermute(value, 'tp', [(0, 1), (1, 0)])]
    unnamed x55 -> x57, local copies, waits for them, and re-layouts: 3.5 us -> 3.54 us
  transfers between devices with their start and end apart: 23 -> 23, of which waited for: 8 -> 8; matrix products, arithmetic and copies ran while one was open for 1% -> 1% of each run, Pallas kernels for 4% -> 0%
where the time goes in v4:
time: 120 us
  blocking collectives  41.5 us (35%)
  starting transfers between devices  35.4 us (30%)
  waiting for transfers between devices  20.5 us (17%)
  Pallas kernels  17.8 us (15%)
  local copies, waits for them, and re-layouts  3.64 us (3%)
    all_to_all x1, blocking collectives, layer(): lax.all_to_all(partial.reshape(chips, ROWS, MAIN), PLANE, 0, 0, tiled=True)  26.7 us
    all_to_all x1, blocking collectives, layer(): at_plane = lax.all_to_all(slot_rows, 'ep_0', 0, 0, tiled=True)  14.8 us
    ppermute x14, starting transfers between devices, swap(): return lax.ppermute(value, 'tp', [(0, 1), (1, 0)])  14.4 us
    ppermute x7, starting transfers between devices, along_z(): lax.ppermute(value, 'ep_0', [(i, (i + shift) % size) for i in range(size)])  8.29 us
    ppermute x7, waiting for transfers between devices, along_z(): lax.ppermute(value, 'ep_0', [(i, (i + shift) % size) for i in range(size)])  8.24 us
    all_to_all x1, waiting for transfers between devices, layer(): home = lax.all_to_all(send, ('ep_0', 'tp'), 0, 0, tiled=True)  8.2 us
    pallas_call x1, Pallas kernels, experts_and_dense(): pl.pallas_call(lambda *refs: branch_kernel(hidden, *refs), name='branch',...  7.36 us
    all_to_all x1, starting transfers between devices, layer(): gathered = lax.all_to_all(copies, PLANE, 0, 0, tiled=True)  6.9 us
  transfers between devices with their start and end apart: 23, of which 8 were waited for; matrix products, arithmetic and copies ran while one was open for 1% of the time, Pallas kernels for 0%

profile of v4, /device:TPU:1, one launch (start us, length us, event | category | flops | bytes accessed | tf_op | source)
XLA Modules:
  0.0 119.8 jit_solution(1446134848966257996)
XLA Ops:
  0.6 3.3 %collective-permute-start = (bf16[16,1024]{1,0:T(8,128)(2,1)}, bf16[16,1024]{1,0:T(8,128)(2,1)S(1)}, u32[]{:S(2)}, u32[]{:S(2)}) collective-permute-start(bf16[16,1024]{1,0:T(8,128)(2,1)} %x_ref.1), channel_id=1, source_target_pairs={{0,1},{1,0},{2,3},{3,2},{4,5},{5,4},{6,7},{7,6},{8,9},{9,8},{10,11... | collective-permute-start | bytes 98312 | tf_op jit(solution)/shard_map/ppermute | solution.py:28
  3.9 1.1 collective-permute-done.y_ref
  5.0 5.3 %mixer.1 = (bf16[16,2048]{1,0:T(8,128)(2,1)S(1)}, f32[16,2,128,128]{3,2,1,0:T(8,128)}) custom-call(s32[1]{0:T(128)} %bitcast.1.core_ref.refs_0_, bf16[16,1024]{1,0:T(8,128)(2,1)} %x_ref.1, bf16[16,1024]{1,0:T(8,128)(2,1)S(1)} %collective-permute-done.y_ref, f32[1,2048]{1,0:T(1,128)} %bitcast.29, bf16[2048,256]{1,0:T(8,128)(2,1)} %wq_hbm.1, ...), custom_call_target="tpu_custom_call" | custom-call | tf_op jit(solution)/shard_map/mixer/pallas_call | solution.py:327
  10.3 0.4 collective-permute-start.1
  10.8 0.2 collective-permute-start.2
  10.9 1.0 collective-permute-done.2
  11.9 1.0 slots.1
  13.0 14.8 %all_to_all.20.x_ref = bf16[8,3,2176]{2,1,0:T(4,128)(2,1)S(1)} all-to-all(bf16[8,3,2176]{2,1,0:T(4,128)(2,1)S(1)} %get-tuple-element.7), channel_id=1, replica_groups=mesh['ep_0'=8,'ep_1'=4,'ep_2'=4,'tp'=2] {'ep_0'}, dimensions={0} | all-to-all | bytes 208896 | tf_op jit(solution)/shard_map/all_to_all | solution.py:486
  27.8 1.4 %spread.1 = bf16[16,24,1792]{2,1,0:T(8,128)(2,1)} custom-call(s32[1]{0:T(128)} %bitcast.1.core_ref.refs_0_, bf16[8,3,2176]{2,1,0:T(4,128)(2,1)S(1)} %all_to_all.20.x_ref), custom_call_target="tpu_custom_call" | custom-call | tf_op jit(solution)/shard_map/spread/pallas_call | solution.py:209
  29.2 0.0 copy-start.2
  29.2 0.0 copy-start.3
  29.2 0.0 copy-start.4
  29.2 6.9 %all-to-all-start.1 = ((bf16[16,24,1792]{2,1,0:T(8,128)(2,1)}), bf16[16,24,1792]{2,1,0:T(8,128)(2,1)S(1)}, u32[]{:S(2)}, u32[]{:S(2)}) async-start(bf16[16,24,1792]{2,1,0:T(8,128)(2,1)} %spread.1), calls=%async_computation.1 | async-start | bytes 2752512 | tf_op jit(solution)/shard_map/all_to_all | solution.py:494
  36.2 0.1 concatenate.3.refs_8_
  36.3 0.4 collective-permute-start.7
  36.7 3.0 %collective-permute-start.6 = (bf16[72,1024]{1,0:T(8,128)(2,1)S(1)}, bf16[72,1024]{1,0:T(8,128)(2,1)S(1)}, u32[]{:S(2)}, u32[]{:S(2)}) collective-permute-start(bf16[72,1024]{1,0:T(8,128)(2,1)S(1)} %concatenate.3.refs_8_), channel_id=1, source_target_pairs={{0,96},{32,128},{64,160},{96,192},{128,224},{160,0},{192,32},{224,... | collective-permute-start | bytes 442376 | tf_op jit(solution)/shard_map/ppermute | solution.py:33
  39.6 2.0 %collective-permute-start.8 = (bf16[72,1024]{1,0:T(8,128)(2,1)S(1)}, bf16[72,1024]{1,0:T(8,128)(2,1)S(1)}, u32[]{:S(2)}, u32[]{:S(2)}) collective-permute-start(bf16[72,1024]{1,0:T(8,128)(2,1)S(1)} %concatenate.3.refs_8_), channel_id=1, source_target_pairs={{0,192},{32,224},{64,0},{96,32},{128,64},{160,96},{192,128},{224,1... | collective-permute-start | bytes 442376 | tf_op jit(solution)/shard_map/ppermute | solution.py:33
  41.7 0.3 collective-permute-start.9
  42.0 1.2 %collective-permute-start.10 = (bf16[72,1024]{1,0:T(8,128)(2,1)S(1)}, bf16[72,1024]{1,0:T(8,128)(2,1)S(1)}, u32[]{:S(2)}, u32[]{:S(2)}) collective-permute-start(bf16[72,1024]{1,0:T(8,128)(2,1)S(1)} %concatenate.3.refs_8_), channel_id=1, source_target_pairs={{0,32},{32,64},{64,96},{96,128},{128,160},{160,192},{192,224},{224... | collective-permute-start | bytes 442376 | tf_op jit(solution)/shard_map/ppermute | solution.py:33
  43.2 5.8 %collective-permute-done.7.refs_10_ = bf16[72,1024]{1,0:T(8,128)(2,1)S(1)} collective-permute-done((bf16[72,1024]{1,0:T(8,128)(2,1)S(1)}, bf16[72,1024]{1,0:T(8,128)(2,1)S(1)}, u32[]{:S(2)}, u32[]{:S(2)}) %collective-permute-start.7) | collective-permute-done | bytes 147488 | tf_op jit(solution)/shard_map/ppermute | solution.py:33
  49.0 5.6 %collective-permute-start.13 = (bf16[72,1024]{1,0:T(8,128)(2,1)S(1)}, bf16[72,1024]{1,0:T(8,128)(2,1)S(1)}, u32[]{:S(2)}, u32[]{:S(2)}) collective-permute-start(bf16[72,1024]{1,0:T(8,128)(2,1)S(1)} %concatenate.3.refs_8_), channel_id=1, source_target_pairs={{0,1},{1,0},{2,3},{3,2},{4,5},{5,4},{6,7},{7,6},{8,9},{9,8},{10,11... | collective-permute-start | bytes 442376 | tf_op jit(solution)/shard_map/ppermute | solution.py:28
  54.6 1.4 %collective-permute-start.12 = (bf16[72,1024]{1,0:T(8,128)(2,1)S(1)}, bf16[72,1024]{1,0:T(8,128)(2,1)S(1)}, u32[]{:S(2)}, u32[]{:S(2)}) collective-permute-start(bf16[72,1024]{1,0:T(8,128)(2,1)S(1)} %collective-permute-done.7.refs_10_), channel_id=1, source_target_pairs={{0,224},{32,0},{64,32},{96,64},{128,96},{160,128},{192,160},{224,1... | collective-permute-start | bytes 442376 | tf_op jit(solution)/shard_map/ppermute | solution.py:33
  56.0 1.1 collective-permute-done.9.refs_12_
  57.1 0.9 collective-permute-start.15
  58.0 1.4 %collective-permute-done.10.refs_13_ = bf16[72,1024]{1,0:T(8,128)(2,1)S(1)} collective-permute-done((bf16[72,1024]{1,0:T(8,128)(2,1)S(1)}, bf16[72,1024]{1,0:T(8,128)(2,1)S(1)}, u32[]{:S(2)}, u32[]{:S(2)}) %collective-permute-start.10) | collective-permute-done | bytes 147488 | tf_op jit(solution)/shard_map/ppermute | solution.py:33
  59.4 1.9 %collective-permute-start.14 = (bf16[72,1024]{1,0:T(8,128)(2,1)S(1)}, bf16[72,1024]{1,0:T(8,128)(2,1)S(1)}, u32[]{:S(2)}, u32[]{:S(2)}) collective-permute-start(bf16[72,1024]{1,0:T(8,128)(2,1)S(1)} %collective-permute-done.6.refs_9_), channel_id=1, source_target_pairs={{0,1},{1,0},{2,3},{3,2},{4,5},{5,4},{6,7},{7,6},{8,9},{9,8},{10,11... | collective-permute-start | bytes 442376 | tf_op jit(solution)/shard_map/ppermute | solution.py:28
  61.2 0.3 collective-permute-start.16
  61.5 0.7 copy-done.14
  62.2 0.2 collective-permute-start.3
  62.4 0.4 collective-permute-start.4
  62.8 0.7 copy-done.16
  63.5 0.2 collective-permute-start.5
  63.7 0.3 collective-permute-start.17
  64.0 0.2 collective-permute-start.18
  64.2 1.1 collective-permute-done.17.refs_20_
  65.3 0.2 collective-permute-start.19
  65.6 0.3 collective-permute-start.20
  65.9 0.9 collective-permute-done.19.refs_22_
  66.8 0.5 copy-done.21
  67.4 0.2 copy-done.6
  67.5 0.8 copy-done.7
  68.3 7.4 %branch.1 = bf16[384,1792]{1,0:T(8,128)(2,1)S(1)} custom-call(s32[1]{0:T(128)} %bitcast.1.core_ref.refs_0_, bf16[384,1792]{1,0:T(8,128)(2,1)S(1)} %bitcast.18, bf16[88,2048]{1,0:T(8,128)(2,1)} %bitcast.21, bf16[88,2048]{1,0:T(8,128)(2,1)} %bitcast.23, bf16[88,2048]{1,0:T(8,128)(2,1)} %bitcast.25, bf16[88,2048]{1,0:T(8,128)(2,1)} %copy-done.5, ...), custom_call_target="tpu_custom_call" | custom-call | tf_op jit(solution)/shard_map/branch/pallas_call | solution.py:158
  75.7 26.7 %all_to_all.21.x_ref = bf16[16,24,1792]{2,1,0:T(8,128)(2,1)S(1)} all-to-all(bf16[16,24,1792]{2,1,0:T(8,128)(2,1)S(1)} %bitcast.19), channel_id=1, replica_groups=mesh['ep_0'=8,'ep_1'=4,'ep_2'=4,'tp'=2] {'ep_1','ep_2'}, dimensions={0} | all-to-all | bytes 2752512 | tf_op jit(solution)/shard_map/all_to_all | solution.py:498
  102.4 1.0 collect.1
  103.5 5.9 %all-to-all-start.3 = ((bf16[16,3,1024]{2,1,0:T(4,128)(2,1)}), bf16[16,3,1024]{2,1,0:T(4,128)(2,1)S(1)}, u32[]{:S(2)}, u32[]{:S(2)}) async-start(bf16[16,3,1024]{2,1,0:T(4,128)(2,1)} %collect.1), calls=%async_computation.3 | async-start | bytes 262144 | tf_op jit(solution)/shard_map/all_to_all | solution.py:500
  109.3 0.7 copy.19.routes_ref
  110.0 8.2 %all-to-all-done.3.home_ref = bf16[16,3,1024]{2,1,0:T(4,128)(2,1)S(1)} async-done(((bf16[16,3,1024]{2,1,0:T(4,128)(2,1)}), bf16[16,3,1024]{2,1,0:T(4,128)(2,1)S(1)}, u32[]{:S(2)}, u32[]{:S(2)}) %all-to-all-start.3) | async-done | bytes 98336 | tf_op jit(solution)/shard_map/all_to_all | solution.py:500
  118.2 1.6 %home.1 = bf16[16,1024]{1,0:T(8,128)(2,1)} custom-call(s32[1]{0:T(128)} %bitcast.z_ref, bf16[16,3,1024]{2,1,0:T(4,128)(2,1)S(1)} %all-to-all-done.3.home_ref, bf16[16,1024]{1,0:T(8,128)(2,1)S(1)} %get-tuple-element.8.after_ref, s32[16,2]{1,0:T(8,128)} %copy.19.routes_ref), custom_call_target="tpu_custom_call" | custom-call | tf_op jit(solution)/shard_map/home/pallas_call | solution.py:442
  (67 shorter events, 0.1 us)
Async XLA Ops:
  0.6 4.4 %collective-permute-start = (bf16[16,1024]{1,0:T(8,128)(2,1)}, bf16[16,1024]{1,0:T(8,128)(2,1)S(1)}, u32[]{:S(2)}, u32[]{:S(2)}) collective-permute-start(bf16[16,1024]{1,0:T(8,128)(2,1)} %x_ref.1), channel_id=1, source_target_pairs={{0,1},{1,0},{2,3},{3,2},{4,5},{5,4},{6,7},{7,6},{8,9},{9,8},{10,11... | collective-permute-start | bytes 98312 | tf_op jit(solution)/shard_map/ppermute | solution.py:28
  5.0 5.8 %copy-start.26 = (f32[1024]{0:T(1024)S(1)}, f32[1024]{0:T(1024)}, u32[]{:S(2)}) copy-start(f32[1024]{0:T(1024)} %param.24) | copy-start | bytes 12292
  5.0 6.9 %copy-start = (bf16[16,1024]{1,0:T(8,128)(2,1)S(1)}, bf16[16,1024]{1,0:T(8,128)(2,1)}, u32[]{:S(2)}) copy-start(bf16[16,1024]{1,0:T(8,128)(2,1)} %x_ref.1) | copy-start | bytes 98308
  10.3 1.6 %collective-permute-start.1 = (bf16[16,2048]{1,0:T(8,128)(2,1)S(1)}, bf16[16,2048]{1,0:T(8,128)(2,1)S(1)}, u32[]{:S(2)}, u32[]{:S(2)}) collective-permute-start(bf16[16,2048]{1,0:T(8,128)(2,1)S(1)} %get-tuple-element.6.mix_ref), channel_id=1, source_target_pairs={{0,1},{1,0},{2,3},{3,2},{4,5},{5,4},{6,7},{7,6},{8,9},{9,8},{10,11... | collective-permute-start | bytes 196616 | tf_op jit(solution)/shard_map/ppermute | solution.py:28
  10.8 1.2 collective-permute-start.2
  29.2 7.0 %copy-start.27 = (bf16[1024]{0:T(1024)(128)(2,1)S(1)}, bf16[1024]{0:T(1024)(128)(2,1)}, u32[]{:S(2)}) copy-start(bf16[1024]{0:T(1024)(128)(2,1)} %param.25) | copy-start | bytes 6148
  29.2 7.0 %copy-start.22 = (bf16[1024,22]{0,1:T(8,128)(2,1)S(1)}, bf16[1024,22]{0,1:T(8,128)(2,1)}, u32[]{:S(2)}) copy-start(bf16[1024,22]{0,1:T(8,128)(2,1)} %param.26) | copy-start | bytes 135172
  29.2 7.0 %copy-start.23 = (bf16[1024,22]{0,1:T(8,128)(2,1)S(1)}, bf16[1024,22]{0,1:T(8,128)(2,1)}, u32[]{:S(2)}) copy-start(bf16[1024,22]{0,1:T(8,128)(2,1)} %param.27) | copy-start | bytes 135172
  29.2 7.0 %copy-start.24 = (bf16[22,1024]{1,0:T(8,128)(2,1)S(1)}, bf16[22,1024]{1,0:T(8,128)(2,1)}, u32[]{:S(2)}) copy-start(bf16[22,1024]{1,0:T(8,128)(2,1)} %param.28) | copy-start | bytes 135172
  29.2 33.0 %copy-start.2 = (bf16[1,2048,88]{1,2,0:T(8,128)(2,1)S(1)}, bf16[1,2048,88]{1,2,0:T(8,128)(2,1)}, u32[]{:S(2)}) copy-start(bf16[1,2048,88]{1,2,0:T(8,128)(2,1)} %param.29) | copy-start | bytes 1081348
  29.2 33.2 %copy-start.3 = (bf16[1,2048,88]{1,2,0:T(8,128)(2,1)S(1)}, bf16[1,2048,88]{1,2,0:T(8,128)(2,1)}, u32[]{:S(2)}) copy-start(bf16[1,2048,88]{1,2,0:T(8,128)(2,1)} %param.30) | copy-start | bytes 1081348
  29.2 34.2 %copy-start.4 = (bf16[1,88,2048]{2,1,0:T(8,128)(2,1)S(1)}, bf16[1,88,2048]{2,1,0:T(8,128)(2,1)}, u32[]{:S(2)}) copy-start(bf16[1,88,2048]{2,1,0:T(8,128)(2,1)} %param.31) | copy-start | bytes 1081348
  29.2 39.1 %all-to-all-start.1 = ((bf16[16,24,1792]{2,1,0:T(8,128)(2,1)}), bf16[16,24,1792]{2,1,0:T(8,128)(2,1)S(1)}, u32[]{:S(2)}, u32[]{:S(2)}) async-start(bf16[16,24,1792]{2,1,0:T(8,128)(2,1)} %spread.1), calls=%async_computation.1 | async-start | bytes 2752512 | tf_op jit(solution)/shard_map/all_to_all | solution.py:494
  36.3 32.0 %copy-start.1 = (bf16[72,1024]{1,0:T(8,128)(2,1)}, bf16[72,1024]{1,0:T(8,128)(2,1)S(1)}, u32[]{:S(2)}) copy-start(bf16[72,1024]{1,0:T(8,128)(2,1)S(1)} %concatenate.3.refs_8_) | copy-start | bytes 442372
  36.3 12.7 %collective-permute-start.7 = (bf16[72,1024]{1,0:T(8,128)(2,1)S(1)}, bf16[72,1024]{1,0:T(8,128)(2,1)S(1)}, u32[]{:S(2)}, u32[]{:S(2)}) collective-permute-start(bf16[72,1024]{1,0:T(8,128)(2,1)S(1)} %concatenate.3.refs_8_), channel_id=1, source_target_pairs={{0,160},{32,192},{64,224},{96,0},{128,32},{160,64},{192,96},{224,1... | collective-permute-start | bytes 442376 | tf_op jit(solution)/shard_map/ppermute | solution.py:33
  36.7 12.3 %collective-permute-start.6 = (bf16[72,1024]{1,0:T(8,128)(2,1)S(1)}, bf16[72,1024]{1,0:T(8,128)(2,1)S(1)}, u32[]{:S(2)}, u32[]{:S(2)}) collective-permute-start(bf16[72,1024]{1,0:T(8,128)(2,1)S(1)} %concatenate.3.refs_8_), channel_id=1, source_target_pairs={{0,96},{32,128},{64,160},{96,192},{128,224},{160,0},{192,32},{224,... | collective-permute-start | bytes 442376 | tf_op jit(solution)/shard_map/ppermute | solution.py:33
  39.6 15.0 %collective-permute-start.8 = (bf16[72,1024]{1,0:T(8,128)(2,1)S(1)}, bf16[72,1024]{1,0:T(8,128)(2,1)S(1)}, u32[]{:S(2)}, u32[]{:S(2)}) collective-permute-start(bf16[72,1024]{1,0:T(8,128)(2,1)S(1)} %concatenate.3.refs_8_), channel_id=1, source_target_pairs={{0,192},{32,224},{64,0},{96,32},{128,64},{160,96},{192,128},{224,1... | collective-permute-start | bytes 442376 | tf_op jit(solution)/shard_map/ppermute | solution.py:33
  41.7 15.4 %collective-permute-start.9 = (bf16[72,1024]{1,0:T(8,128)(2,1)S(1)}, bf16[72,1024]{1,0:T(8,128)(2,1)S(1)}, u32[]{:S(2)}, u32[]{:S(2)}) collective-permute-start(bf16[72,1024]{1,0:T(8,128)(2,1)S(1)} %concatenate.3.refs_8_), channel_id=1, source_target_pairs={{0,64},{32,96},{64,128},{96,160},{128,192},{160,224},{192,0},{224,... | collective-permute-start | bytes 442376 | tf_op jit(solution)/shard_map/ppermute | solution.py:33
  42.0 17.3 %collective-permute-start.10 = (bf16[72,1024]{1,0:T(8,128)(2,1)S(1)}, bf16[72,1024]{1,0:T(8,128)(2,1)S(1)}, u32[]{:S(2)}, u32[]{:S(2)}) collective-permute-start(bf16[72,1024]{1,0:T(8,128)(2,1)S(1)} %concatenate.3.refs_8_), channel_id=1, source_target_pairs={{0,32},{32,64},{64,96},{96,128},{128,160},{160,192},{192,224},{224... | collective-permute-start | bytes 442376 | tf_op jit(solution)/shard_map/ppermute | solution.py:33
  49.0 19.4 %copy-start.8 = (bf16[72,1024]{1,0:T(8,128)(2,1)}, bf16[72,1024]{1,0:T(8,128)(2,1)S(1)}, u32[]{:S(2)}) copy-start(bf16[72,1024]{1,0:T(8,128)(2,1)S(1)} %collective-permute-done.7.refs_10_) | copy-start | bytes 442372
  49.0 12.3 %collective-permute-start.11 = (bf16[72,1024]{1,0:T(8,128)(2,1)S(1)}, bf16[72,1024]{1,0:T(8,128)(2,1)S(1)}, u32[]{:S(2)}, u32[]{:S(2)}) collective-permute-start(bf16[72,1024]{1,0:T(8,128)(2,1)S(1)} %concatenate.3.refs_8_), channel_id=1, source_target_pairs={{0,224},{32,0},{64,32},{96,64},{128,96},{160,128},{192,160},{224,1... | collective-permute-start | bytes 442376 | tf_op jit(solution)/shard_map/ppermute | solution.py:33
  49.0 19.3 %copy-start.9 = (bf16[72,1024]{1,0:T(8,128)(2,1)}, bf16[72,1024]{1,0:T(8,128)(2,1)S(1)}, u32[]{:S(2)}) copy-start(bf16[72,1024]{1,0:T(8,128)(2,1)S(1)} %collective-permute-done.6.refs_9_) | copy-start | bytes 442372
  49.0 12.5 %collective-permute-start.13 = (bf16[72,1024]{1,0:T(8,128)(2,1)S(1)}, bf16[72,1024]{1,0:T(8,128)(2,1)S(1)}, u32[]{:S(2)}, u32[]{:S(2)}) collective-permute-start(bf16[72,1024]{1,0:T(8,128)(2,1)S(1)} %concatenate.3.refs_8_), channel_id=1, source_target_pairs={{0,1},{1,0},{2,3},{3,2},{4,5},{5,4},{6,7},{7,6},{8,9},{9,8},{10,11... | collective-permute-start | bytes 442376 | tf_op jit(solution)/shard_map/ppermute | solution.py:28
  54.6 13.7 %copy-start.10 = (bf16[72,1024]{1,0:T(8,128)(2,1)}, bf16[72,1024]{1,0:T(8,128)(2,1)S(1)}, u32[]{:S(2)}) copy-start(bf16[72,1024]{1,0:T(8,128)(2,1)S(1)} %collective-permute-done.8.refs_11_) | copy-start | bytes 442372
  54.6 7.8 %collective-permute-start.12 = (bf16[72,1024]{1,0:T(8,128)(2,1)S(1)}, bf16[72,1024]{1,0:T(8,128)(2,1)S(1)}, u32[]{:S(2)}, u32[]{:S(2)}) collective-permute-start(bf16[72,1024]{1,0:T(8,128)(2,1)S(1)} %collective-permute-done.7.refs_10_), channel_id=1, source_target_pairs={{0,224},{32,0},{64,32},{96,64},{128,96},{160,128},{192,160},{224,1... | collective-permute-start | bytes 442376 | tf_op jit(solution)/shard_map/ppermute | solution.py:33
  57.1 9.6 %copy-start.11 = (bf16[72,1024]{1,0:T(8,128)(2,1)}, bf16[72,1024]{1,0:T(8,128)(2,1)S(1)}, u32[]{:S(2)}) copy-start(bf16[72,1024]{1,0:T(8,128)(2,1)S(1)} %collective-permute-done.9.refs_12_) | copy-start | bytes 442372
  57.1 5.7 %collective-permute-start.15 = (bf16[72,1024]{1,0:T(8,128)(2,1)S(1)}, bf16[72,1024]{1,0:T(8,128)(2,1)S(1)}, u32[]{:S(2)}, u32[]{:S(2)}) collective-permute-start(bf16[72,1024]{1,0:T(8,128)(2,1)S(1)} %collective-permute-done.7.refs_10_), channel_id=1, source_target_pairs={{0,1},{1,0},{2,3},{3,2},{4,5},{5,4},{6,7},{7,6},{8,9},{9,8},{10,11... | collective-permute-start | bytes 442376 | tf_op jit(solution)/shard_map/ppermute | solution.py:28
  59.4 7.4 %copy-start.12 = (bf16[72,1024]{1,0:T(8,128)(2,1)}, bf16[72,1024]{1,0:T(8,128)(2,1)S(1)}, u32[]{:S(2)}) copy-start(bf16[72,1024]{1,0:T(8,128)(2,1)S(1)} %collective-permute-done.10.refs_13_) | copy-start | bytes 442372
  59.4 4.3 %collective-permute-start.14 = (bf16[72,1024]{1,0:T(8,128)(2,1)S(1)}, bf16[72,1024]{1,0:T(8,128)(2,1)S(1)}, u32[]{:S(2)}, u32[]{:S(2)}) collective-permute-start(bf16[72,1024]{1,0:T(8,128)(2,1)S(1)} %collective-permute-done.6.refs_9_), channel_id=1, source_target_pairs={{0,1},{1,0},{2,3},{3,2},{4,5},{5,4},{6,7},{7,6},{8,9},{9,8},{10,11... | collective-permute-start | bytes 442376 | tf_op jit(solution)/shard_map/ppermute | solution.py:28
  61.2 5.5 %copy-start.13 = (bf16[72,1024]{1,0:T(8,128)(2,1)}, bf16[72,1024]{1,0:T(8,128)(2,1)S(1)}, u32[]{:S(2)}) copy-start(bf16[72,1024]{1,0:T(8,128)(2,1)S(1)} %collective-permute-done.11.refs_14_) | copy-start | bytes 442372
  61.2 2.7 %collective-permute-start.16 = (bf16[72,1024]{1,0:T(8,128)(2,1)S(1)}, bf16[72,1024]{1,0:T(8,128)(2,1)S(1)}, u32[]{:S(2)}, u32[]{:S(2)}) collective-permute-start(bf16[72,1024]{1,0:T(8,128)(2,1)S(1)} %collective-permute-done.8.refs_11_), channel_id=1, source_target_pairs={{0,1},{1,0},{2,3},{3,2},{4,5},{5,4},{6,7},{7,6},{8,9},{9,8},{10,11... | collective-permute-start | bytes 442376 | tf_op jit(solution)/shard_map/ppermute | solution.py:28
  62.2 4.5 %collective-permute-start.3 = (bf16[88,2048]{1,0:T(8,128)(2,1)S(1)}, bf16[88,2048]{1,0:T(8,128)(2,1)S(1)}, u32[]{:S(2)}, u32[]{:S(2)}) collective-permute-start(bf16[88,2048]{1,0:T(8,128)(2,1)S(1)} %bitcast.22), channel_id=1, source_target_pairs={{0,1},{1,0},{2,3},{3,2},{4,5},{5,4},{6,7},{7,6},{8,9},{9,8},{10,11... | collective-permute-start | bytes 1081352 | tf_op jit(solution)/shard_map/ppermute | solution.py:28
  62.4 4.4 %copy-start.15 = (bf16[72,1024]{1,0:T(8,128)(2,1)}, bf16[72,1024]{1,0:T(8,128)(2,1)S(1)}, u32[]{:S(2)}) copy-start(bf16[72,1024]{1,0:T(8,128)(2,1)S(1)} %collective-permute-done.12.refs_15_) | copy-start | bytes 442372
  62.4 4.3 %collective-permute-start.4 = (bf16[88,2048]{1,0:T(8,128)(2,1)S(1)}, bf16[88,2048]{1,0:T(8,128)(2,1)S(1)}, u32[]{:S(2)}, u32[]{:S(2)}) collective-permute-start(bf16[88,2048]{1,0:T(8,128)(2,1)S(1)} %bitcast.24), channel_id=1, source_target_pairs={{0,1},{1,0},{2,3},{3,2},{4,5},{5,4},{6,7},{7,6},{8,9},{9,8},{10,11... | collective-permute-start | bytes 1081352 | tf_op jit(solution)/shard_map/ppermute | solution.py:28
  63.5 3.3 %collective-permute-start.5 = (bf16[88,2048]{1,0:T(8,128)(2,1)S(1)}, bf16[88,2048]{1,0:T(8,128)(2,1)S(1)}, u32[]{:S(2)}, u32[]{:S(2)}) collective-permute-start(bf16[88,2048]{1,0:T(8,128)(2,1)S(1)} %bitcast.26), channel_id=1, source_target_pairs={{0,1},{1,0},{2,3},{3,2},{4,5},{5,4},{6,7},{7,6},{8,9},{9,8},{10,11... | collective-permute-start | bytes 1081352 | tf_op jit(solution)/shard_map/ppermute | solution.py:28
  63.7 3.1 %copy-start.17 = (bf16[72,1024]{1,0:T(8,128)(2,1)}, bf16[72,1024]{1,0:T(8,128)(2,1)S(1)}, u32[]{:S(2)}) copy-start(bf16[72,1024]{1,0:T(8,128)(2,1)S(1)} %collective-permute-done.14.refs_17_) | copy-start | bytes 442372
  63.7 1.7 %collective-permute-start.17 = (bf16[72,1024]{1,0:T(8,128)(2,1)S(1)}, bf16[72,1024]{1,0:T(8,128)(2,1)S(1)}, u32[]{:S(2)}, u32[]{:S(2)}) collective-permute-start(bf16[72,1024]{1,0:T(8,128)(2,1)S(1)} %collective-permute-done.9.refs_12_), channel_id=1, source_target_pairs={{0,1},{1,0},{2,3},{3,2},{4,5},{5,4},{6,7},{7,6},{8,9},{9,8},{10,11... | collective-permute-start | bytes 442376 | tf_op jit(solution)/shard_map/ppermute | solution.py:28
  64.0 2.8 %copy-start.18 = (bf16[72,1024]{1,0:T(8,128)(2,1)}, bf16[72,1024]{1,0:T(8,128)(2,1)S(1)}, u32[]{:S(2)}) copy-start(bf16[72,1024]{1,0:T(8,128)(2,1)S(1)} %collective-permute-done.16.refs_19_) | copy-start | bytes 442372
  64.0 1.6 %collective-permute-start.18 = (bf16[72,1024]{1,0:T(8,128)(2,1)S(1)}, bf16[72,1024]{1,0:T(8,128)(2,1)S(1)}, u32[]{:S(2)}, u32[]{:S(2)}) collective-permute-start(bf16[72,1024]{1,0:T(8,128)(2,1)S(1)} %collective-permute-done.10.refs_13_), channel_id=1, source_target_pairs={{0,1},{1,0},{2,3},{3,2},{4,5},{5,4},{6,7},{7,6},{8,9},{9,8},{10,11... | collective-permute-start | bytes 442376 | tf_op jit(solution)/shard_map/ppermute | solution.py:28
  65.3 1.5 %copy-start.19 = (bf16[72,1024]{1,0:T(8,128)(2,1)}, bf16[72,1024]{1,0:T(8,128)(2,1)S(1)}, u32[]{:S(2)}) copy-start(bf16[72,1024]{1,0:T(8,128)(2,1)S(1)} %collective-permute-done.17.refs_20_) | copy-start | bytes 442372
  65.3 1.4 %collective-permute-start.19 = (bf16[72,1024]{1,0:T(8,128)(2,1)S(1)}, bf16[72,1024]{1,0:T(8,128)(2,1)S(1)}, u32[]{:S(2)}, u32[]{:S(2)}) collective-permute-start(bf16[72,1024]{1,0:T(8,128)(2,1)S(1)} %collective-permute-done.11.refs_14_), channel_id=1, source_target_pairs={{0,1},{1,0},{2,3},{3,2},{4,5},{5,4},{6,7},{7,6},{8,9},{9,8},{10,11... | collective-permute-start | bytes 442376 | tf_op jit(solution)/shard_map/ppermute | solution.py:28
  65.6 1.2 %copy-start.20 = (bf16[72,1024]{1,0:T(8,128)(2,1)}, bf16[72,1024]{1,0:T(8,128)(2,1)S(1)}, u32[]{:S(2)}) copy-start(bf16[72,1024]{1,0:T(8,128)(2,1)S(1)} %collective-permute-done.18.refs_21_) | copy-start | bytes 442372
  65.6 2.7 %collective-permute-start.20 = (bf16[72,1024]{1,0:T(8,128)(2,1)S(1)}, bf16[72,1024]{1,0:T(8,128)(2,1)}, u32[]{:S(2)}, u32[]{:S(2)}) collective-permute-start(bf16[72,1024]{1,0:T(8,128)(2,1)S(1)} %collective-permute-done.12.refs_15_), channel_id=1, source_target_pairs={{0,1},{1,0},{2,3},{3,2},{4,5},{5,4},{6,7},{7,6},{8,9},{9,8},{10,11... | collective-permute-start | bytes 442376 | tf_op jit(solution)/shard_map/ppermute | solution.py:28
  66.7 1.6 %copy-start.5 = (bf16[88,2048]{1,0:T(8,128)(2,1)}, bf16[88,2048]{1,0:T(8,128)(2,1)S(1)}, u32[]{:S(2)}) copy-start(bf16[88,2048]{1,0:T(8,128)(2,1)S(1)} %collective-permute-done.3.refs_5_) | copy-start | bytes 1081348
  66.7 0.8 copy-start.6
  67.5 0.8 copy-start.7
  102.4 6.9 %copy-start.25 = (s32[16,2]{0,1:T(2,128)S(1)}, s32[16,2]{0,1:T(2,128)}, u32[]{:S(2)}) copy-start(s32[16,2]{0,1:T(2,128)} %param.32) | copy-start | bytes 388
  103.5 14.7 %all-to-all-start.3 = ((bf16[16,3,1024]{2,1,0:T(4,128)(2,1)}), bf16[16,3,1024]{2,1,0:T(4,128)(2,1)S(1)}, u32[]{:S(2)}, u32[]{:S(2)}) async-start(bf16[16,3,1024]{2,1,0:T(4,128)(2,1)} %collect.1), calls=%async_computation.3 | async-start | bytes 262144 | tf_op jit(solution)/shard_map/all_to_all | solution.py:500
  (3 other events, 2.0 us)

commit v5 on v4

--- a/solution.py
+++ b/solution.py
@@ -16,8 +16,7 @@
 LIVE = 20
 MAIN = 1792
 TAIL = 256
-SENT = 72
-CHUNK = 80
+CHUNK = 48
 
 epsilon = 1e-06
 F32 = jnp.float32
@@ -68,10 +67,9 @@
 
 
 def branch_kernel(hidden, core_ref, x_ref, *refs):
-    weights, pieces, (out_ref, full_ref, up_ref, down_ref, own_ref, other_ref, acc_ref, sem) = (
-        refs[:6], refs[6:-8], refs[-8:],
-    )
-    half = own_ref.shape[1]
+    weights, pieces = refs[:6], refs[6:-8]
+    out_ref, full_ref, up_ref, down_ref, dense_up, dense_down, acc_ref, sem = refs[-8:]
+    half = dense_up.shape[2]
     count = len(pieces) // 2
     units = weights[0].shape[0]
     lanes = up_ref.shape[0] // 4
@@ -86,9 +84,6 @@
             fetch(weights[k], up_ref.at[pl.ds(place * lanes, units)])
     for k, place in ((2, 0), (5, 1)):
         fetch(weights[k], down_ref.at[pl.ds(place * lanes, units)])
-    for k, piece in enumerate(pieces):
-        into = (own_ref, other_ref)[k // count]
-        fetch(piece, into.at[pl.ds((k % count) * CHUNK, SENT)])
     core = core_ref[0]
     here = pl.multiple_of(core * half, half)
     there = pl.multiple_of((1 - core) * half, half)
@@ -111,32 +106,35 @@
         full_ref[band, :MAIN] = x_ref[band, :]
         full_ref[band, MAIN:] = tail.astype(BF16)
     w = jnp.concatenate(weight, axis=0)
-    for copy in copies[:6]:
+    for copy in copies:
         copy.wait()
+    first = len(copies)
+    for k, piece in enumerate(pieces):
+        at = (k % count) * CHUNK
+        fetch(piece.at[pl.ds(0, CHUNK)], dense_up.at[k // count, pl.ds(at, CHUNK)])
+        fetch(piece.at[pl.ds(CHUNK, PAD)], dense_down.at[k // count, pl.ds(at, PAD)])
     for k in range(2):
         down_ref[k * lanes + units : (k + 1) * lanes, :] = jnp.zeros(
             (lanes - units, 2 * half), BF16
         )
     pre = dot_t(full_ref[...], up_ref[...])
     h = w * silu(pre[:, : 2 * lanes]) * pre[:, 2 * lanes :]
-    h = jnp.where((iota2(h.shape, 1) & (lanes - 1)) < units, h, 0.0).astype(BF16)
+    h = jnp.where((iota2((1, 2 * lanes), 1) & (lanes - 1)) < units, h, 0.0).astype(BF16)
     acc_ref[...] = dot(h, down_ref[...])
-    for copy in copies[6:]:
+    for copy in copies[first:]:
         copy.wait()
-    for ref in (own_ref, other_ref):
+    for ref in (dense_down.at[0], dense_down.at[1]):
         for k in range(count):
-            ref[k * CHUNK + SENT : (k + 1) * CHUNK, :] = jnp.zeros((CHUNK - SENT, half), BF16)
-    pre = dot_t(full_ref[:, pl.ds(here, half)], own_ref[...])
-    pre = pre + dot_t(full_ref[:, pl.ds(there, half)], other_ref[...])
+            ref[k * CHUNK + PAD : (k + 1) * CHUNK, :] = jnp.zeros((CHUNK - PAD, half), BF16)
+    pre = dot_t(full_ref[:, pl.ds(here, half)], dense_up[0])
+    pre = pre + dot_t(full_ref[:, pl.ds(there, half)], dense_up[1])
     logit = pre[:, hidden : hidden + 1]
-    gate = pltpu.roll(pre, 2 * PAD, 1)
-    up = pltpu.roll(pre, PAD, 1)
-    unit = iota2(pre.shape, 1) % CHUNK
-    live = (unit >= 2 * PAD) & (unit < 2 * PAD + hidden) & (w > 0.0)
+    up = pltpu.roll(pre, pre.shape[1] - PAD, 1)
+    live = (iota2((1, pre.shape[1]), 1) % CHUNK < hidden) & (w > 0.0)
     scale = 0.5 / (1.0 + jnp.exp(-logit))
-    hd = jnp.where(live, scale * silu(gate) * up, 0.0).astype(BF16)
-    acc_ref[:, pl.ds(here, half)] += dot(hd, own_ref[...])
-    acc_ref[:, pl.ds(there, half)] += dot(hd, other_ref[...])
+    hd = jnp.where(live, scale * silu(pre) * up, 0.0).astype(BF16)
+    acc_ref[:, pl.ds(here, half)] += dot(hd, dense_down[0])
+    acc_ref[:, pl.ds(there, half)] += dot(hd, dense_down[1])
     for band in bands:
         tail = acc_ref[band, MAIN:].astype(BF16)
         for g in range(groups):
@@ -165,10 +163,10 @@
             pltpu.VMEM((rows, width), BF16),
             pltpu.VMEM((4 * 128, width), BF16),
             pltpu.VMEM((2 * 128, width), BF16),
-            pltpu.VMEM((units, half), BF16),
-            pltpu.VMEM((units, half), BF16),
+            pltpu.VMEM((2, units, half), BF16),
+            pltpu.VMEM((2, units, half), BF16),
             pltpu.VMEM((rows, width), F32),
-            pltpu.SemaphoreType.DMA((6 + 2 * len(pieces),)),
+            pltpu.SemaphoreType.DMA((6 + 4 * len(pieces),)),
         ],
     )(core.reshape(1), in_vmem(x), *own, *other, *pieces, *pieces2)
 
@@ -260,7 +258,8 @@
     pairs = ((x_hbm, x_ref), (wq_hbm, wq), (wk_hbm, wk), (wv_hbm, wv), (state_hbm, state_ref), (wo_hbm, wo))
     for k, (source, into) in enumerate(pairs):
         loads.append(pltpu.make_async_copy(source, into, load_sem.at[k]))
-        loads[-1].start()
+    for load in loads[:4]:
+        load.start()
     core = core_ref[0]
     here = pl.multiple_of(core * half, half)
     there = pl.multiple_of((1 - core) * half, half)
@@ -277,6 +276,8 @@
         return both.astype(BF16).astype(F32)
 
     loads[1].wait()
+    for load in loads[4:]:
+        load.start()
     query = project(wq)
     loads[2].wait()
     key = project(wk) * head ** (-0.5)
@@ -414,7 +415,8 @@
         out_specs=(vmem, vmem),
     )(
         place[0].reshape(1), place[1].reshape(1), in_vmem(own), in_vmem(other), in_vmem(mix), in_vmem(mix2),
-        gain.reshape(1, half), in_vmem(gain2.reshape(1, half)), routes.T, route_w.T,
+        in_vmem(gain.reshape(1, half)), in_vmem(gain2.reshape(1, half)), in_vmem(routes.T),
+        in_vmem(route_w.T),
     )
 
 
@@ -446,7 +448,7 @@
         in_specs=[pl.BlockSpec(memory_space=pltpu.SMEM)] + [vmem] * 3,
         out_specs=vmem,
         scratch_shapes=[pltpu.VMEM((home.shape[0] * SLOTS, home.shape[2]), F32)],
-    )(place[1].reshape(1), in_vmem(home), in_vmem(after), routes)
+    )(place[1].reshape(1), in_vmem(home), in_vmem(after), in_vmem(routes))
 
 
 def layer(
@@ -470,7 +472,7 @@
             dense_up.T,
             fill(PAD - hidden),
             dense_down,
-            fill(SENT - 2 * PAD - hidden),
+            fill(PAD - hidden),
         ],
         axis=0,
     )

time: 120 us -> 118 us (0.983)
  Pallas kernels: 17.8 us -> 15.6 us
    pallas_call x1, Pallas kernels: 7.36 us -> 6.08 us  [experts_and_dense(): pl.pallas_call(lambda *refs: branch_kernel(hidden, *refs), name='branch',...]
    unnamed x57 -> x59, local copies, waits for them, and re-layouts: 3.54 us -> 2.94 us
  transfers between devices with their start and end apart: 23 -> 23, of which waited for: 8 -> 8; matrix products, arithmetic and copies ran while one was open for 1% -> 0% of each run, Pallas kernels for 0% -> 0%
where the time goes in v5:
time: 118 us
  blocking collectives  41.5 us (35%)
  starting transfers between devices  35.5 us (30%)
  waiting for transfers between devices  21.1 us (18%)
  Pallas kernels  15.6 us (13%)
  local copies, waits for them, and re-layouts  3.05 us (3%)
    all_to_all x1, blocking collectives, layer(): lax.all_to_all(partial.reshape(chips, ROWS, MAIN), PLANE, 0, 0, tiled=True)  26.7 us
    all_to_all x1, blocking collectives, layer(): at_plane = lax.all_to_all(slot_rows, 'ep_0', 0, 0, tiled=True)  14.8 us
    ppermute x14, starting transfers between devices, swap(): return lax.ppermute(value, 'tp', [(0, 1), (1, 0)])  14.5 us
    all_to_all x1, waiting for transfers between devices, layer(): home = lax.all_to_all(send, ('ep_0', 'tp'), 0, 0, tiled=True)  8.8 us
    ppermute x7, starting transfers between devices, along_z(): lax.ppermute(value, 'ep_0', [(i, (i + shift) % size) for i in range(size)])  8.28 us
    ppermute x7, waiting for transfers between devices, along_z(): lax.ppermute(value, 'ep_0', [(i, (i + shift) % size) for i in range(size)])  8.15 us
    all_to_all x1, starting transfers between devices, layer(): gathered = lax.all_to_all(copies, PLANE, 0, 0, tiled=True)  6.89 us
    pallas_call x1, Pallas kernels, experts_and_dense(): pl.pallas_call(lambda *refs: branch_kernel(hidden, *refs), name='branch',...  6.08 us
  transfers between devices with their start and end apart: 23, of which 8 were waited for; matrix products, arithmetic and copies ran while one was open for 0% of the time, Pallas kernels for 0%

profile of v5, /device:TPU:1, one launch (start us, length us, event | category | flops | bytes accessed | tf_op | source)
XLA Modules:
  0.0 117.6 jit_solution(14942892878420518299)
XLA Ops:
  0.6 3.3 %collective-permute-start = (bf16[16,1024]{1,0:T(8,128)(2,1)}, bf16[16,1024]{1,0:T(8,128)(2,1)S(1)}, u32[]{:S(2)}, u32[]{:S(2)}) collective-permute-start(bf16[16,1024]{1,0:T(8,128)(2,1)} %x_ref.1), channel_id=1, source_target_pairs={{0,1},{1,0},{2,3},{3,2},{4,5},{5,4},{6,7},{7,6},{8,9},{9,8},{10,11... | collective-permute-start | bytes 98312 | tf_op jit(solution)/shard_map/ppermute | solution.py:27
  3.9 1.1 collective-permute-done.y_ref
  5.0 5.8 %mixer.1 = (bf16[16,2048]{1,0:T(8,128)(2,1)S(1)}, f32[16,2,128,128]{3,2,1,0:T(8,128)}) custom-call(s32[1]{0:T(128)} %bitcast.1.core_ref.refs_0_, bf16[16,1024]{1,0:T(8,128)(2,1)} %x_ref.1, bf16[16,1024]{1,0:T(8,128)(2,1)S(1)} %collective-permute-done.y_ref, f32[1,2048]{1,0:T(1,128)} %bitcast.32, bf16[2048,256]{1,0:T(8,128)(2,1)} %wq_hbm.1, ...), custom_call_target="tpu_custom_call" | custom-call | tf_op jit(solution)/shard_map/mixer/pallas_call | solution.py:328
  10.8 0.5 collective-permute-start.1
  11.2 0.1 collective-permute-start.2
  11.4 1.0 collective-permute-done.2
  12.4 0.3 slots.1
  12.8 14.8 %all_to_all.20.x_ref = bf16[8,3,2176]{2,1,0:T(4,128)(2,1)S(1)} all-to-all(bf16[8,3,2176]{2,1,0:T(4,128)(2,1)S(1)} %get-tuple-element.7), channel_id=1, replica_groups=mesh['ep_0'=8,'ep_1'=4,'ep_2'=4,'tp'=2] {'ep_0'}, dimensions={0} | all-to-all | bytes 208896 | tf_op jit(solution)/shard_map/all_to_all | solution.py:488
  27.6 1.4 %spread.1 = bf16[16,24,1792]{2,1,0:T(8,128)(2,1)} custom-call(s32[1]{0:T(128)} %bitcast.1.core_ref.refs_0_, bf16[8,3,2176]{2,1,0:T(4,128)(2,1)S(1)} %all_to_all.20.x_ref), custom_call_target="tpu_custom_call" | custom-call | tf_op jit(solution)/shard_map/spread/pallas_call | solution.py:207
  29.0 0.0 copy-start.5
  29.0 0.0 copy-start.6
  29.0 0.0 copy-start.7
  29.0 6.9 %all-to-all-start.1 = ((bf16[16,24,1792]{2,1,0:T(8,128)(2,1)}), bf16[16,24,1792]{2,1,0:T(8,128)(2,1)S(1)}, u32[]{:S(2)}, u32[]{:S(2)}) async-start(bf16[16,24,1792]{2,1,0:T(8,128)(2,1)} %spread.1), calls=%async_computation.1 | async-start | bytes 2752512 | tf_op jit(solution)/shard_map/all_to_all | solution.py:496
  36.0 0.1 concatenate.3.refs_8_
  36.1 0.4 collective-permute-start.7
  36.5 3.0 %collective-permute-start.6 = (bf16[72,1024]{1,0:T(8,128)(2,1)S(1)}, bf16[72,1024]{1,0:T(8,128)(2,1)S(1)}, u32[]{:S(2)}, u32[]{:S(2)}) collective-permute-start(bf16[72,1024]{1,0:T(8,128)(2,1)S(1)} %concatenate.3.refs_8_), channel_id=1, source_target_pairs={{0,96},{32,128},{64,160},{96,192},{128,224},{160,0},{192,32},{224,... | collective-permute-start | bytes 442376 | tf_op jit(solution)/shard_map/ppermute | solution.py:32
  39.4 2.0 %collective-permute-start.8 = (bf16[72,1024]{1,0:T(8,128)(2,1)S(1)}, bf16[72,1024]{1,0:T(8,128)(2,1)S(1)}, u32[]{:S(2)}, u32[]{:S(2)}) collective-permute-start(bf16[72,1024]{1,0:T(8,128)(2,1)S(1)} %concatenate.3.refs_8_), channel_id=1, source_target_pairs={{0,192},{32,224},{64,0},{96,32},{128,64},{160,96},{192,128},{224,1... | collective-permute-start | bytes 442376 | tf_op jit(solution)/shard_map/ppermute | solution.py:32
  41.5 0.3 collective-permute-start.9
  41.8 1.2 %collective-permute-start.10 = (bf16[72,1024]{1,0:T(8,128)(2,1)S(1)}, bf16[72,1024]{1,0:T(8,128)(2,1)S(1)}, u32[]{:S(2)}, u32[]{:S(2)}) collective-permute-start(bf16[72,1024]{1,0:T(8,128)(2,1)S(1)} %concatenate.3.refs_8_), channel_id=1, source_target_pairs={{0,32},{32,64},{64,96},{96,128},{128,160},{160,192},{192,224},{224... | collective-permute-start | bytes 442376 | tf_op jit(solution)/shard_map/ppermute | solution.py:32
  43.0 5.7 %collective-permute-done.7.refs_10_ = bf16[72,1024]{1,0:T(8,128)(2,1)S(1)} collective-permute-done((bf16[72,1024]{1,0:T(8,128)(2,1)S(1)}, bf16[72,1024]{1,0:T(8,128)(2,1)S(1)}, u32[]{:S(2)}, u32[]{:S(2)}) %collective-permute-start.7) | collective-permute-done | bytes 147488 | tf_op jit(solution)/shard_map/ppermute | solution.py:32
  48.7 5.7 %collective-permute-start.13 = (bf16[72,1024]{1,0:T(8,128)(2,1)S(1)}, bf16[72,1024]{1,0:T(8,128)(2,1)S(1)}, u32[]{:S(2)}, u32[]{:S(2)}) collective-permute-start(bf16[72,1024]{1,0:T(8,128)(2,1)S(1)} %concatenate.3.refs_8_), channel_id=1, source_target_pairs={{0,1},{1,0},{2,3},{3,2},{4,5},{5,4},{6,7},{7,6},{8,9},{9,8},{10,11... | collective-permute-start | bytes 442376 | tf_op jit(solution)/shard_map/ppermute | solution.py:27
  54.4 1.4 %collective-permute-start.12 = (bf16[72,1024]{1,0:T(8,128)(2,1)S(1)}, bf16[72,1024]{1,0:T(8,128)(2,1)S(1)}, u32[]{:S(2)}, u32[]{:S(2)}) collective-permute-start(bf16[72,1024]{1,0:T(8,128)(2,1)S(1)} %collective-permute-done.7.refs_10_), channel_id=1, source_target_pairs={{0,224},{32,0},{64,32},{96,64},{128,96},{160,128},{192,160},{224,1... | collective-permute-start | bytes 442376 | tf_op jit(solution)/shard_map/ppermute | solution.py:32
  55.8 1.1 collective-permute-done.9.refs_12_
  56.9 0.9 collective-permute-start.15
  57.8 1.4 %collective-permute-done.10.refs_13_ = bf16[72,1024]{1,0:T(8,128)(2,1)S(1)} collective-permute-done((bf16[72,1024]{1,0:T(8,128)(2,1)S(1)}, bf16[72,1024]{1,0:T(8,128)(2,1)S(1)}, u32[]{:S(2)}, u32[]{:S(2)}) %collective-permute-start.10) | collective-permute-done | bytes 147488 | tf_op jit(solution)/shard_map/ppermute | solution.py:32
  59.1 1.9 %collective-permute-start.14 = (bf16[72,1024]{1,0:T(8,128)(2,1)S(1)}, bf16[72,1024]{1,0:T(8,128)(2,1)S(1)}, u32[]{:S(2)}, u32[]{:S(2)}) collective-permute-start(bf16[72,1024]{1,0:T(8,128)(2,1)S(1)} %collective-permute-done.6.refs_9_), channel_id=1, source_target_pairs={{0,1},{1,0},{2,3},{3,2},{4,5},{5,4},{6,7},{7,6},{8,9},{9,8},{10,11... | collective-permute-start | bytes 442376 | tf_op jit(solution)/shard_map/ppermute | solution.py:27
  61.0 0.3 collective-permute-start.16
  61.3 0.7 copy-done.17
  62.0 0.2 collective-permute-start.3
  62.2 0.4 collective-permute-start.4
  62.6 0.7 copy-done.19
  63.3 0.2 collective-permute-start.5
  63.5 0.3 collective-permute-start.17
  63.8 0.2 collective-permute-start.18
  64.0 1.1 collective-permute-done.17.refs_20_
  65.1 0.2 collective-permute-start.19
  65.4 0.3 collective-permute-start.20
  65.7 0.9 collective-permute-done.19.refs_22_
  66.6 0.5 copy-done.24
  67.2 0.1 copy-done.9
  67.3 0.8 copy-done.10
  68.1 6.1 %branch.1 = bf16[384,1792]{1,0:T(8,128)(2,1)S(1)} custom-call(s32[1]{0:T(128)} %bitcast.1.core_ref.refs_0_, bf16[384,1792]{1,0:T(8,128)(2,1)S(1)} %bitcast.18, bf16[88,2048]{1,0:T(8,128)(2,1)} %bitcast.24, bf16[88,2048]{1,0:T(8,128)(2,1)} %bitcast.26, bf16[88,2048]{1,0:T(8,128)(2,1)} %bitcast.28, bf16[88,2048]{1,0:T(8,128)(2,1)} %copy-done.8, ...), custom_call_target="tpu_custom_call" | custom-call | tf_op jit(solution)/shard_map/branch/pallas_call | solution.py:156
  74.2 26.7 %all_to_all.21.x_ref = bf16[16,24,1792]{2,1,0:T(8,128)(2,1)S(1)} all-to-all(bf16[16,24,1792]{2,1,0:T(8,128)(2,1)S(1)} %bitcast.19), channel_id=1, replica_groups=mesh['ep_0'=8,'ep_1'=4,'ep_2'=4,'tp'=2] {'ep_1','ep_2'}, dimensions={0} | all-to-all | bytes 2752512 | tf_op jit(solution)/shard_map/all_to_all | solution.py:500
  100.9 1.0 collect.1
  102.0 5.9 %all-to-all-start.3 = ((bf16[16,3,1024]{2,1,0:T(4,128)(2,1)}), bf16[16,3,1024]{2,1,0:T(4,128)(2,1)S(1)}, u32[]{:S(2)}, u32[]{:S(2)}) async-start(bf16[16,3,1024]{2,1,0:T(4,128)(2,1)} %collect.1), calls=%async_computation.3 | async-start | bytes 262144 | tf_op jit(solution)/shard_map/all_to_all | solution.py:502
  107.8 0.1 copy.19.routes_ref
  107.9 8.8 %all-to-all-done.3.home_ref = bf16[16,3,1024]{2,1,0:T(4,128)(2,1)S(1)} async-done(((bf16[16,3,1024]{2,1,0:T(4,128)(2,1)}), bf16[16,3,1024]{2,1,0:T(4,128)(2,1)S(1)}, u32[]{:S(2)}, u32[]{:S(2)}) %all-to-all-start.3) | async-done | bytes 98336 | tf_op jit(solution)/shard_map/all_to_all | solution.py:502
  116.7 0.9 home.1
  (69 shorter events, 0.2 us)
Async XLA Ops:
  0.6 4.4 %collective-permute-start = (bf16[16,1024]{1,0:T(8,128)(2,1)}, bf16[16,1024]{1,0:T(8,128)(2,1)S(1)}, u32[]{:S(2)}, u32[]{:S(2)}) collective-permute-start(bf16[16,1024]{1,0:T(8,128)(2,1)} %x_ref.1), channel_id=1, source_target_pairs={{0,1},{1,0},{2,3},{3,2},{4,5},{5,4},{6,7},{7,6},{8,9},{9,8},{10,11... | collective-permute-start | bytes 98312 | tf_op jit(solution)/shard_map/ppermute | solution.py:27
  5.0 6.2 %copy-start.2 = (f32[1024]{0:T(1024)S(1)}, f32[1024]{0:T(1024)}, u32[]{:S(2)}) copy-start(f32[1024]{0:T(1024)} %param.24) | copy-start | bytes 12292
  5.0 7.4 %copy-start = (bf16[16,1024]{1,0:T(8,128)(2,1)S(1)}, bf16[16,1024]{1,0:T(8,128)(2,1)}, u32[]{:S(2)}) copy-start(bf16[16,1024]{1,0:T(8,128)(2,1)} %x_ref.1) | copy-start | bytes 98308
  5.0 7.4 %copy-start.1 = (s32[16,2]{0,1:T(2,128)S(1)}, s32[16,2]{0,1:T(2,128)}, u32[]{:S(2)}) copy-start(s32[16,2]{0,1:T(2,128)} %param.32) | copy-start | bytes 388
  5.0 7.4 %copy-start.3 = (bf16[16,2]{0,1:T(2,128)(2,1)S(1)}, bf16[16,2]{0,1:T(2,128)(2,1)}, u32[]{:S(2)}) copy-start(bf16[16,2]{0,1:T(2,128)(2,1)} %param.33) | copy-start | bytes 196
  10.8 1.6 %collective-permute-start.1 = (bf16[16,2048]{1,0:T(8,128)(2,1)S(1)}, bf16[16,2048]{1,0:T(8,128)(2,1)S(1)}, u32[]{:S(2)}, u32[]{:S(2)}) collective-permute-start(bf16[16,2048]{1,0:T(8,128)(2,1)S(1)} %get-tuple-element.6.mix_ref), channel_id=1, source_target_pairs={{0,1},{1,0},{2,3},{3,2},{4,5},{5,4},{6,7},{7,6},{8,9},{9,8},{10,11... | collective-permute-start | bytes 196616 | tf_op jit(solution)/shard_map/ppermute | solution.py:27
  11.2 1.2 collective-permute-start.2
  29.0 7.0 %copy-start.28 = (bf16[1024]{0:T(1024)(128)(2,1)S(1)}, bf16[1024]{0:T(1024)(128)(2,1)}, u32[]{:S(2)}) copy-start(bf16[1024]{0:T(1024)(128)(2,1)} %param.25) | copy-start | bytes 6148
  29.0 7.0 %copy-start.25 = (bf16[1024,22]{0,1:T(8,128)(2,1)S(1)}, bf16[1024,22]{0,1:T(8,128)(2,1)}, u32[]{:S(2)}) copy-start(bf16[1024,22]{0,1:T(8,128)(2,1)} %param.26) | copy-start | bytes 135172
  29.0 7.0 %copy-start.26 = (bf16[1024,22]{0,1:T(8,128)(2,1)S(1)}, bf16[1024,22]{0,1:T(8,128)(2,1)}, u32[]{:S(2)}) copy-start(bf16[1024,22]{0,1:T(8,128)(2,1)} %param.27) | copy-start | bytes 135172
  29.0 7.0 %copy-start.27 = (bf16[22,1024]{1,0:T(8,128)(2,1)S(1)}, bf16[22,1024]{1,0:T(8,128)(2,1)}, u32[]{:S(2)}) copy-start(bf16[22,1024]{1,0:T(8,128)(2,1)} %param.28) | copy-start | bytes 135172
  29.0 33.0 %copy-start.5 = (bf16[1,2048,88]{1,2,0:T(8,128)(2,1)S(1)}, bf16[1,2048,88]{1,2,0:T(8,128)(2,1)}, u32[]{:S(2)}) copy-start(bf16[1,2048,88]{1,2,0:T(8,128)(2,1)} %param.29) | copy-start | bytes 1081348
  29.0 33.2 %copy-start.6 = (bf16[1,2048,88]{1,2,0:T(8,128)(2,1)S(1)}, bf16[1,2048,88]{1,2,0:T(8,128)(2,1)}, u32[]{:S(2)}) copy-start(bf16[1,2048,88]{1,2,0:T(8,128)(2,1)} %param.30) | copy-start | bytes 1081348
  29.0 34.3 %copy-start.7 = (bf16[1,88,2048]{2,1,0:T(8,128)(2,1)S(1)}, bf16[1,88,2048]{2,1,0:T(8,128)(2,1)}, u32[]{:S(2)}) copy-start(bf16[1,88,2048]{2,1,0:T(8,128)(2,1)} %param.31) | copy-start | bytes 1081348
  29.0 39.1 %all-to-all-start.1 = ((bf16[16,24,1792]{2,1,0:T(8,128)(2,1)}), bf16[16,24,1792]{2,1,0:T(8,128)(2,1)S(1)}, u32[]{:S(2)}, u32[]{:S(2)}) async-start(bf16[16,24,1792]{2,1,0:T(8,128)(2,1)} %spread.1), calls=%async_computation.1 | async-start | bytes 2752512 | tf_op jit(solution)/shard_map/all_to_all | solution.py:496
  36.1 32.0 %copy-start.4 = (bf16[72,1024]{1,0:T(8,128)(2,1)}, bf16[72,1024]{1,0:T(8,128)(2,1)S(1)}, u32[]{:S(2)}) copy-start(bf16[72,1024]{1,0:T(8,128)(2,1)S(1)} %concatenate.3.refs_8_) | copy-start | bytes 442372
  36.1 12.6 %collective-permute-start.7 = (bf16[72,1024]{1,0:T(8,128)(2,1)S(1)}, bf16[72,1024]{1,0:T(8,128)(2,1)S(1)}, u32[]{:S(2)}, u32[]{:S(2)}) collective-permute-start(bf16[72,1024]{1,0:T(8,128)(2,1)S(1)} %concatenate.3.refs_8_), channel_id=1, source_target_pairs={{0,160},{32,192},{64,224},{96,0},{128,32},{160,64},{192,96},{224,1... | collective-permute-start | bytes 442376 | tf_op jit(solution)/shard_map/ppermute | solution.py:32
  36.5 12.2 %collective-permute-start.6 = (bf16[72,1024]{1,0:T(8,128)(2,1)S(1)}, bf16[72,1024]{1,0:T(8,128)(2,1)S(1)}, u32[]{:S(2)}, u32[]{:S(2)}) collective-permute-start(bf16[72,1024]{1,0:T(8,128)(2,1)S(1)} %concatenate.3.refs_8_), channel_id=1, source_target_pairs={{0,96},{32,128},{64,160},{96,192},{128,224},{160,0},{192,32},{224,... | collective-permute-start | bytes 442376 | tf_op jit(solution)/shard_map/ppermute | solution.py:32
  39.4 15.0 %collective-permute-start.8 = (bf16[72,1024]{1,0:T(8,128)(2,1)S(1)}, bf16[72,1024]{1,0:T(8,128)(2,1)S(1)}, u32[]{:S(2)}, u32[]{:S(2)}) collective-permute-start(bf16[72,1024]{1,0:T(8,128)(2,1)S(1)} %concatenate.3.refs_8_), channel_id=1, source_target_pairs={{0,192},{32,224},{64,0},{96,32},{128,64},{160,96},{192,128},{224,1... | collective-permute-start | bytes 442376 | tf_op jit(solution)/shard_map/ppermute | solution.py:32
  41.5 15.5 %collective-permute-start.9 = (bf16[72,1024]{1,0:T(8,128)(2,1)S(1)}, bf16[72,1024]{1,0:T(8,128)(2,1)S(1)}, u32[]{:S(2)}, u32[]{:S(2)}) collective-permute-start(bf16[72,1024]{1,0:T(8,128)(2,1)S(1)} %concatenate.3.refs_8_), channel_id=1, source_target_pairs={{0,64},{32,96},{64,128},{96,160},{128,192},{160,224},{192,0},{224,... | collective-permute-start | bytes 442376 | tf_op jit(solution)/shard_map/ppermute | solution.py:32
  41.8 17.3 %collective-permute-start.10 = (bf16[72,1024]{1,0:T(8,128)(2,1)S(1)}, bf16[72,1024]{1,0:T(8,128)(2,1)S(1)}, u32[]{:S(2)}, u32[]{:S(2)}) collective-permute-start(bf16[72,1024]{1,0:T(8,128)(2,1)S(1)} %concatenate.3.refs_8_), channel_id=1, source_target_pairs={{0,32},{32,64},{64,96},{96,128},{128,160},{160,192},{192,224},{224... | collective-permute-start | bytes 442376 | tf_op jit(solution)/shard_map/ppermute | solution.py:32
  48.7 19.4 %copy-start.11 = (bf16[72,1024]{1,0:T(8,128)(2,1)}, bf16[72,1024]{1,0:T(8,128)(2,1)S(1)}, u32[]{:S(2)}) copy-start(bf16[72,1024]{1,0:T(8,128)(2,1)S(1)} %collective-permute-done.7.refs_10_) | copy-start | bytes 442372
  48.7 12.3 %collective-permute-start.11 = (bf16[72,1024]{1,0:T(8,128)(2,1)S(1)}, bf16[72,1024]{1,0:T(8,128)(2,1)S(1)}, u32[]{:S(2)}, u32[]{:S(2)}) collective-permute-start(bf16[72,1024]{1,0:T(8,128)(2,1)S(1)} %concatenate.3.refs_8_), channel_id=1, source_target_pairs={{0,224},{32,0},{64,32},{96,64},{128,96},{160,128},{192,160},{224,1... | collective-permute-start | bytes 442376 | tf_op jit(solution)/shard_map/ppermute | solution.py:32
  48.7 19.4 %copy-start.12 = (bf16[72,1024]{1,0:T(8,128)(2,1)}, bf16[72,1024]{1,0:T(8,128)(2,1)S(1)}, u32[]{:S(2)}) copy-start(bf16[72,1024]{1,0:T(8,128)(2,1)S(1)} %collective-permute-done.6.refs_9_) | copy-start | bytes 442372
  48.7 12.6 %collective-permute-start.13 = (bf16[72,1024]{1,0:T(8,128)(2,1)S(1)}, bf16[72,1024]{1,0:T(8,128)(2,1)S(1)}, u32[]{:S(2)}, u32[]{:S(2)}) collective-permute-start(bf16[72,1024]{1,0:T(8,128)(2,1)S(1)} %concatenate.3.refs_8_), channel_id=1, source_target_pairs={{0,1},{1,0},{2,3},{3,2},{4,5},{5,4},{6,7},{7,6},{8,9},{9,8},{10,11... | collective-permute-start | bytes 442376 | tf_op jit(solution)/shard_map/ppermute | solution.py:27
  54.4 13.6 %copy-start.13 = (bf16[72,1024]{1,0:T(8,128)(2,1)}, bf16[72,1024]{1,0:T(8,128)(2,1)S(1)}, u32[]{:S(2)}) copy-start(bf16[72,1024]{1,0:T(8,128)(2,1)S(1)} %collective-permute-done.8.refs_11_) | copy-start | bytes 442372
  54.4 7.8 %collective-permute-start.12 = (bf16[72,1024]{1,0:T(8,128)(2,1)S(1)}, bf16[72,1024]{1,0:T(8,128)(2,1)S(1)}, u32[]{:S(2)}, u32[]{:S(2)}) collective-permute-start(bf16[72,1024]{1,0:T(8,128)(2,1)S(1)} %collective-permute-done.7.refs_10_), channel_id=1, source_target_pairs={{0,224},{32,0},{64,32},{96,64},{128,96},{160,128},{192,160},{224,1... | collective-permute-start | bytes 442376 | tf_op jit(solution)/shard_map/ppermute | solution.py:32
  56.9 9.6 %copy-start.14 = (bf16[72,1024]{1,0:T(8,128)(2,1)}, bf16[72,1024]{1,0:T(8,128)(2,1)S(1)}, u32[]{:S(2)}) copy-start(bf16[72,1024]{1,0:T(8,128)(2,1)S(1)} %collective-permute-done.9.refs_12_) | copy-start | bytes 442372
  56.9 5.7 %collective-permute-start.15 = (bf16[72,1024]{1,0:T(8,128)(2,1)S(1)}, bf16[72,1024]{1,0:T(8,128)(2,1)S(1)}, u32[]{:S(2)}, u32[]{:S(2)}) collective-permute-start(bf16[72,1024]{1,0:T(8,128)(2,1)S(1)} %collective-permute-done.7.refs_10_), channel_id=1, source_target_pairs={{0,1},{1,0},{2,3},{3,2},{4,5},{5,4},{6,7},{7,6},{8,9},{9,8},{10,11... | collective-permute-start | bytes 442376 | tf_op jit(solution)/shard_map/ppermute | solution.py:27
  59.1 7.4 %copy-start.15 = (bf16[72,1024]{1,0:T(8,128)(2,1)}, bf16[72,1024]{1,0:T(8,128)(2,1)S(1)}, u32[]{:S(2)}) copy-start(bf16[72,1024]{1,0:T(8,128)(2,1)S(1)} %collective-permute-done.10.refs_13_) | copy-start | bytes 442372
  59.1 4.3 %collective-permute-start.14 = (bf16[72,1024]{1,0:T(8,128)(2,1)S(1)}, bf16[72,1024]{1,0:T(8,128)(2,1)S(1)}, u32[]{:S(2)}, u32[]{:S(2)}) collective-permute-start(bf16[72,1024]{1,0:T(8,128)(2,1)S(1)} %collective-permute-done.6.refs_9_), channel_id=1, source_target_pairs={{0,1},{1,0},{2,3},{3,2},{4,5},{5,4},{6,7},{7,6},{8,9},{9,8},{10,11... | collective-permute-start | bytes 442376 | tf_op jit(solution)/shard_map/ppermute | solution.py:27
  61.0 5.5 %copy-start.16 = (bf16[72,1024]{1,0:T(8,128)(2,1)}, bf16[72,1024]{1,0:T(8,128)(2,1)S(1)}, u32[]{:S(2)}) copy-start(bf16[72,1024]{1,0:T(8,128)(2,1)S(1)} %collective-permute-done.11.refs_14_) | copy-start | bytes 442372
  61.0 2.7 %collective-permute-start.16 = (bf16[72,1024]{1,0:T(8,128)(2,1)S(1)}, bf16[72,1024]{1,0:T(8,128)(2,1)S(1)}, u32[]{:S(2)}, u32[]{:S(2)}) collective-permute-start(bf16[72,1024]{1,0:T(8,128)(2,1)S(1)} %collective-permute-done.8.refs_11_), channel_id=1, source_target_pairs={{0,1},{1,0},{2,3},{3,2},{4,5},{5,4},{6,7},{7,6},{8,9},{9,8},{10,11... | collective-permute-start | bytes 442376 | tf_op jit(solution)/shard_map/ppermute | solution.py:27
  62.0 4.5 %collective-permute-start.3 = (bf16[88,2048]{1,0:T(8,128)(2,1)S(1)}, bf16[88,2048]{1,0:T(8,128)(2,1)S(1)}, u32[]{:S(2)}, u32[]{:S(2)}) collective-permute-start(bf16[88,2048]{1,0:T(8,128)(2,1)S(1)} %bitcast.25), channel_id=1, source_target_pairs={{0,1},{1,0},{2,3},{3,2},{4,5},{5,4},{6,7},{7,6},{8,9},{9,8},{10,11... | collective-permute-start | bytes 1081352 | tf_op jit(solution)/shard_map/ppermute | solution.py:27
  62.2 4.4 %copy-start.18 = (bf16[72,1024]{1,0:T(8,128)(2,1)}, bf16[72,1024]{1,0:T(8,128)(2,1)S(1)}, u32[]{:S(2)}) copy-start(bf16[72,1024]{1,0:T(8,128)(2,1)S(1)} %collective-permute-done.12.refs_15_) | copy-start | bytes 442372
  62.2 4.3 %collective-permute-start.4 = (bf16[88,2048]{1,0:T(8,128)(2,1)S(1)}, bf16[88,2048]{1,0:T(8,128)(2,1)S(1)}, u32[]{:S(2)}, u32[]{:S(2)}) collective-permute-start(bf16[88,2048]{1,0:T(8,128)(2,1)S(1)} %bitcast.27), channel_id=1, source_target_pairs={{0,1},{1,0},{2,3},{3,2},{4,5},{5,4},{6,7},{7,6},{8,9},{9,8},{10,11... | collective-permute-start | bytes 1081352 | tf_op jit(solution)/shard_map/ppermute | solution.py:27
  63.3 3.3 %collective-permute-start.5 = (bf16[88,2048]{1,0:T(8,128)(2,1)S(1)}, bf16[88,2048]{1,0:T(8,128)(2,1)S(1)}, u32[]{:S(2)}, u32[]{:S(2)}) collective-permute-start(bf16[88,2048]{1,0:T(8,128)(2,1)S(1)} %bitcast.29), channel_id=1, source_target_pairs={{0,1},{1,0},{2,3},{3,2},{4,5},{5,4},{6,7},{7,6},{8,9},{9,8},{10,11... | collective-permute-start | bytes 1081352 | tf_op jit(solution)/shard_map/ppermute | solution.py:27
  63.5 3.1 %copy-start.20 = (bf16[72,1024]{1,0:T(8,128)(2,1)}, bf16[72,1024]{1,0:T(8,128)(2,1)S(1)}, u32[]{:S(2)}) copy-start(bf16[72,1024]{1,0:T(8,128)(2,1)S(1)} %collective-permute-done.14.refs_17_) | copy-start | bytes 442372
  63.5 1.7 %collective-permute-start.17 = (bf16[72,1024]{1,0:T(8,128)(2,1)S(1)}, bf16[72,1024]{1,0:T(8,128)(2,1)S(1)}, u32[]{:S(2)}, u32[]{:S(2)}) collective-permute-start(bf16[72,1024]{1,0:T(8,128)(2,1)S(1)} %collective-permute-done.9.refs_12_), channel_id=1, source_target_pairs={{0,1},{1,0},{2,3},{3,2},{4,5},{5,4},{6,7},{7,6},{8,9},{9,8},{10,11... | collective-permute-start | bytes 442376 | tf_op jit(solution)/shard_map/ppermute | solution.py:27
  63.8 2.8 %copy-start.21 = (bf16[72,1024]{1,0:T(8,128)(2,1)}, bf16[72,1024]{1,0:T(8,128)(2,1)S(1)}, u32[]{:S(2)}) copy-start(bf16[72,1024]{1,0:T(8,128)(2,1)S(1)} %collective-permute-done.16.refs_19_) | copy-start | bytes 442372
  63.8 1.6 %collective-permute-start.18 = (bf16[72,1024]{1,0:T(8,128)(2,1)S(1)}, bf16[72,1024]{1,0:T(8,128)(2,1)S(1)}, u32[]{:S(2)}, u32[]{:S(2)}) collective-permute-start(bf16[72,1024]{1,0:T(8,128)(2,1)S(1)} %collective-permute-done.10.refs_13_), channel_id=1, source_target_pairs={{0,1},{1,0},{2,3},{3,2},{4,5},{5,4},{6,7},{7,6},{8,9},{9,8},{10,11... | collective-permute-start | bytes 442376 | tf_op jit(solution)/shard_map/ppermute | solution.py:27
  65.1 1.5 %copy-start.22 = (bf16[72,1024]{1,0:T(8,128)(2,1)}, bf16[72,1024]{1,0:T(8,128)(2,1)S(1)}, u32[]{:S(2)}) copy-start(bf16[72,1024]{1,0:T(8,128)(2,1)S(1)} %collective-permute-done.17.refs_20_) | copy-start | bytes 442372
  65.1 1.4 %collective-permute-start.19 = (bf16[72,1024]{1,0:T(8,128)(2,1)S(1)}, bf16[72,1024]{1,0:T(8,128)(2,1)S(1)}, u32[]{:S(2)}, u32[]{:S(2)}) collective-permute-start(bf16[72,1024]{1,0:T(8,128)(2,1)S(1)} %collective-permute-done.11.refs_14_), channel_id=1, source_target_pairs={{0,1},{1,0},{2,3},{3,2},{4,5},{5,4},{6,7},{7,6},{8,9},{9,8},{10,11... | collective-permute-start | bytes 442376 | tf_op jit(solution)/shard_map/ppermute | solution.py:27
  65.4 1.2 %copy-start.23 = (bf16[72,1024]{1,0:T(8,128)(2,1)}, bf16[72,1024]{1,0:T(8,128)(2,1)S(1)}, u32[]{:S(2)}) copy-start(bf16[72,1024]{1,0:T(8,128)(2,1)S(1)} %collective-permute-done.18.refs_21_) | copy-start | bytes 442372
  65.4 2.7 %collective-permute-start.20 = (bf16[72,1024]{1,0:T(8,128)(2,1)S(1)}, bf16[72,1024]{1,0:T(8,128)(2,1)}, u32[]{:S(2)}, u32[]{:S(2)}) collective-permute-start(bf16[72,1024]{1,0:T(8,128)(2,1)S(1)} %collective-permute-done.12.refs_15_), channel_id=1, source_target_pairs={{0,1},{1,0},{2,3},{3,2},{4,5},{5,4},{6,7},{7,6},{8,9},{9,8},{10,11... | collective-permute-start | bytes 442376 | tf_op jit(solution)/shard_map/ppermute | solution.py:27
  66.5 1.6 %copy-start.8 = (bf16[88,2048]{1,0:T(8,128)(2,1)}, bf16[88,2048]{1,0:T(8,128)(2,1)S(1)}, u32[]{:S(2)}) copy-start(bf16[88,2048]{1,0:T(8,128)(2,1)S(1)} %collective-permute-done.3.refs_5_) | copy-start | bytes 1081348
  66.5 0.8 copy-start.9
  102.0 14.8 %all-to-all-start.3 = ((bf16[16,3,1024]{2,1,0:T(4,128)(2,1)}), bf16[16,3,1024]{2,1,0:T(4,128)(2,1)S(1)}, u32[]{:S(2)}, u32[]{:S(2)}) async-start(bf16[16,3,1024]{2,1,0:T(4,128)(2,1)} %collect.1), calls=%async_computation.3 | async-start | bytes 262144 | tf_op jit(solution)/shard_map/all_to_all | solution.py:502
  (4 other events, 2.7 us)

commit v6 on v5

--- a/solution.py
+++ b/solution.py
@@ -84,6 +84,10 @@
             fetch(weights[k], up_ref.at[pl.ds(place * lanes, units)])
     for k, place in ((2, 0), (5, 1)):
         fetch(weights[k], down_ref.at[pl.ds(place * lanes, units)])
+    for k, piece in enumerate(pieces):
+        at = (k % count) * CHUNK
+        fetch(piece.at[pl.ds(0, CHUNK)], dense_up.at[k // count, pl.ds(at, CHUNK)])
+        fetch(piece.at[pl.ds(CHUNK, PAD)], dense_down.at[k // count, pl.ds(at, PAD)])
     core = core_ref[0]
     here = pl.multiple_of(core * half, half)
     there = pl.multiple_of((1 - core) * half, half)
@@ -106,13 +110,8 @@
         full_ref[band, :MAIN] = x_ref[band, :]
         full_ref[band, MAIN:] = tail.astype(BF16)
     w = jnp.concatenate(weight, axis=0)
-    for copy in copies:
+    for copy in copies[:6]:
         copy.wait()
-    first = len(copies)
-    for k, piece in enumerate(pieces):
-        at = (k % count) * CHUNK
-        fetch(piece.at[pl.ds(0, CHUNK)], dense_up.at[k // count, pl.ds(at, CHUNK)])
-        fetch(piece.at[pl.ds(CHUNK, PAD)], dense_down.at[k // count, pl.ds(at, PAD)])
     for k in range(2):
         down_ref[k * lanes + units : (k + 1) * lanes, :] = jnp.zeros(
             (lanes - units, 2 * half), BF16
@@ -121,7 +120,7 @@
     h = w * silu(pre[:, : 2 * lanes]) * pre[:, 2 * lanes :]
     h = jnp.where((iota2((1, 2 * lanes), 1) & (lanes - 1)) < units, h, 0.0).astype(BF16)
     acc_ref[...] = dot(h, down_ref[...])
-    for copy in copies[first:]:
+    for copy in copies[6:]:
         copy.wait()
     for ref in (dense_down.at[0], dense_down.at[1]):
         for k in range(count):
@@ -178,7 +177,7 @@
     return 6 * pair + jnp.where(core == 0, place, crossed)
 
 
-def spread_kernel(core_ref, x_ref, out_ref, rows_ref):
+def spread_kernel(core_ref, x_ref, out_ref, rows_ref, packed_ref, sem):
     core = core_ref[0]
     for k in range(x_ref.shape[0]):
         rows_ref[k * SLOTS : (k + 1) * SLOTS, :] = x_ref[k].astype(F32)
@@ -197,9 +196,15 @@
         weight = weight + jnp.where(lane == g, dot(pick, x[:, width:]), 0.0)
     parts.append(main[:, groups * TAIL : groups * TAIL + 128] + weight)
     parts.append(main[:, groups * TAIL + 128 :])
-    packed = jnp.concatenate(parts, axis=1).astype(BF16)
-    for k in range(out_ref.shape[0]):
-        out_ref[k] = packed
+    packed_ref[...] = jnp.concatenate(parts, axis=1).astype(BF16)
+    copies = [
+        pltpu.make_async_copy(packed_ref, out_ref.at[k], sem.at[k])
+        for k in range(out_ref.shape[0])
+    ]
+    for copy in copies:
+        copy.start()
+    for copy in copies:
+        copy.wait()
 
 
 def spread(core, x, chips):
@@ -207,10 +212,14 @@
     return pl.pallas_call(
         spread_kernel,
         name="spread",
-        out_shape=pltpu.VMEM((chips, ROWS, MAIN), BF16),
+        out_shape=jax.ShapeDtypeStruct((chips, ROWS, MAIN), BF16),
         in_specs=[pl.BlockSpec(memory_space=pltpu.SMEM), vmem],
-        out_specs=vmem,
-        scratch_shapes=[pltpu.VMEM((EXPERTS * SLOTS, x.shape[2]), F32)],
+        out_specs=pl.BlockSpec(memory_space=pl.ANY),
+        scratch_shapes=[
+            pltpu.VMEM((EXPERTS * SLOTS, x.shape[2]), F32),
+            pltpu.VMEM((ROWS, MAIN), BF16),
+            pltpu.SemaphoreType.DMA((chips,)),
+        ],
     )(core.reshape(1), in_vmem(x))
 
 
@@ -258,8 +267,7 @@
     pairs = ((x_hbm, x_ref), (wq_hbm, wq), (wk_hbm, wk), (wv_hbm, wv), (state_hbm, state_ref), (wo_hbm, wo))
     for k, (source, into) in enumerate(pairs):
         loads.append(pltpu.make_async_copy(source, into, load_sem.at[k]))
-    for load in loads[:4]:
-        load.start()
+        loads[-1].start()
     core = core_ref[0]
     here = pl.multiple_of(core * half, half)
     there = pl.multiple_of((1 - core) * half, half)
@@ -276,8 +284,6 @@
         return both.astype(BF16).astype(F32)
 
     loads[1].wait()
-    for load in loads[4:]:
-        load.start()
     query = project(wq)
     loads[2].wait()
     key = project(wk) * head ** (-0.5)
@@ -420,13 +426,10 @@
     )
 
 
-def home_kernel(z_ref, home_ref, after_ref, routes_ref, out_ref, rows_ref):
+def pick_kernel(z_ref, routes_ref, pick_ref):
     odd = z_ref[0] & 1
-    rows = after_ref.shape[0]
-    count = home_ref.shape[0]
-    for k in range(count):
-        rows_ref[k * SLOTS : (k + 1) * SLOTS, :] = home_ref[k].astype(F32)
-    shape = (rows, count * SLOTS)
+    shape = pick_ref.shape
+    rows = shape[0]
     slot = iota2(shape, 1)
     source = divided(slot, 3)
     expert = source >> 1
@@ -434,21 +437,37 @@
     member = (routes_ref[:, 0:1] == expert).astype(F32) + (routes_ref[:, 1:2] == expert).astype(F32)
     earlier = iota2((rows, rows), 1) < iota2((rows, rows), 0)
     place = dot(one_hot(earlier), member.astype(BF16))
-    select = jnp.where(place == slot.astype(F32), member, 0.0).astype(BF16)
-    total = after_ref[...].astype(F32) + dot(select, rows_ref[...].astype(BF16))
+    pick_ref[...] = jnp.where(place == slot.astype(F32), member, 0.0).astype(BF16)
+
+
+def to_pick(z, routes):
+    vmem = pl.BlockSpec(memory_space=pltpu.VMEM)
+    return pl.pallas_call(
+        pick_kernel,
+        name="pick",
+        out_shape=pltpu.VMEM((routes.shape[0], 2 * EXPERTS * SLOTS), BF16),
+        in_specs=[pl.BlockSpec(memory_space=pltpu.SMEM), vmem],
+        out_specs=vmem,
+    )(z.reshape(1), in_vmem(routes))
+
+
+def home_kernel(home_ref, after_ref, pick_ref, out_ref, rows_ref):
+    for k in range(home_ref.shape[0]):
+        rows_ref[k * SLOTS : (k + 1) * SLOTS, :] = home_ref[k].astype(F32)
+    total = after_ref[...].astype(F32) + dot(pick_ref[...], rows_ref[...].astype(BF16))
     out_ref[...] = total.astype(BF16)
 
 
-def at_home(place, home, after, routes):
+def at_home(home, after, pick):
     vmem = pl.BlockSpec(memory_space=pltpu.VMEM)
     return pl.pallas_call(
         home_kernel,
         name="home",
         out_shape=jax.ShapeDtypeStruct(after.shape, BF16),
-        in_specs=[pl.BlockSpec(memory_space=pltpu.SMEM)] + [vmem] * 3,
+        in_specs=[vmem] * 3,
         out_specs=vmem,
         scratch_shapes=[pltpu.VMEM((home.shape[0] * SLOTS, home.shape[2]), F32)],
-    )(place[1].reshape(1), in_vmem(home), in_vmem(after), in_vmem(routes))
+    )(in_vmem(home), in_vmem(after), in_vmem(pick))
 
 
 def layer(
@@ -500,7 +519,7 @@
     back = lax.all_to_all(partial.reshape(chips, ROWS, MAIN), PLANE, 0, 0, tiled=True)
     send = collect(core, back)
     home = lax.all_to_all(send, ("ep_0", "tp"), 0, 0, tiled=True)
-    return (at_home(place, home, after, routes), new_state)
+    return (at_home(home, after, to_pick(place[1], routes)), new_state)
 
 
 def solution(mesh):

time: 118 us -> 117 us (level)
  no operation moved by 1% of the time
where the time goes in v6:
time: 117 us
  blocking collectives  41.5 us (35%)
  starting transfers between devices  35.5 us (30%)
  waiting for transfers between devices  20.9 us (18%)
  Pallas kernels  15.1 us (13%)
  local copies, waits for them, and re-layouts  3.06 us (3%)
    all_to_all x1, blocking collectives, layer(): lax.all_to_all(partial.reshape(chips, ROWS, MAIN), PLANE, 0, 0, tiled=True)  26.7 us
    all_to_all x1, blocking collectives, layer(): at_plane = lax.all_to_all(slot_rows, 'ep_0', 0, 0, tiled=True)  14.8 us
    ppermute x14, starting transfers between devices, swap(): return lax.ppermute(value, 'tp', [(0, 1), (1, 0)])  14.5 us
    all_to_all x1, waiting for transfers between devices, layer(): home = lax.all_to_all(send, ('ep_0', 'tp'), 0, 0, tiled=True)  8.61 us
    ppermute x7, starting transfers between devices, along_z(): lax.ppermute(value, 'ep_0', [(i, (i + shift) % size) for i in range(size)])  8.27 us
    ppermute x7, waiting for transfers between devices, along_z(): lax.ppermute(value, 'ep_0', [(i, (i + shift) % size) for i in range(size)])  8.15 us
    all_to_all x1, starting transfers between devices, layer(): gathered = lax.all_to_all(copies, PLANE, 0, 0, tiled=True)  6.9 us
    pallas_call x1, Pallas kernels, experts_and_dense(): pl.pallas_call(lambda *refs: branch_kernel(hidden, *refs), name='branch',...  5.96 us
  transfers between devices with their start and end apart: 23, of which 8 were waited for; matrix products, arithmetic and copies ran while one was open for 0% of the time, Pallas kernels for 0%

profile of v6, /device:TPU:1, one launch (start us, length us, event | category | flops | bytes accessed | tf_op | source)
XLA Modules:
  0.0 117.1 jit_solution(2364490017557890572)
XLA Ops:
  0.6 3.3 %collective-permute-start = (bf16[16,1024]{1,0:T(8,128)(2,1)}, bf16[16,1024]{1,0:T(8,128)(2,1)S(1)}, u32[]{:S(2)}, u32[]{:S(2)}) collective-permute-start(bf16[16,1024]{1,0:T(8,128)(2,1)} %x_ref.1), channel_id=1, source_target_pairs={{0,1},{1,0},{2,3},{3,2},{4,5},{5,4},{6,7},{7,6},{8,9},{9,8},{10,11... | collective-permute-start | bytes 98312 | tf_op jit(solution)/shard_map/ppermute | solution.py:27
  3.9 1.1 collective-permute-done.y_ref
  5.0 5.3 %mixer.1 = (bf16[16,2048]{1,0:T(8,128)(2,1)S(1)}, f32[16,2,128,128]{3,2,1,0:T(8,128)}) custom-call(s32[1]{0:T(128)} %bitcast.core_ref.refs_0_, bf16[16,1024]{1,0:T(8,128)(2,1)} %x_ref.1, bf16[16,1024]{1,0:T(8,128)(2,1)S(1)} %collective-permute-done.y_ref, f32[1,2048]{1,0:T(1,128)} %bitcast.32, bf16[2048,256]{1,0:T(8,128)(2,1)} %wq_hbm.1, ...), custom_call_target="tpu_custom_call" | custom-call | tf_op jit(solution)/shard_map/mixer/pallas_call | solution.py:334
  10.3 0.5 collective-permute-start.1
  10.8 0.1 collective-permute-start.2
  10.9 1.0 collective-permute-done.2
  12.0 0.3 slots.1
  12.3 14.8 %all_to_all.20.x_ref = bf16[8,3,2176]{2,1,0:T(4,128)(2,1)S(1)} all-to-all(bf16[8,3,2176]{2,1,0:T(4,128)(2,1)S(1)} %get-tuple-element.7), channel_id=1, replica_groups=mesh['ep_0'=8,'ep_1'=4,'ep_2'=4,'tp'=2] {'ep_0'}, dimensions={0} | all-to-all | bytes 208896 | tf_op jit(solution)/shard_map/all_to_all | solution.py:507
  27.1 1.5 %spread.1 = bf16[16,24,1792]{2,1,0:T(8,128)(2,1)} custom-call(s32[1]{0:T(128)} %bitcast.core_ref.refs_0_, bf16[8,3,2176]{2,1,0:T(4,128)(2,1)S(1)} %all_to_all.20.x_ref), custom_call_target="tpu_custom_call" | custom-call | tf_op jit(solution)/shard_map/spread/pallas_call | solution.py:212
  28.6 0.0 copy-start.25
  28.7 0.0 copy-start.26
  28.7 6.9 %all-to-all-start.1 = ((bf16[16,24,1792]{2,1,0:T(8,128)(2,1)}), bf16[16,24,1792]{2,1,0:T(8,128)(2,1)S(1)}, u32[]{:S(2)}, u32[]{:S(2)}) async-start(bf16[16,24,1792]{2,1,0:T(8,128)(2,1)} %spread.1), calls=%async_computation.1 | async-start | bytes 2752512 | tf_op jit(solution)/shard_map/all_to_all | solution.py:515
  35.7 0.1 concatenate.3.refs_8_
  35.8 0.4 collective-permute-start.7
  36.2 3.0 %collective-permute-start.6 = (bf16[72,1024]{1,0:T(8,128)(2,1)S(1)}, bf16[72,1024]{1,0:T(8,128)(2,1)S(1)}, u32[]{:S(2)}, u32[]{:S(2)}) collective-permute-start(bf16[72,1024]{1,0:T(8,128)(2,1)S(1)} %concatenate.3.refs_8_), channel_id=1, source_target_pairs={{0,96},{32,128},{64,160},{96,192},{128,224},{160,0},{192,32},{224,... | collective-permute-start | bytes 442376 | tf_op jit(solution)/shard_map/ppermute | solution.py:32
  39.1 2.0 %collective-permute-start.8 = (bf16[72,1024]{1,0:T(8,128)(2,1)S(1)}, bf16[72,1024]{1,0:T(8,128)(2,1)S(1)}, u32[]{:S(2)}, u32[]{:S(2)}) collective-permute-start(bf16[72,1024]{1,0:T(8,128)(2,1)S(1)} %concatenate.3.refs_8_), channel_id=1, source_target_pairs={{0,192},{32,224},{64,0},{96,32},{128,64},{160,96},{192,128},{224,1... | collective-permute-start | bytes 442376 | tf_op jit(solution)/shard_map/ppermute | solution.py:32
  41.2 0.3 collective-permute-start.9
  41.5 1.2 %collective-permute-start.10 = (bf16[72,1024]{1,0:T(8,128)(2,1)S(1)}, bf16[72,1024]{1,0:T(8,128)(2,1)S(1)}, u32[]{:S(2)}, u32[]{:S(2)}) collective-permute-start(bf16[72,1024]{1,0:T(8,128)(2,1)S(1)} %concatenate.3.refs_8_), channel_id=1, source_target_pairs={{0,32},{32,64},{64,96},{96,128},{128,160},{160,192},{192,224},{224... | collective-permute-start | bytes 442376 | tf_op jit(solution)/shard_map/ppermute | solution.py:32
  42.7 5.7 %collective-permute-done.7.refs_10_ = bf16[72,1024]{1,0:T(8,128)(2,1)S(1)} collective-permute-done((bf16[72,1024]{1,0:T(8,128)(2,1)S(1)}, bf16[72,1024]{1,0:T(8,128)(2,1)S(1)}, u32[]{:S(2)}, u32[]{:S(2)}) %collective-permute-start.7) | collective-permute-done | bytes 147488 | tf_op jit(solution)/shard_map/ppermute | solution.py:32
  48.4 5.7 %collective-permute-start.13 = (bf16[72,1024]{1,0:T(8,128)(2,1)S(1)}, bf16[72,1024]{1,0:T(8,128)(2,1)S(1)}, u32[]{:S(2)}, u32[]{:S(2)}) collective-permute-start(bf16[72,1024]{1,0:T(8,128)(2,1)S(1)} %concatenate.3.refs_8_), channel_id=1, source_target_pairs={{0,1},{1,0},{2,3},{3,2},{4,5},{5,4},{6,7},{7,6},{8,9},{9,8},{10,11... | collective-permute-start | bytes 442376 | tf_op jit(solution)/shard_map/ppermute | solution.py:27
  54.2 1.3 %collective-permute-start.12 = (bf16[72,1024]{1,0:T(8,128)(2,1)S(1)}, bf16[72,1024]{1,0:T(8,128)(2,1)S(1)}, u32[]{:S(2)}, u32[]{:S(2)}) collective-permute-start(bf16[72,1024]{1,0:T(8,128)(2,1)S(1)} %collective-permute-done.7.refs_10_), channel_id=1, source_target_pairs={{0,224},{32,0},{64,32},{96,64},{128,96},{160,128},{192,160},{224,1... | collective-permute-start | bytes 442376 | tf_op jit(solution)/shard_map/ppermute | solution.py:32
  55.5 1.1 collective-permute-done.9.refs_12_
  56.6 0.9 collective-permute-start.15
  57.5 1.4 %collective-permute-done.10.refs_13_ = bf16[72,1024]{1,0:T(8,128)(2,1)S(1)} collective-permute-done((bf16[72,1024]{1,0:T(8,128)(2,1)S(1)}, bf16[72,1024]{1,0:T(8,128)(2,1)S(1)}, u32[]{:S(2)}, u32[]{:S(2)}) %collective-permute-start.10) | collective-permute-done | bytes 147488 | tf_op jit(solution)/shard_map/ppermute | solution.py:32
  58.9 1.9 %collective-permute-start.14 = (bf16[72,1024]{1,0:T(8,128)(2,1)S(1)}, bf16[72,1024]{1,0:T(8,128)(2,1)S(1)}, u32[]{:S(2)}, u32[]{:S(2)}) collective-permute-start(bf16[72,1024]{1,0:T(8,128)(2,1)S(1)} %collective-permute-done.6.refs_9_), channel_id=1, source_target_pairs={{0,1},{1,0},{2,3},{3,2},{4,5},{5,4},{6,7},{7,6},{8,9},{9,8},{10,11... | collective-permute-start | bytes 442376 | tf_op jit(solution)/shard_map/ppermute | solution.py:27
  60.7 0.3 collective-permute-start.16
  61.0 0.7 copy-done.17
  61.7 0.2 collective-permute-start.3
  61.9 0.4 collective-permute-start.4
  62.3 0.7 copy-done.19
  63.0 0.2 collective-permute-start.5
  63.2 0.3 collective-permute-start.17
  63.5 0.2 collective-permute-start.18
  63.7 1.1 collective-permute-done.17.refs_20_
  64.9 0.2 collective-permute-start.19
  65.1 0.3 collective-permute-start.20
  65.4 0.9 collective-permute-done.19.refs_22_
  66.3 0.5 copy-done.24
  66.9 0.1 copy-done.9
  67.0 0.8 copy-done.10
  67.8 6.0 %branch.1 = bf16[384,1792]{1,0:T(8,128)(2,1)S(1)} custom-call(s32[1]{0:T(128)} %bitcast.core_ref.refs_0_, bf16[384,1792]{1,0:T(8,128)(2,1)S(1)} %bitcast.18, bf16[88,2048]{1,0:T(8,128)(2,1)} %bitcast.24, bf16[88,2048]{1,0:T(8,128)(2,1)} %bitcast.26, bf16[88,2048]{1,0:T(8,128)(2,1)} %bitcast.28, bf16[88,2048]{1,0:T(8,128)(2,1)} %copy-done.8, ...), custom_call_target="tpu_custom_call" | custom-call | tf_op jit(solution)/shard_map/branch/pallas_call | solution.py:155
  73.8 26.7 %all_to_all.21.x_ref = bf16[16,24,1792]{2,1,0:T(8,128)(2,1)S(1)} all-to-all(bf16[16,24,1792]{2,1,0:T(8,128)(2,1)S(1)} %bitcast.19), channel_id=1, replica_groups=mesh['ep_0'=8,'ep_1'=4,'ep_2'=4,'tp'=2] {'ep_1','ep_2'}, dimensions={0} | all-to-all | bytes 2752512 | tf_op jit(solution)/shard_map/all_to_all | solution.py:519
  100.5 1.0 collect.1
  101.5 5.9 %all-to-all-start.3 = ((bf16[16,3,1024]{2,1,0:T(4,128)(2,1)}), bf16[16,3,1024]{2,1,0:T(4,128)(2,1)S(1)}, u32[]{:S(2)}, u32[]{:S(2)}) async-start(bf16[16,3,1024]{2,1,0:T(4,128)(2,1)} %collect.1), calls=%async_computation.3 | async-start | bytes 262144 | tf_op jit(solution)/shard_map/all_to_all | solution.py:521
  107.4 0.1 copy.19.routes_ref
  107.5 0.2 pick.1.pick_ref
  107.7 8.6 %all-to-all-done.3.home_ref = bf16[16,3,1024]{2,1,0:T(4,128)(2,1)S(1)} async-done(((bf16[16,3,1024]{2,1,0:T(4,128)(2,1)}), bf16[16,3,1024]{2,1,0:T(4,128)(2,1)S(1)}, u32[]{:S(2)}, u32[]{:S(2)}) %all-to-all-start.3) | async-done | bytes 98336 | tf_op jit(solution)/shard_map/all_to_all | solution.py:521
  116.3 0.8 home.1
  (70 shorter events, 0.2 us)
Async XLA Ops:
  0.6 4.4 %collective-permute-start = (bf16[16,1024]{1,0:T(8,128)(2,1)}, bf16[16,1024]{1,0:T(8,128)(2,1)S(1)}, u32[]{:S(2)}, u32[]{:S(2)}) collective-permute-start(bf16[16,1024]{1,0:T(8,128)(2,1)} %x_ref.1), channel_id=1, source_target_pairs={{0,1},{1,0},{2,3},{3,2},{4,5},{5,4},{6,7},{7,6},{8,9},{9,8},{10,11... | collective-permute-start | bytes 98312 | tf_op jit(solution)/shard_map/ppermute | solution.py:27
  5.0 5.8 %copy-start.2 = (f32[1024]{0:T(1024)S(1)}, f32[1024]{0:T(1024)}, u32[]{:S(2)}) copy-start(f32[1024]{0:T(1024)} %param.24) | copy-start | bytes 12292
  5.0 7.0 %copy-start = (bf16[16,1024]{1,0:T(8,128)(2,1)S(1)}, bf16[16,1024]{1,0:T(8,128)(2,1)}, u32[]{:S(2)}) copy-start(bf16[16,1024]{1,0:T(8,128)(2,1)} %x_ref.1) | copy-start | bytes 98308
  5.0 7.0 %copy-start.1 = (s32[16,2]{0,1:T(2,128)S(1)}, s32[16,2]{0,1:T(2,128)}, u32[]{:S(2)}) copy-start(s32[16,2]{0,1:T(2,128)} %param.32) | copy-start | bytes 388
  5.0 7.0 %copy-start.3 = (bf16[16,2]{0,1:T(2,128)(2,1)S(1)}, bf16[16,2]{0,1:T(2,128)(2,1)}, u32[]{:S(2)}) copy-start(bf16[16,2]{0,1:T(2,128)(2,1)} %param.33) | copy-start | bytes 196
  10.3 1.6 %collective-permute-start.1 = (bf16[16,2048]{1,0:T(8,128)(2,1)S(1)}, bf16[16,2048]{1,0:T(8,128)(2,1)S(1)}, u32[]{:S(2)}, u32[]{:S(2)}) collective-permute-start(bf16[16,2048]{1,0:T(8,128)(2,1)S(1)} %get-tuple-element.6.mix_ref), channel_id=1, source_target_pairs={{0,1},{1,0},{2,3},{3,2},{4,5},{5,4},{6,7},{7,6},{8,9},{9,8},{10,11... | collective-permute-start | bytes 196616 | tf_op jit(solution)/shard_map/ppermute | solution.py:27
  10.8 1.2 collective-permute-start.2
  28.6 7.0 %copy-start.28 = (bf16[1024]{0:T(1024)(128)(2,1)S(1)}, bf16[1024]{0:T(1024)(128)(2,1)}, u32[]{:S(2)}) copy-start(bf16[1024]{0:T(1024)(128)(2,1)} %param.25) | copy-start | bytes 6148
  28.6 7.0 %copy-start.25 = (bf16[1024,22]{0,1:T(8,128)(2,1)S(1)}, bf16[1024,22]{0,1:T(8,128)(2,1)}, u32[]{:S(2)}) copy-start(bf16[1024,22]{0,1:T(8,128)(2,1)} %param.26) | copy-start | bytes 135172
  28.7 7.0 %copy-start.26 = (bf16[1024,22]{0,1:T(8,128)(2,1)S(1)}, bf16[1024,22]{0,1:T(8,128)(2,1)}, u32[]{:S(2)}) copy-start(bf16[1024,22]{0,1:T(8,128)(2,1)} %param.27) | copy-start | bytes 135172
  28.7 7.0 %copy-start.27 = (bf16[22,1024]{1,0:T(8,128)(2,1)S(1)}, bf16[22,1024]{1,0:T(8,128)(2,1)}, u32[]{:S(2)}) copy-start(bf16[22,1024]{1,0:T(8,128)(2,1)} %param.28) | copy-start | bytes 135172
  28.7 33.0 %copy-start.5 = (bf16[1,2048,88]{1,2,0:T(8,128)(2,1)S(1)}, bf16[1,2048,88]{1,2,0:T(8,128)(2,1)}, u32[]{:S(2)}) copy-start(bf16[1,2048,88]{1,2,0:T(8,128)(2,1)} %param.29) | copy-start | bytes 1081348
  28.7 33.2 %copy-start.6 = (bf16[1,2048,88]{1,2,0:T(8,128)(2,1)S(1)}, bf16[1,2048,88]{1,2,0:T(8,128)(2,1)}, u32[]{:S(2)}) copy-start(bf16[1,2048,88]{1,2,0:T(8,128)(2,1)} %param.30) | copy-start | bytes 1081348
  28.7 34.3 %copy-start.7 = (bf16[1,88,2048]{2,1,0:T(8,128)(2,1)S(1)}, bf16[1,88,2048]{2,1,0:T(8,128)(2,1)}, u32[]{:S(2)}) copy-start(bf16[1,88,2048]{2,1,0:T(8,128)(2,1)} %param.31) | copy-start | bytes 1081348
  28.7 39.1 %all-to-all-start.1 = ((bf16[16,24,1792]{2,1,0:T(8,128)(2,1)}), bf16[16,24,1792]{2,1,0:T(8,128)(2,1)S(1)}, u32[]{:S(2)}, u32[]{:S(2)}) async-start(bf16[16,24,1792]{2,1,0:T(8,128)(2,1)} %spread.1), calls=%async_computation.1 | async-start | bytes 2752512 | tf_op jit(solution)/shard_map/all_to_all | solution.py:515
  35.8 32.0 %copy-start.4 = (bf16[72,1024]{1,0:T(8,128)(2,1)}, bf16[72,1024]{1,0:T(8,128)(2,1)S(1)}, u32[]{:S(2)}) copy-start(bf16[72,1024]{1,0:T(8,128)(2,1)S(1)} %concatenate.3.refs_8_) | copy-start | bytes 442372
  35.8 12.6 %collective-permute-start.7 = (bf16[72,1024]{1,0:T(8,128)(2,1)S(1)}, bf16[72,1024]{1,0:T(8,128)(2,1)S(1)}, u32[]{:S(2)}, u32[]{:S(2)}) collective-permute-start(bf16[72,1024]{1,0:T(8,128)(2,1)S(1)} %concatenate.3.refs_8_), channel_id=1, source_target_pairs={{0,160},{32,192},{64,224},{96,0},{128,32},{160,64},{192,96},{224,1... | collective-permute-start | bytes 442376 | tf_op jit(solution)/shard_map/ppermute | solution.py:32
  36.2 12.2 %collective-permute-start.6 = (bf16[72,1024]{1,0:T(8,128)(2,1)S(1)}, bf16[72,1024]{1,0:T(8,128)(2,1)S(1)}, u32[]{:S(2)}, u32[]{:S(2)}) collective-permute-start(bf16[72,1024]{1,0:T(8,128)(2,1)S(1)} %concatenate.3.refs_8_), channel_id=1, source_target_pairs={{0,96},{32,128},{64,160},{96,192},{128,224},{160,0},{192,32},{224,... | collective-permute-start | bytes 442376 | tf_op jit(solution)/shard_map/ppermute | solution.py:32
  39.1 15.0 %collective-permute-start.8 = (bf16[72,1024]{1,0:T(8,128)(2,1)S(1)}, bf16[72,1024]{1,0:T(8,128)(2,1)S(1)}, u32[]{:S(2)}, u32[]{:S(2)}) collective-permute-start(bf16[72,1024]{1,0:T(8,128)(2,1)S(1)} %concatenate.3.refs_8_), channel_id=1, source_target_pairs={{0,192},{32,224},{64,0},{96,32},{128,64},{160,96},{192,128},{224,1... | collective-permute-start | bytes 442376 | tf_op jit(solution)/shard_map/ppermute | solution.py:32
  41.2 15.5 %collective-permute-start.9 = (bf16[72,1024]{1,0:T(8,128)(2,1)S(1)}, bf16[72,1024]{1,0:T(8,128)(2,1)S(1)}, u32[]{:S(2)}, u32[]{:S(2)}) collective-permute-start(bf16[72,1024]{1,0:T(8,128)(2,1)S(1)} %concatenate.3.refs_8_), channel_id=1, source_target_pairs={{0,64},{32,96},{64,128},{96,160},{128,192},{160,224},{192,0},{224,... | collective-permute-start | bytes 442376 | tf_op jit(solution)/shard_map/ppermute | solution.py:32
  41.5 17.3 %collective-permute-start.10 = (bf16[72,1024]{1,0:T(8,128)(2,1)S(1)}, bf16[72,1024]{1,0:T(8,128)(2,1)S(1)}, u32[]{:S(2)}, u32[]{:S(2)}) collective-permute-start(bf16[72,1024]{1,0:T(8,128)(2,1)S(1)} %concatenate.3.refs_8_), channel_id=1, source_target_pairs={{0,32},{32,64},{64,96},{96,128},{128,160},{160,192},{192,224},{224... | collective-permute-start | bytes 442376 | tf_op jit(solution)/shard_map/ppermute | solution.py:32
  48.4 19.4 %copy-start.11 = (bf16[72,1024]{1,0:T(8,128)(2,1)}, bf16[72,1024]{1,0:T(8,128)(2,1)S(1)}, u32[]{:S(2)}) copy-start(bf16[72,1024]{1,0:T(8,128)(2,1)S(1)} %collective-permute-done.7.refs_10_) | copy-start | bytes 442372
  48.4 12.4 %collective-permute-start.11 = (bf16[72,1024]{1,0:T(8,128)(2,1)S(1)}, bf16[72,1024]{1,0:T(8,128)(2,1)S(1)}, u32[]{:S(2)}, u32[]{:S(2)}) collective-permute-start(bf16[72,1024]{1,0:T(8,128)(2,1)S(1)} %concatenate.3.refs_8_), channel_id=1, source_target_pairs={{0,224},{32,0},{64,32},{96,64},{128,96},{160,128},{192,160},{224,1... | collective-permute-start | bytes 442376 | tf_op jit(solution)/shard_map/ppermute | solution.py:32
  48.4 19.4 %copy-start.12 = (bf16[72,1024]{1,0:T(8,128)(2,1)}, bf16[72,1024]{1,0:T(8,128)(2,1)S(1)}, u32[]{:S(2)}) copy-start(bf16[72,1024]{1,0:T(8,128)(2,1)S(1)} %collective-permute-done.6.refs_9_) | copy-start | bytes 442372
  48.4 12.6 %collective-permute-start.13 = (bf16[72,1024]{1,0:T(8,128)(2,1)S(1)}, bf16[72,1024]{1,0:T(8,128)(2,1)S(1)}, u32[]{:S(2)}, u32[]{:S(2)}) collective-permute-start(bf16[72,1024]{1,0:T(8,128)(2,1)S(1)} %concatenate.3.refs_8_), channel_id=1, source_target_pairs={{0,1},{1,0},{2,3},{3,2},{4,5},{5,4},{6,7},{7,6},{8,9},{9,8},{10,11... | collective-permute-start | bytes 442376 | tf_op jit(solution)/shard_map/ppermute | solution.py:27
  54.1 13.6 %copy-start.13 = (bf16[72,1024]{1,0:T(8,128)(2,1)}, bf16[72,1024]{1,0:T(8,128)(2,1)S(1)}, u32[]{:S(2)}) copy-start(bf16[72,1024]{1,0:T(8,128)(2,1)S(1)} %collective-permute-done.8.refs_11_) | copy-start | bytes 442372
  54.2 7.8 %collective-permute-start.12 = (bf16[72,1024]{1,0:T(8,128)(2,1)S(1)}, bf16[72,1024]{1,0:T(8,128)(2,1)S(1)}, u32[]{:S(2)}, u32[]{:S(2)}) collective-permute-start(bf16[72,1024]{1,0:T(8,128)(2,1)S(1)} %collective-permute-done.7.refs_10_), channel_id=1, source_target_pairs={{0,224},{32,0},{64,32},{96,64},{128,96},{160,128},{192,160},{224,1... | collective-permute-start | bytes 442376 | tf_op jit(solution)/shard_map/ppermute | solution.py:32
  56.6 9.6 %copy-start.14 = (bf16[72,1024]{1,0:T(8,128)(2,1)}, bf16[72,1024]{1,0:T(8,128)(2,1)S(1)}, u32[]{:S(2)}) copy-start(bf16[72,1024]{1,0:T(8,128)(2,1)S(1)} %collective-permute-done.9.refs_12_) | copy-start | bytes 442372
  56.6 5.7 %collective-permute-start.15 = (bf16[72,1024]{1,0:T(8,128)(2,1)S(1)}, bf16[72,1024]{1,0:T(8,128)(2,1)S(1)}, u32[]{:S(2)}, u32[]{:S(2)}) collective-permute-start(bf16[72,1024]{1,0:T(8,128)(2,1)S(1)} %collective-permute-done.7.refs_10_), channel_id=1, source_target_pairs={{0,1},{1,0},{2,3},{3,2},{4,5},{5,4},{6,7},{7,6},{8,9},{9,8},{10,11... | collective-permute-start | bytes 442376 | tf_op jit(solution)/shard_map/ppermute | solution.py:27
  58.9 7.4 %copy-start.15 = (bf16[72,1024]{1,0:T(8,128)(2,1)}, bf16[72,1024]{1,0:T(8,128)(2,1)S(1)}, u32[]{:S(2)}) copy-start(bf16[72,1024]{1,0:T(8,128)(2,1)S(1)} %collective-permute-done.10.refs_13_) | copy-start | bytes 442372
  58.9 4.3 %collective-permute-start.14 = (bf16[72,1024]{1,0:T(8,128)(2,1)S(1)}, bf16[72,1024]{1,0:T(8,128)(2,1)S(1)}, u32[]{:S(2)}, u32[]{:S(2)}) collective-permute-start(bf16[72,1024]{1,0:T(8,128)(2,1)S(1)} %collective-permute-done.6.refs_9_), channel_id=1, source_target_pairs={{0,1},{1,0},{2,3},{3,2},{4,5},{5,4},{6,7},{7,6},{8,9},{9,8},{10,11... | collective-permute-start | bytes 442376 | tf_op jit(solution)/shard_map/ppermute | solution.py:27
  60.7 5.5 %copy-start.16 = (bf16[72,1024]{1,0:T(8,128)(2,1)}, bf16[72,1024]{1,0:T(8,128)(2,1)S(1)}, u32[]{:S(2)}) copy-start(bf16[72,1024]{1,0:T(8,128)(2,1)S(1)} %collective-permute-done.11.refs_14_) | copy-start | bytes 442372
  60.7 2.7 %collective-permute-start.16 = (bf16[72,1024]{1,0:T(8,128)(2,1)S(1)}, bf16[72,1024]{1,0:T(8,128)(2,1)S(1)}, u32[]{:S(2)}, u32[]{:S(2)}) collective-permute-start(bf16[72,1024]{1,0:T(8,128)(2,1)S(1)} %collective-permute-done.8.refs_11_), channel_id=1, source_target_pairs={{0,1},{1,0},{2,3},{3,2},{4,5},{5,4},{6,7},{7,6},{8,9},{9,8},{10,11... | collective-permute-start | bytes 442376 | tf_op jit(solution)/shard_map/ppermute | solution.py:27
  61.7 4.5 %collective-permute-start.3 = (bf16[88,2048]{1,0:T(8,128)(2,1)S(1)}, bf16[88,2048]{1,0:T(8,128)(2,1)S(1)}, u32[]{:S(2)}, u32[]{:S(2)}) collective-permute-start(bf16[88,2048]{1,0:T(8,128)(2,1)S(1)} %bitcast.25), channel_id=1, source_target_pairs={{0,1},{1,0},{2,3},{3,2},{4,5},{5,4},{6,7},{7,6},{8,9},{9,8},{10,11... | collective-permute-start | bytes 1081352 | tf_op jit(solution)/shard_map/ppermute | solution.py:27
  61.9 4.4 %copy-start.18 = (bf16[72,1024]{1,0:T(8,128)(2,1)}, bf16[72,1024]{1,0:T(8,128)(2,1)S(1)}, u32[]{:S(2)}) copy-start(bf16[72,1024]{1,0:T(8,128)(2,1)S(1)} %collective-permute-done.12.refs_15_) | copy-start | bytes 442372
  61.9 4.3 %collective-permute-start.4 = (bf16[88,2048]{1,0:T(8,128)(2,1)S(1)}, bf16[88,2048]{1,0:T(8,128)(2,1)S(1)}, u32[]{:S(2)}, u32[]{:S(2)}) collective-permute-start(bf16[88,2048]{1,0:T(8,128)(2,1)S(1)} %bitcast.27), channel_id=1, source_target_pairs={{0,1},{1,0},{2,3},{3,2},{4,5},{5,4},{6,7},{7,6},{8,9},{9,8},{10,11... | collective-permute-start | bytes 1081352 | tf_op jit(solution)/shard_map/ppermute | solution.py:27
  63.0 3.3 %collective-permute-start.5 = (bf16[88,2048]{1,0:T(8,128)(2,1)S(1)}, bf16[88,2048]{1,0:T(8,128)(2,1)S(1)}, u32[]{:S(2)}, u32[]{:S(2)}) collective-permute-start(bf16[88,2048]{1,0:T(8,128)(2,1)S(1)} %bitcast.29), channel_id=1, source_target_pairs={{0,1},{1,0},{2,3},{3,2},{4,5},{5,4},{6,7},{7,6},{8,9},{9,8},{10,11... | collective-permute-start | bytes 1081352 | tf_op jit(solution)/shard_map/ppermute | solution.py:27
  63.2 3.1 %copy-start.20 = (bf16[72,1024]{1,0:T(8,128)(2,1)}, bf16[72,1024]{1,0:T(8,128)(2,1)S(1)}, u32[]{:S(2)}) copy-start(bf16[72,1024]{1,0:T(8,128)(2,1)S(1)} %collective-permute-done.14.refs_17_) | copy-start | bytes 442372
  63.2 1.7 %collective-permute-start.17 = (bf16[72,1024]{1,0:T(8,128)(2,1)S(1)}, bf16[72,1024]{1,0:T(8,128)(2,1)S(1)}, u32[]{:S(2)}, u32[]{:S(2)}) collective-permute-start(bf16[72,1024]{1,0:T(8,128)(2,1)S(1)} %collective-permute-done.9.refs_12_), channel_id=1, source_target_pairs={{0,1},{1,0},{2,3},{3,2},{4,5},{5,4},{6,7},{7,6},{8,9},{9,8},{10,11... | collective-permute-start | bytes 442376 | tf_op jit(solution)/shard_map/ppermute | solution.py:27
  63.5 2.8 %copy-start.21 = (bf16[72,1024]{1,0:T(8,128)(2,1)}, bf16[72,1024]{1,0:T(8,128)(2,1)S(1)}, u32[]{:S(2)}) copy-start(bf16[72,1024]{1,0:T(8,128)(2,1)S(1)} %collective-permute-done.16.refs_19_) | copy-start | bytes 442372
  63.5 1.6 %collective-permute-start.18 = (bf16[72,1024]{1,0:T(8,128)(2,1)S(1)}, bf16[72,1024]{1,0:T(8,128)(2,1)S(1)}, u32[]{:S(2)}, u32[]{:S(2)}) collective-permute-start(bf16[72,1024]{1,0:T(8,128)(2,1)S(1)} %collective-permute-done.10.refs_13_), channel_id=1, source_target_pairs={{0,1},{1,0},{2,3},{3,2},{4,5},{5,4},{6,7},{7,6},{8,9},{9,8},{10,11... | collective-permute-start | bytes 442376 | tf_op jit(solution)/shard_map/ppermute | solution.py:27
  64.8 1.5 %copy-start.22 = (bf16[72,1024]{1,0:T(8,128)(2,1)}, bf16[72,1024]{1,0:T(8,128)(2,1)S(1)}, u32[]{:S(2)}) copy-start(bf16[72,1024]{1,0:T(8,128)(2,1)S(1)} %collective-permute-done.17.refs_20_) | copy-start | bytes 442372
  64.9 1.4 %collective-permute-start.19 = (bf16[72,1024]{1,0:T(8,128)(2,1)S(1)}, bf16[72,1024]{1,0:T(8,128)(2,1)S(1)}, u32[]{:S(2)}, u32[]{:S(2)}) collective-permute-start(bf16[72,1024]{1,0:T(8,128)(2,1)S(1)} %collective-permute-done.11.refs_14_), channel_id=1, source_target_pairs={{0,1},{1,0},{2,3},{3,2},{4,5},{5,4},{6,7},{7,6},{8,9},{9,8},{10,11... | collective-permute-start | bytes 442376 | tf_op jit(solution)/shard_map/ppermute | solution.py:27
  65.1 1.2 %copy-start.23 = (bf16[72,1024]{1,0:T(8,128)(2,1)}, bf16[72,1024]{1,0:T(8,128)(2,1)S(1)}, u32[]{:S(2)}) copy-start(bf16[72,1024]{1,0:T(8,128)(2,1)S(1)} %collective-permute-done.18.refs_21_) | copy-start | bytes 442372
  65.1 2.7 %collective-permute-start.20 = (bf16[72,1024]{1,0:T(8,128)(2,1)S(1)}, bf16[72,1024]{1,0:T(8,128)(2,1)}, u32[]{:S(2)}, u32[]{:S(2)}) collective-permute-start(bf16[72,1024]{1,0:T(8,128)(2,1)S(1)} %collective-permute-done.12.refs_15_), channel_id=1, source_target_pairs={{0,1},{1,0},{2,3},{3,2},{4,5},{5,4},{6,7},{7,6},{8,9},{9,8},{10,11... | collective-permute-start | bytes 442376 | tf_op jit(solution)/shard_map/ppermute | solution.py:27
  66.2 1.6 %copy-start.8 = (bf16[88,2048]{1,0:T(8,128)(2,1)}, bf16[88,2048]{1,0:T(8,128)(2,1)S(1)}, u32[]{:S(2)}) copy-start(bf16[88,2048]{1,0:T(8,128)(2,1)S(1)} %collective-permute-done.3.refs_5_) | copy-start | bytes 1081348
  66.2 0.8 copy-start.9
  101.5 14.8 %all-to-all-start.3 = ((bf16[16,3,1024]{2,1,0:T(4,128)(2,1)}), bf16[16,3,1024]{2,1,0:T(4,128)(2,1)S(1)}, u32[]{:S(2)}, u32[]{:S(2)}) async-start(bf16[16,3,1024]{2,1,0:T(4,128)(2,1)} %collect.1), calls=%async_computation.3 | async-start | bytes 262144 | tf_op jit(solution)/shard_map/all_to_all | solution.py:521
  (4 other events, 2.7 us)

commit v7 on v5

--- a/solution.py
+++ b/solution.py
@@ -84,6 +84,10 @@
             fetch(weights[k], up_ref.at[pl.ds(place * lanes, units)])
     for k, place in ((2, 0), (5, 1)):
         fetch(weights[k], down_ref.at[pl.ds(place * lanes, units)])
+    for k, piece in enumerate(pieces):
+        at = (k % count) * CHUNK
+        fetch(piece.at[pl.ds(0, CHUNK)], dense_up.at[k // count, pl.ds(at, CHUNK)])
+        fetch(piece.at[pl.ds(CHUNK, PAD)], dense_down.at[k // count, pl.ds(at, PAD)])
     core = core_ref[0]
     here = pl.multiple_of(core * half, half)
     there = pl.multiple_of((1 - core) * half, half)
@@ -106,13 +110,8 @@
         full_ref[band, :MAIN] = x_ref[band, :]
         full_ref[band, MAIN:] = tail.astype(BF16)
     w = jnp.concatenate(weight, axis=0)
-    for copy in copies:
+    for copy in copies[:6]:
         copy.wait()
-    first = len(copies)
-    for k, piece in enumerate(pieces):
-        at = (k % count) * CHUNK
-        fetch(piece.at[pl.ds(0, CHUNK)], dense_up.at[k // count, pl.ds(at, CHUNK)])
-        fetch(piece.at[pl.ds(CHUNK, PAD)], dense_down.at[k // count, pl.ds(at, PAD)])
     for k in range(2):
         down_ref[k * lanes + units : (k + 1) * lanes, :] = jnp.zeros(
             (lanes - units, 2 * half), BF16
@@ -121,7 +120,7 @@
     h = w * silu(pre[:, : 2 * lanes]) * pre[:, 2 * lanes :]
     h = jnp.where((iota2((1, 2 * lanes), 1) & (lanes - 1)) < units, h, 0.0).astype(BF16)
     acc_ref[...] = dot(h, down_ref[...])
-    for copy in copies[first:]:
+    for copy in copies[6:]:
         copy.wait()
     for ref in (dense_down.at[0], dense_down.at[1]):
         for k in range(count):
@@ -258,8 +257,7 @@
     pairs = ((x_hbm, x_ref), (wq_hbm, wq), (wk_hbm, wk), (wv_hbm, wv), (state_hbm, state_ref), (wo_hbm, wo))
     for k, (source, into) in enumerate(pairs):
         loads.append(pltpu.make_async_copy(source, into, load_sem.at[k]))
-    for load in loads[:4]:
-        load.start()
+        loads[-1].start()
     core = core_ref[0]
     here = pl.multiple_of(core * half, half)
     there = pl.multiple_of((1 - core) * half, half)
@@ -276,8 +274,6 @@
         return both.astype(BF16).astype(F32)
 
     loads[1].wait()
-    for load in loads[4:]:
-        load.start()
     query = project(wq)
     loads[2].wait()
     key = project(wk) * head ** (-0.5)

time: 118 us -> 117 us (level)
  no operation moved by 1% of the time
where the time goes in v7:
time: 117 us
  blocking collectives  41.5 us (35%)
  starting transfers between devices  35.6 us (30%)
  waiting for transfers between devices  21.1 us (18%)
  Pallas kernels  15 us (13%)
  local copies, waits for them, and re-layouts  3.05 us (3%)
    all_to_all x1, blocking collectives, layer(): lax.all_to_all(partial.reshape(chips, ROWS, MAIN), PLANE, 0, 0, tiled=True)  26.7 us
    all_to_all x1, blocking collectives, layer(): at_plane = lax.all_to_all(slot_rows, 'ep_0', 0, 0, tiled=True)  14.8 us
    ppermute x14, starting transfers between devices, swap(): return lax.ppermute(value, 'tp', [(0, 1), (1, 0)])  14.5 us
    all_to_all x1, waiting for transfers between devices, layer(): home = lax.all_to_all(send, ('ep_0', 'tp'), 0, 0, tiled=True)  8.8 us
    ppermute x7, starting transfers between devices, along_z(): lax.ppermute(value, 'ep_0', [(i, (i + shift) % size) for i in range(size)])  8.28 us
    ppermute x7, waiting for transfers between devices, along_z(): lax.ppermute(value, 'ep_0', [(i, (i + shift) % size) for i in range(size)])  8.15 us
    all_to_all x1, starting transfers between devices, layer(): gathered = lax.all_to_all(copies, PLANE, 0, 0, tiled=True)  6.9 us
    pallas_call x1, Pallas kernels, experts_and_dense(): pl.pallas_call(lambda *refs: branch_kernel(hidden, *refs), name='branch',...  5.94 us
  transfers between devices with their start and end apart: 23, of which 8 were waited for; matrix products, arithmetic and copies ran while one was open for 0% of the time, Pallas kernels for 0%

profile of v7, /device:TPU:1, one launch (start us, length us, event | category | flops | bytes accessed | tf_op | source)
XLA Modules:
  0.0 117.1 jit_solution(371383434110373717)
XLA Ops:
  0.6 3.3 %collective-permute-start = (bf16[16,1024]{1,0:T(8,128)(2,1)}, bf16[16,1024]{1,0:T(8,128)(2,1)S(1)}, u32[]{:S(2)}, u32[]{:S(2)}) collective-permute-start(bf16[16,1024]{1,0:T(8,128)(2,1)} %x_ref.1), channel_id=1, source_target_pairs={{0,1},{1,0},{2,3},{3,2},{4,5},{5,4},{6,7},{7,6},{8,9},{9,8},{10,11... | collective-permute-start | bytes 98312 | tf_op jit(solution)/shard_map/ppermute | solution.py:27
  3.9 1.1 collective-permute-done.y_ref
  5.0 5.3 %mixer.1 = (bf16[16,2048]{1,0:T(8,128)(2,1)S(1)}, f32[16,2,128,128]{3,2,1,0:T(8,128)}) custom-call(s32[1]{0:T(128)} %bitcast.1.core_ref.refs_0_, bf16[16,1024]{1,0:T(8,128)(2,1)} %x_ref.1, bf16[16,1024]{1,0:T(8,128)(2,1)S(1)} %collective-permute-done.y_ref, f32[1,2048]{1,0:T(1,128)} %bitcast.32, bf16[2048,256]{1,0:T(8,128)(2,1)} %wq_hbm.1, ...), custom_call_target="tpu_custom_call" | custom-call | tf_op jit(solution)/shard_map/mixer/pallas_call | solution.py:324
  10.3 0.5 collective-permute-start.1
  10.8 0.1 collective-permute-start.2
  10.9 1.0 collective-permute-done.2
  12.0 0.3 slots.1
  12.3 14.8 %all_to_all.20.x_ref = bf16[8,3,2176]{2,1,0:T(4,128)(2,1)S(1)} all-to-all(bf16[8,3,2176]{2,1,0:T(4,128)(2,1)S(1)} %get-tuple-element.7), channel_id=1, replica_groups=mesh['ep_0'=8,'ep_1'=4,'ep_2'=4,'tp'=2] {'ep_0'}, dimensions={0} | all-to-all | bytes 208896 | tf_op jit(solution)/shard_map/all_to_all | solution.py:484
  27.1 1.4 %spread.1 = bf16[16,24,1792]{2,1,0:T(8,128)(2,1)} custom-call(s32[1]{0:T(128)} %bitcast.1.core_ref.refs_0_, bf16[8,3,2176]{2,1,0:T(4,128)(2,1)S(1)} %all_to_all.20.x_ref), custom_call_target="tpu_custom_call" | custom-call | tf_op jit(solution)/shard_map/spread/pallas_call | solution.py:206
  28.5 0.0 copy-start.5
  28.6 0.0 copy-start.6
  28.6 0.0 copy-start.7
  28.6 6.9 %all-to-all-start.1 = ((bf16[16,24,1792]{2,1,0:T(8,128)(2,1)}), bf16[16,24,1792]{2,1,0:T(8,128)(2,1)S(1)}, u32[]{:S(2)}, u32[]{:S(2)}) async-start(bf16[16,24,1792]{2,1,0:T(8,128)(2,1)} %spread.1), calls=%async_computation.1 | async-start | bytes 2752512 | tf_op jit(solution)/shard_map/all_to_all | solution.py:492
  35.6 0.1 concatenate.3.refs_8_
  35.7 0.4 collective-permute-start.7
  36.1 3.0 %collective-permute-start.6 = (bf16[72,1024]{1,0:T(8,128)(2,1)S(1)}, bf16[72,1024]{1,0:T(8,128)(2,1)S(1)}, u32[]{:S(2)}, u32[]{:S(2)}) collective-permute-start(bf16[72,1024]{1,0:T(8,128)(2,1)S(1)} %concatenate.3.refs_8_), channel_id=1, source_target_pairs={{0,96},{32,128},{64,160},{96,192},{128,224},{160,0},{192,32},{224,... | collective-permute-start | bytes 442376 | tf_op jit(solution)/shard_map/ppermute | solution.py:32
  39.0 2.0 %collective-permute-start.8 = (bf16[72,1024]{1,0:T(8,128)(2,1)S(1)}, bf16[72,1024]{1,0:T(8,128)(2,1)S(1)}, u32[]{:S(2)}, u32[]{:S(2)}) collective-permute-start(bf16[72,1024]{1,0:T(8,128)(2,1)S(1)} %concatenate.3.refs_8_), channel_id=1, source_target_pairs={{0,192},{32,224},{64,0},{96,32},{128,64},{160,96},{192,128},{224,1... | collective-permute-start | bytes 442376 | tf_op jit(solution)/shard_map/ppermute | solution.py:32
  41.0 0.3 collective-permute-start.9
  41.4 1.2 %collective-permute-start.10 = (bf16[72,1024]{1,0:T(8,128)(2,1)S(1)}, bf16[72,1024]{1,0:T(8,128)(2,1)S(1)}, u32[]{:S(2)}, u32[]{:S(2)}) collective-permute-start(bf16[72,1024]{1,0:T(8,128)(2,1)S(1)} %concatenate.3.refs_8_), channel_id=1, source_target_pairs={{0,32},{32,64},{64,96},{96,128},{128,160},{160,192},{192,224},{224... | collective-permute-start | bytes 442376 | tf_op jit(solution)/shard_map/ppermute | solution.py:32
  42.6 5.7 %collective-permute-done.7.refs_10_ = bf16[72,1024]{1,0:T(8,128)(2,1)S(1)} collective-permute-done((bf16[72,1024]{1,0:T(8,128)(2,1)S(1)}, bf16[72,1024]{1,0:T(8,128)(2,1)S(1)}, u32[]{:S(2)}, u32[]{:S(2)}) %collective-permute-start.7) | collective-permute-done | bytes 147488 | tf_op jit(solution)/shard_map/ppermute | solution.py:32
  48.3 5.7 %collective-permute-start.13 = (bf16[72,1024]{1,0:T(8,128)(2,1)S(1)}, bf16[72,1024]{1,0:T(8,128)(2,1)S(1)}, u32[]{:S(2)}, u32[]{:S(2)}) collective-permute-start(bf16[72,1024]{1,0:T(8,128)(2,1)S(1)} %concatenate.3.refs_8_), channel_id=1, source_target_pairs={{0,1},{1,0},{2,3},{3,2},{4,5},{5,4},{6,7},{7,6},{8,9},{9,8},{10,11... | collective-permute-start | bytes 442376 | tf_op jit(solution)/shard_map/ppermute | solution.py:27
  54.0 1.4 %collective-permute-start.12 = (bf16[72,1024]{1,0:T(8,128)(2,1)S(1)}, bf16[72,1024]{1,0:T(8,128)(2,1)S(1)}, u32[]{:S(2)}, u32[]{:S(2)}) collective-permute-start(bf16[72,1024]{1,0:T(8,128)(2,1)S(1)} %collective-permute-done.7.refs_10_), channel_id=1, source_target_pairs={{0,224},{32,0},{64,32},{96,64},{128,96},{160,128},{192,160},{224,1... | collective-permute-start | bytes 442376 | tf_op jit(solution)/shard_map/ppermute | solution.py:32
  55.4 1.1 collective-permute-done.9.refs_12_
  56.5 0.9 collective-permute-start.15
  57.4 1.4 %collective-permute-done.10.refs_13_ = bf16[72,1024]{1,0:T(8,128)(2,1)S(1)} collective-permute-done((bf16[72,1024]{1,0:T(8,128)(2,1)S(1)}, bf16[72,1024]{1,0:T(8,128)(2,1)S(1)}, u32[]{:S(2)}, u32[]{:S(2)}) %collective-permute-start.10) | collective-permute-done | bytes 147488 | tf_op jit(solution)/shard_map/ppermute | solution.py:32
  58.7 1.9 %collective-permute-start.14 = (bf16[72,1024]{1,0:T(8,128)(2,1)S(1)}, bf16[72,1024]{1,0:T(8,128)(2,1)S(1)}, u32[]{:S(2)}, u32[]{:S(2)}) collective-permute-start(bf16[72,1024]{1,0:T(8,128)(2,1)S(1)} %collective-permute-done.6.refs_9_), channel_id=1, source_target_pairs={{0,1},{1,0},{2,3},{3,2},{4,5},{5,4},{6,7},{7,6},{8,9},{9,8},{10,11... | collective-permute-start | bytes 442376 | tf_op jit(solution)/shard_map/ppermute | solution.py:27
  60.6 0.3 collective-permute-start.16
  60.9 0.7 copy-done.17
  61.6 0.2 collective-permute-start.3
  61.8 0.4 collective-permute-start.4
  62.2 0.7 copy-done.19
  62.8 0.2 collective-permute-start.5
  63.1 0.3 collective-permute-start.17
  63.4 0.2 collective-permute-start.18
  63.6 1.1 collective-permute-done.17.refs_20_
  64.7 0.2 collective-permute-start.19
  65.0 0.3 collective-permute-start.20
  65.2 0.9 collective-permute-done.19.refs_22_
  66.2 0.5 copy-done.24
  66.7 0.1 copy-done.9
  66.9 0.8 copy-done.10
  67.7 5.9 %branch.1 = bf16[384,1792]{1,0:T(8,128)(2,1)S(1)} custom-call(s32[1]{0:T(128)} %bitcast.1.core_ref.refs_0_, bf16[384,1792]{1,0:T(8,128)(2,1)S(1)} %bitcast.18, bf16[88,2048]{1,0:T(8,128)(2,1)} %bitcast.24, bf16[88,2048]{1,0:T(8,128)(2,1)} %bitcast.26, bf16[88,2048]{1,0:T(8,128)(2,1)} %bitcast.28, bf16[88,2048]{1,0:T(8,128)(2,1)} %copy-done.8, ...), custom_call_target="tpu_custom_call" | custom-call | tf_op jit(solution)/shard_map/branch/pallas_call | solution.py:155
  73.6 26.7 %all_to_all.21.x_ref = bf16[16,24,1792]{2,1,0:T(8,128)(2,1)S(1)} all-to-all(bf16[16,24,1792]{2,1,0:T(8,128)(2,1)S(1)} %bitcast.19), channel_id=1, replica_groups=mesh['ep_0'=8,'ep_1'=4,'ep_2'=4,'tp'=2] {'ep_1','ep_2'}, dimensions={0} | all-to-all | bytes 2752512 | tf_op jit(solution)/shard_map/all_to_all | solution.py:496
  100.4 1.0 collect.1
  101.4 5.9 %all-to-all-start.3 = ((bf16[16,3,1024]{2,1,0:T(4,128)(2,1)}), bf16[16,3,1024]{2,1,0:T(4,128)(2,1)S(1)}, u32[]{:S(2)}, u32[]{:S(2)}) async-start(bf16[16,3,1024]{2,1,0:T(4,128)(2,1)} %collect.1), calls=%async_computation.3 | async-start | bytes 262144 | tf_op jit(solution)/shard_map/all_to_all | solution.py:498
  107.3 0.1 copy.19.routes_ref
  107.4 8.8 %all-to-all-done.3.home_ref = bf16[16,3,1024]{2,1,0:T(4,128)(2,1)S(1)} async-done(((bf16[16,3,1024]{2,1,0:T(4,128)(2,1)}), bf16[16,3,1024]{2,1,0:T(4,128)(2,1)S(1)}, u32[]{:S(2)}, u32[]{:S(2)}) %all-to-all-start.3) | async-done | bytes 98336 | tf_op jit(solution)/shard_map/all_to_all | solution.py:498
  116.2 0.9 home.1
  (69 shorter events, 0.2 us)
Async XLA Ops:
  0.6 4.4 %collective-permute-start = (bf16[16,1024]{1,0:T(8,128)(2,1)}, bf16[16,1024]{1,0:T(8,128)(2,1)S(1)}, u32[]{:S(2)}, u32[]{:S(2)}) collective-permute-start(bf16[16,1024]{1,0:T(8,128)(2,1)} %x_ref.1), channel_id=1, source_target_pairs={{0,1},{1,0},{2,3},{3,2},{4,5},{5,4},{6,7},{7,6},{8,9},{9,8},{10,11... | collective-permute-start | bytes 98312 | tf_op jit(solution)/shard_map/ppermute | solution.py:27
  5.0 5.8 %copy-start.2 = (f32[1024]{0:T(1024)S(1)}, f32[1024]{0:T(1024)}, u32[]{:S(2)}) copy-start(f32[1024]{0:T(1024)} %param.24) | copy-start | bytes 12292
  5.0 7.0 %copy-start = (bf16[16,1024]{1,0:T(8,128)(2,1)S(1)}, bf16[16,1024]{1,0:T(8,128)(2,1)}, u32[]{:S(2)}) copy-start(bf16[16,1024]{1,0:T(8,128)(2,1)} %x_ref.1) | copy-start | bytes 98308
  5.0 7.0 %copy-start.1 = (s32[16,2]{0,1:T(2,128)S(1)}, s32[16,2]{0,1:T(2,128)}, u32[]{:S(2)}) copy-start(s32[16,2]{0,1:T(2,128)} %param.32) | copy-start | bytes 388
  5.0 7.0 %copy-start.3 = (bf16[16,2]{0,1:T(2,128)(2,1)S(1)}, bf16[16,2]{0,1:T(2,128)(2,1)}, u32[]{:S(2)}) copy-start(bf16[16,2]{0,1:T(2,128)(2,1)} %param.33) | copy-start | bytes 196
  10.3 1.6 %collective-permute-start.1 = (bf16[16,2048]{1,0:T(8,128)(2,1)S(1)}, bf16[16,2048]{1,0:T(8,128)(2,1)S(1)}, u32[]{:S(2)}, u32[]{:S(2)}) collective-permute-start(bf16[16,2048]{1,0:T(8,128)(2,1)S(1)} %get-tuple-element.6.mix_ref), channel_id=1, source_target_pairs={{0,1},{1,0},{2,3},{3,2},{4,5},{5,4},{6,7},{7,6},{8,9},{9,8},{10,11... | collective-permute-start | bytes 196616 | tf_op jit(solution)/shard_map/ppermute | solution.py:27
  10.8 1.2 collective-permute-start.2
  28.5 7.0 %copy-start.28 = (bf16[1024]{0:T(1024)(128)(2,1)S(1)}, bf16[1024]{0:T(1024)(128)(2,1)}, u32[]{:S(2)}) copy-start(bf16[1024]{0:T(1024)(128)(2,1)} %param.25) | copy-start | bytes 6148
  28.5 7.0 %copy-start.25 = (bf16[1024,22]{0,1:T(8,128)(2,1)S(1)}, bf16[1024,22]{0,1:T(8,128)(2,1)}, u32[]{:S(2)}) copy-start(bf16[1024,22]{0,1:T(8,128)(2,1)} %param.26) | copy-start | bytes 135172
  28.5 7.0 %copy-start.26 = (bf16[1024,22]{0,1:T(8,128)(2,1)S(1)}, bf16[1024,22]{0,1:T(8,128)(2,1)}, u32[]{:S(2)}) copy-start(bf16[1024,22]{0,1:T(8,128)(2,1)} %param.27) | copy-start | bytes 135172
  28.5 7.0 %copy-start.27 = (bf16[22,1024]{1,0:T(8,128)(2,1)S(1)}, bf16[22,1024]{1,0:T(8,128)(2,1)}, u32[]{:S(2)}) copy-start(bf16[22,1024]{1,0:T(8,128)(2,1)} %param.28) | copy-start | bytes 135172
  28.5 33.0 %copy-start.5 = (bf16[1,2048,88]{1,2,0:T(8,128)(2,1)S(1)}, bf16[1,2048,88]{1,2,0:T(8,128)(2,1)}, u32[]{:S(2)}) copy-start(bf16[1,2048,88]{1,2,0:T(8,128)(2,1)} %param.29) | copy-start | bytes 1081348
  28.6 33.2 %copy-start.6 = (bf16[1,2048,88]{1,2,0:T(8,128)(2,1)S(1)}, bf16[1,2048,88]{1,2,0:T(8,128)(2,1)}, u32[]{:S(2)}) copy-start(bf16[1,2048,88]{1,2,0:T(8,128)(2,1)} %param.30) | copy-start | bytes 1081348
  28.6 34.3 %copy-start.7 = (bf16[1,88,2048]{2,1,0:T(8,128)(2,1)S(1)}, bf16[1,88,2048]{2,1,0:T(8,128)(2,1)}, u32[]{:S(2)}) copy-start(bf16[1,88,2048]{2,1,0:T(8,128)(2,1)} %param.31) | copy-start | bytes 1081348
  28.6 39.1 %all-to-all-start.1 = ((bf16[16,24,1792]{2,1,0:T(8,128)(2,1)}), bf16[16,24,1792]{2,1,0:T(8,128)(2,1)S(1)}, u32[]{:S(2)}, u32[]{:S(2)}) async-start(bf16[16,24,1792]{2,1,0:T(8,128)(2,1)} %spread.1), calls=%async_computation.1 | async-start | bytes 2752512 | tf_op jit(solution)/shard_map/all_to_all | solution.py:492
  35.7 32.0 %copy-start.4 = (bf16[72,1024]{1,0:T(8,128)(2,1)}, bf16[72,1024]{1,0:T(8,128)(2,1)S(1)}, u32[]{:S(2)}) copy-start(bf16[72,1024]{1,0:T(8,128)(2,1)S(1)} %concatenate.3.refs_8_) | copy-start | bytes 442372
  35.7 12.6 %collective-permute-start.7 = (bf16[72,1024]{1,0:T(8,128)(2,1)S(1)}, bf16[72,1024]{1,0:T(8,128)(2,1)S(1)}, u32[]{:S(2)}, u32[]{:S(2)}) collective-permute-start(bf16[72,1024]{1,0:T(8,128)(2,1)S(1)} %concatenate.3.refs_8_), channel_id=1, source_target_pairs={{0,160},{32,192},{64,224},{96,0},{128,32},{160,64},{192,96},{224,1... | collective-permute-start | bytes 442376 | tf_op jit(solution)/shard_map/ppermute | solution.py:32
  36.1 12.2 %collective-permute-start.6 = (bf16[72,1024]{1,0:T(8,128)(2,1)S(1)}, bf16[72,1024]{1,0:T(8,128)(2,1)S(1)}, u32[]{:S(2)}, u32[]{:S(2)}) collective-permute-start(bf16[72,1024]{1,0:T(8,128)(2,1)S(1)} %concatenate.3.refs_8_), channel_id=1, source_target_pairs={{0,96},{32,128},{64,160},{96,192},{128,224},{160,0},{192,32},{224,... | collective-permute-start | bytes 442376 | tf_op jit(solution)/shard_map/ppermute | solution.py:32
  39.0 15.0 %collective-permute-start.8 = (bf16[72,1024]{1,0:T(8,128)(2,1)S(1)}, bf16[72,1024]{1,0:T(8,128)(2,1)S(1)}, u32[]{:S(2)}, u32[]{:S(2)}) collective-permute-start(bf16[72,1024]{1,0:T(8,128)(2,1)S(1)} %concatenate.3.refs_8_), channel_id=1, source_target_pairs={{0,192},{32,224},{64,0},{96,32},{128,64},{160,96},{192,128},{224,1... | collective-permute-start | bytes 442376 | tf_op jit(solution)/shard_map/ppermute | solution.py:32
  41.0 15.5 %collective-permute-start.9 = (bf16[72,1024]{1,0:T(8,128)(2,1)S(1)}, bf16[72,1024]{1,0:T(8,128)(2,1)S(1)}, u32[]{:S(2)}, u32[]{:S(2)}) collective-permute-start(bf16[72,1024]{1,0:T(8,128)(2,1)S(1)} %concatenate.3.refs_8_), channel_id=1, source_target_pairs={{0,64},{32,96},{64,128},{96,160},{128,192},{160,224},{192,0},{224,... | collective-permute-start | bytes 442376 | tf_op jit(solution)/shard_map/ppermute | solution.py:32
  41.4 17.3 %collective-permute-start.10 = (bf16[72,1024]{1,0:T(8,128)(2,1)S(1)}, bf16[72,1024]{1,0:T(8,128)(2,1)S(1)}, u32[]{:S(2)}, u32[]{:S(2)}) collective-permute-start(bf16[72,1024]{1,0:T(8,128)(2,1)S(1)} %concatenate.3.refs_8_), channel_id=1, source_target_pairs={{0,32},{32,64},{64,96},{96,128},{128,160},{160,192},{192,224},{224... | collective-permute-start | bytes 442376 | tf_op jit(solution)/shard_map/ppermute | solution.py:32
  48.3 19.4 %copy-start.11 = (bf16[72,1024]{1,0:T(8,128)(2,1)}, bf16[72,1024]{1,0:T(8,128)(2,1)S(1)}, u32[]{:S(2)}) copy-start(bf16[72,1024]{1,0:T(8,128)(2,1)S(1)} %collective-permute-done.7.refs_10_) | copy-start | bytes 442372
  48.3 12.3 %collective-permute-start.11 = (bf16[72,1024]{1,0:T(8,128)(2,1)S(1)}, bf16[72,1024]{1,0:T(8,128)(2,1)S(1)}, u32[]{:S(2)}, u32[]{:S(2)}) collective-permute-start(bf16[72,1024]{1,0:T(8,128)(2,1)S(1)} %concatenate.3.refs_8_), channel_id=1, source_target_pairs={{0,224},{32,0},{64,32},{96,64},{128,96},{160,128},{192,160},{224,1... | collective-permute-start | bytes 442376 | tf_op jit(solution)/shard_map/ppermute | solution.py:32
  48.3 19.4 %copy-start.12 = (bf16[72,1024]{1,0:T(8,128)(2,1)}, bf16[72,1024]{1,0:T(8,128)(2,1)S(1)}, u32[]{:S(2)}) copy-start(bf16[72,1024]{1,0:T(8,128)(2,1)S(1)} %collective-permute-done.6.refs_9_) | copy-start | bytes 442372
  48.3 12.6 %collective-permute-start.13 = (bf16[72,1024]{1,0:T(8,128)(2,1)S(1)}, bf16[72,1024]{1,0:T(8,128)(2,1)S(1)}, u32[]{:S(2)}, u32[]{:S(2)}) collective-permute-start(bf16[72,1024]{1,0:T(8,128)(2,1)S(1)} %concatenate.3.refs_8_), channel_id=1, source_target_pairs={{0,1},{1,0},{2,3},{3,2},{4,5},{5,4},{6,7},{7,6},{8,9},{9,8},{10,11... | collective-permute-start | bytes 442376 | tf_op jit(solution)/shard_map/ppermute | solution.py:27
  54.0 13.6 %copy-start.13 = (bf16[72,1024]{1,0:T(8,128)(2,1)}, bf16[72,1024]{1,0:T(8,128)(2,1)S(1)}, u32[]{:S(2)}) copy-start(bf16[72,1024]{1,0:T(8,128)(2,1)S(1)} %collective-permute-done.8.refs_11_) | copy-start | bytes 442372
  54.0 7.8 %collective-permute-start.12 = (bf16[72,1024]{1,0:T(8,128)(2,1)S(1)}, bf16[72,1024]{1,0:T(8,128)(2,1)S(1)}, u32[]{:S(2)}, u32[]{:S(2)}) collective-permute-start(bf16[72,1024]{1,0:T(8,128)(2,1)S(1)} %collective-permute-done.7.refs_10_), channel_id=1, source_target_pairs={{0,224},{32,0},{64,32},{96,64},{128,96},{160,128},{192,160},{224,1... | collective-permute-start | bytes 442376 | tf_op jit(solution)/shard_map/ppermute | solution.py:32
  56.5 9.6 %copy-start.14 = (bf16[72,1024]{1,0:T(8,128)(2,1)}, bf16[72,1024]{1,0:T(8,128)(2,1)S(1)}, u32[]{:S(2)}) copy-start(bf16[72,1024]{1,0:T(8,128)(2,1)S(1)} %collective-permute-done.9.refs_12_) | copy-start | bytes 442372
  56.5 5.7 %collective-permute-start.15 = (bf16[72,1024]{1,0:T(8,128)(2,1)S(1)}, bf16[72,1024]{1,0:T(8,128)(2,1)S(1)}, u32[]{:S(2)}, u32[]{:S(2)}) collective-permute-start(bf16[72,1024]{1,0:T(8,128)(2,1)S(1)} %collective-permute-done.7.refs_10_), channel_id=1, source_target_pairs={{0,1},{1,0},{2,3},{3,2},{4,5},{5,4},{6,7},{7,6},{8,9},{9,8},{10,11... | collective-permute-start | bytes 442376 | tf_op jit(solution)/shard_map/ppermute | solution.py:27
  58.7 7.4 %copy-start.15 = (bf16[72,1024]{1,0:T(8,128)(2,1)}, bf16[72,1024]{1,0:T(8,128)(2,1)S(1)}, u32[]{:S(2)}) copy-start(bf16[72,1024]{1,0:T(8,128)(2,1)S(1)} %collective-permute-done.10.refs_13_) | copy-start | bytes 442372
  58.7 4.3 %collective-permute-start.14 = (bf16[72,1024]{1,0:T(8,128)(2,1)S(1)}, bf16[72,1024]{1,0:T(8,128)(2,1)S(1)}, u32[]{:S(2)}, u32[]{:S(2)}) collective-permute-start(bf16[72,1024]{1,0:T(8,128)(2,1)S(1)} %collective-permute-done.6.refs_9_), channel_id=1, source_target_pairs={{0,1},{1,0},{2,3},{3,2},{4,5},{5,4},{6,7},{7,6},{8,9},{9,8},{10,11... | collective-permute-start | bytes 442376 | tf_op jit(solution)/shard_map/ppermute | solution.py:27
  60.6 5.5 %copy-start.16 = (bf16[72,1024]{1,0:T(8,128)(2,1)}, bf16[72,1024]{1,0:T(8,128)(2,1)S(1)}, u32[]{:S(2)}) copy-start(bf16[72,1024]{1,0:T(8,128)(2,1)S(1)} %collective-permute-done.11.refs_14_) | copy-start | bytes 442372
  60.6 2.7 %collective-permute-start.16 = (bf16[72,1024]{1,0:T(8,128)(2,1)S(1)}, bf16[72,1024]{1,0:T(8,128)(2,1)S(1)}, u32[]{:S(2)}, u32[]{:S(2)}) collective-permute-start(bf16[72,1024]{1,0:T(8,128)(2,1)S(1)} %collective-permute-done.8.refs_11_), channel_id=1, source_target_pairs={{0,1},{1,0},{2,3},{3,2},{4,5},{5,4},{6,7},{7,6},{8,9},{9,8},{10,11... | collective-permute-start | bytes 442376 | tf_op jit(solution)/shard_map/ppermute | solution.py:27
  61.6 4.5 %collective-permute-start.3 = (bf16[88,2048]{1,0:T(8,128)(2,1)S(1)}, bf16[88,2048]{1,0:T(8,128)(2,1)S(1)}, u32[]{:S(2)}, u32[]{:S(2)}) collective-permute-start(bf16[88,2048]{1,0:T(8,128)(2,1)S(1)} %bitcast.25), channel_id=1, source_target_pairs={{0,1},{1,0},{2,3},{3,2},{4,5},{5,4},{6,7},{7,6},{8,9},{9,8},{10,11... | collective-permute-start | bytes 1081352 | tf_op jit(solution)/shard_map/ppermute | solution.py:27
  61.8 4.4 %copy-start.18 = (bf16[72,1024]{1,0:T(8,128)(2,1)}, bf16[72,1024]{1,0:T(8,128)(2,1)S(1)}, u32[]{:S(2)}) copy-start(bf16[72,1024]{1,0:T(8,128)(2,1)S(1)} %collective-permute-done.12.refs_15_) | copy-start | bytes 442372
  61.8 4.3 %collective-permute-start.4 = (bf16[88,2048]{1,0:T(8,128)(2,1)S(1)}, bf16[88,2048]{1,0:T(8,128)(2,1)S(1)}, u32[]{:S(2)}, u32[]{:S(2)}) collective-permute-start(bf16[88,2048]{1,0:T(8,128)(2,1)S(1)} %bitcast.27), channel_id=1, source_target_pairs={{0,1},{1,0},{2,3},{3,2},{4,5},{5,4},{6,7},{7,6},{8,9},{9,8},{10,11... | collective-permute-start | bytes 1081352 | tf_op jit(solution)/shard_map/ppermute | solution.py:27
  62.8 3.3 %collective-permute-start.5 = (bf16[88,2048]{1,0:T(8,128)(2,1)S(1)}, bf16[88,2048]{1,0:T(8,128)(2,1)S(1)}, u32[]{:S(2)}, u32[]{:S(2)}) collective-permute-start(bf16[88,2048]{1,0:T(8,128)(2,1)S(1)} %bitcast.29), channel_id=1, source_target_pairs={{0,1},{1,0},{2,3},{3,2},{4,5},{5,4},{6,7},{7,6},{8,9},{9,8},{10,11... | collective-permute-start | bytes 1081352 | tf_op jit(solution)/shard_map/ppermute | solution.py:27
  63.1 3.1 %copy-start.20 = (bf16[72,1024]{1,0:T(8,128)(2,1)}, bf16[72,1024]{1,0:T(8,128)(2,1)S(1)}, u32[]{:S(2)}) copy-start(bf16[72,1024]{1,0:T(8,128)(2,1)S(1)} %collective-permute-done.14.refs_17_) | copy-start | bytes 442372
  63.1 1.7 %collective-permute-start.17 = (bf16[72,1024]{1,0:T(8,128)(2,1)S(1)}, bf16[72,1024]{1,0:T(8,128)(2,1)S(1)}, u32[]{:S(2)}, u32[]{:S(2)}) collective-permute-start(bf16[72,1024]{1,0:T(8,128)(2,1)S(1)} %collective-permute-done.9.refs_12_), channel_id=1, source_target_pairs={{0,1},{1,0},{2,3},{3,2},{4,5},{5,4},{6,7},{7,6},{8,9},{9,8},{10,11... | collective-permute-start | bytes 442376 | tf_op jit(solution)/shard_map/ppermute | solution.py:27
  63.3 2.8 %copy-start.21 = (bf16[72,1024]{1,0:T(8,128)(2,1)}, bf16[72,1024]{1,0:T(8,128)(2,1)S(1)}, u32[]{:S(2)}) copy-start(bf16[72,1024]{1,0:T(8,128)(2,1)S(1)} %collective-permute-done.16.refs_19_) | copy-start | bytes 442372
  63.4 1.6 %collective-permute-start.18 = (bf16[72,1024]{1,0:T(8,128)(2,1)S(1)}, bf16[72,1024]{1,0:T(8,128)(2,1)S(1)}, u32[]{:S(2)}, u32[]{:S(2)}) collective-permute-start(bf16[72,1024]{1,0:T(8,128)(2,1)S(1)} %collective-permute-done.10.refs_13_), channel_id=1, source_target_pairs={{0,1},{1,0},{2,3},{3,2},{4,5},{5,4},{6,7},{7,6},{8,9},{9,8},{10,11... | collective-permute-start | bytes 442376 | tf_op jit(solution)/shard_map/ppermute | solution.py:27
  64.7 1.5 %copy-start.22 = (bf16[72,1024]{1,0:T(8,128)(2,1)}, bf16[72,1024]{1,0:T(8,128)(2,1)S(1)}, u32[]{:S(2)}) copy-start(bf16[72,1024]{1,0:T(8,128)(2,1)S(1)} %collective-permute-done.17.refs_20_) | copy-start | bytes 442372
  64.7 1.4 %collective-permute-start.19 = (bf16[72,1024]{1,0:T(8,128)(2,1)S(1)}, bf16[72,1024]{1,0:T(8,128)(2,1)S(1)}, u32[]{:S(2)}, u32[]{:S(2)}) collective-permute-start(bf16[72,1024]{1,0:T(8,128)(2,1)S(1)} %collective-permute-done.11.refs_14_), channel_id=1, source_target_pairs={{0,1},{1,0},{2,3},{3,2},{4,5},{5,4},{6,7},{7,6},{8,9},{9,8},{10,11... | collective-permute-start | bytes 442376 | tf_op jit(solution)/shard_map/ppermute | solution.py:27
  65.0 1.2 %copy-start.23 = (bf16[72,1024]{1,0:T(8,128)(2,1)}, bf16[72,1024]{1,0:T(8,128)(2,1)S(1)}, u32[]{:S(2)}) copy-start(bf16[72,1024]{1,0:T(8,128)(2,1)S(1)} %collective-permute-done.18.refs_21_) | copy-start | bytes 442372
  65.0 2.7 %collective-permute-start.20 = (bf16[72,1024]{1,0:T(8,128)(2,1)S(1)}, bf16[72,1024]{1,0:T(8,128)(2,1)}, u32[]{:S(2)}, u32[]{:S(2)}) collective-permute-start(bf16[72,1024]{1,0:T(8,128)(2,1)S(1)} %collective-permute-done.12.refs_15_), channel_id=1, source_target_pairs={{0,1},{1,0},{2,3},{3,2},{4,5},{5,4},{6,7},{7,6},{8,9},{9,8},{10,11... | collective-permute-start | bytes 442376 | tf_op jit(solution)/shard_map/ppermute | solution.py:27
  66.1 1.6 %copy-start.8 = (bf16[88,2048]{1,0:T(8,128)(2,1)}, bf16[88,2048]{1,0:T(8,128)(2,1)S(1)}, u32[]{:S(2)}) copy-start(bf16[88,2048]{1,0:T(8,128)(2,1)S(1)} %collective-permute-done.3.refs_5_) | copy-start | bytes 1081348
  66.1 0.8 copy-start.9
  101.4 14.8 %all-to-all-start.3 = ((bf16[16,3,1024]{2,1,0:T(4,128)(2,1)}), bf16[16,3,1024]{2,1,0:T(4,128)(2,1)S(1)}, u32[]{:S(2)}, u32[]{:S(2)}) async-start(bf16[16,3,1024]{2,1,0:T(4,128)(2,1)} %collect.1), calls=%async_computation.3 | async-start | bytes 262144 | tf_op jit(solution)/shard_map/all_to_all | solution.py:498
  (4 other events, 2.7 us)
